TPU v7x, 128 devices: a 2x2x16 block of a 8x8x16 slice. The times are simulated.
128 devices in a mesh: grp: 4 (over y, x), ep: 32 (over z, core).
Axes of the slice: x: 2, y: 2, z: 16, core: 2. Of those that a mesh axis runs over, the one named last changes fastest.
The devices are a block of a 8x8x16 slice.
Arguments:
- tokens: bfloat16 [65536, 2048], P(('grp', 'ep')), parts along dimension 0, may hold values from -6 to 6
- norm_gain: float32 [2048], replicated, may hold values from 0.1 to 1.9
- route_ids: int32 [65536, 2], P(('grp', 'ep')), parts along dimension 0, may hold values from 0 to 31, all different within a row; in each aligned block of 512 rows (0 to 511, 512 to 1023, ...) at most 48 rows name the same one
- route_gates: float32 [65536, 2], P(('grp', 'ep')), parts along dimension 0, may hold values from 0.05 to 1
- w_gate: bfloat16 [32, 2048, 1024], P('ep'), may hold values from -0.125 to 0.125
- w_up: bfloat16 [32, 2048, 1024], P('ep'), may hold values from -0.125 to 0.125
- w_down: bfloat16 [32, 1024, 2048], P('ep'), may hold values from -0.1875 to 0.1875
Outputs:
- mixed: bfloat16 [65536, 2048], P(('grp', 'ep')), parts along dimension 0
There are 4 independent parts, one for each index of `grp`. A program takes and returns all parts, laid end to end along the dimension named above; an argument that names none is the same for every part. Nothing has to cross between parts.
Inputs may be any that keep to these rules, and one draw needn't show every extreme that they name: `route_ids`: each row names 2 different experts. Among the rows of one device no expert is named more than 48 times, and in some devices' rows one expert is named exactly 48 times.
All inputs are finite; a program needn't handle non-finite values.
Results may differ from a plain program's by a relative error of at most 0.0071.
Values may be sent and summed in bfloat16 or wider, within the bound.
No kernel may reach another device: no remote copies, remote signals or barrier semaphores. Data moves between devices by JAX's collectives and lax.ppermute only.
A program may use at most 128 MiB of HBM per device.

v0:
```python
import jax
import jax.numpy as jnp
from jax import lax
from jax.sharding import PartitionSpec as P

EPS = 1e-06


def rms_norm(tokens, norm_gain):
    floats = tokens.astype(jnp.float32)
    scale = lax.rsqrt(jnp.mean(floats * floats, axis=-1, keepdims=True) + EPS)
    return (floats * scale * norm_gain).astype(jnp.bfloat16)


def slot_index(route_ids, experts, capacity):
    flat_ids = route_ids.reshape(-1)
    onehot = (flat_ids[:, None] == jnp.arange(experts, dtype=jnp.int32)[None, :]).astype(jnp.int32)
    ranked = jnp.cumsum(onehot, axis=0) - onehot
    return flat_ids * capacity + jnp.sum(ranked * onehot, axis=1)


def expert_block(arrived, w_gate, w_up, w_down):
    gate_pre = jnp.einsum("sjcd,jdf->sjcf", arrived, w_gate, preferred_element_type=jnp.float32)
    up_pre = jnp.einsum("sjcd,jdf->sjcf", arrived, w_up, preferred_element_type=jnp.float32)
    hidden = (jax.nn.silu(gate_pre) * up_pre).astype(jnp.bfloat16)
    return jnp.einsum("sjcf,jfd->sjcd", hidden, w_down, preferred_element_type=jnp.float32).astype(
        jnp.bfloat16
    )


def body(tokens, norm_gain, route_ids, route_gates, w_gate, w_up, w_down):
    tok_rows, width = tokens.shape
    top_count = route_ids.shape[1]
    devices = lax.axis_size("ep")
    local_experts = w_gate.shape[0]
    experts = local_experts * devices
    capacity = 3 * tok_rows * top_count // (2 * experts)
    normed = rms_norm(tokens, norm_gain)
    weights = route_gates / jnp.sum(route_gates, axis=1, keepdims=True)
    places = slot_index(route_ids, experts, capacity)
    row_of = jnp.arange(tok_rows * top_count, dtype=jnp.int32) // top_count
    outgoing = jnp.zeros((experts * capacity, width), jnp.bfloat16).at[places].set(normed[row_of])
    outgoing = outgoing.reshape(devices, local_experts, capacity, width)
    finished = expert_block(
        lax.all_to_all(outgoing, "ep", split_axis=0, concat_axis=0, tiled=True),
        w_gate,
        w_up,
        w_down,
    )
    returned = lax.all_to_all(finished, "ep", split_axis=0, concat_axis=0, tiled=True)
    picked = returned.reshape(experts * capacity, width)[places]
    shaped = picked.astype(jnp.float32).reshape(tok_rows, top_count, width)
    return jnp.sum(shaped * weights[:, :, None], axis=1).astype(jnp.bfloat16)


def solution(mesh):
    placed = (
        P(("grp", "ep"), None),
        P(),
        P(("grp", "ep"), None),
        P(("grp", "ep"), None),
        P("ep", None, None),
        P("ep", None, None),
        P("ep", None, None),
    )
    return jax.shard_map(
        body, mesh=mesh, in_specs=placed, out_specs=P(("grp", "ep"), None), check_vma=False
    )
```

profile of v0, /device:TPU:70, one launch (start us, length us, event | category | flops | bytes accessed | tf_op | source)
XLA Modules:
  0.0 682.9 jit_solution(12134281093027894184)
XLA Ops:
  0.0 0.0 copy-start
  0.0 0.0 copy-start.2
  0.0 1.0 copy.16
  1.0 0.2 eq.29
  1.2 0.2 eq.25
  1.3 0.7 broadcast_multiply_fusion
  2.0 9.0 %reduce-window.6 = s32[32,8,128]{2,1,0:T(8,128)S(1)} reduce-window(s32[32,8,128]{2,1,0:T(8,128)S(1)} %fusion.25, s32[]{:T(128)} %constant.31.clone.1), window={size=1x1x128 pad=0_0x0_0x127_0}, to_apply=%region_0.0 | reduce-window | flops 4161536 | bytes 262148 | tf_op jit(solution)/shard_map/reduce-window
  11.1 0.1 slice.12
  11.2 0.1 copy.18
  11.3 0.1 copy.19
  11.4 0.1 broadcast_add_fusion
  11.5 0.1 copy.15
  11.7 0.2 mul.55
  11.9 2.1 fusion.8
  14.0 0.0 copy-done
  14.0 0.0 copy-done.2
  14.0 1.9 fusion.10
  15.9 22.0 %scatter_custom_fusion = bf16[1536,2048]{1,0:T(8,128)(2,1)} fusion(s32[1024]{0:T(1024)S(1)} %bitcast.84, bf16[512,2048]{1,0:T(8,128)(2,1)} %fusion.10, s32[1024]{0:T(1024)S(1)} %broadcast_clamp_fusion.1, bf16[]{:T(256)} %constant.29.clone.1), kind=kCustom, calls=%fused_computation.24 | custom fusion | bytes 6291968 | tf_op jit(solution)/shard_map/scatter | solution.py:42
  37.9 0.0 copy-start.3
  37.9 298.1 %all_to_all.10 = bf16[32,1,48,2048]{3,2,1,0:T(8,128)(2,1)S(1)} all-to-all(bf16[32,1,48,2048]{3,2,1,0:T(8,128)(2,1)} %bitcast.80), channel_id=1, replica_groups=mesh['grp'=4,'ep'=32] {'ep'}, dimensions={0} | all-to-all | bytes 12582912 | tf_op jit(solution)/shard_map/all_to_all | solution.py:45
  336.0 0.0 copy-done.3
  336.0 0.0 copy-start.4
  336.0 6.8 fusion.4
  342.8 0.0 copy-done.4
  342.8 0.0 copy-start.5
  342.8 7.7 %fusion = bf16[32,1,48,1024]{3,2,0,1:T(8,128)(2,1)S(1)} fusion(f32[32,48,1024]{2,1,0:T(8,128)S(1)} %fusion.4, bf16[1,2048,1024]{2,1,0:T(8,128)(2,1)S(1)} %copy-done.4, bf16[32,1,48,2048]{3,2,1,0:T(8,128)(2,1)S(1)} %all_to_all.10), kind=kOutput, calls=%fused_computation.5 | convolution fusion | flops 6451888128 | bytes 19922944 | tf_op jit(solution)/shard_map/sjcd,jdf->sjcf/dot_general | solution.py:23
  350.5 0.0 copy-done.5
  350.5 8.7 %convert_bitcast_fusion = bf16[32,1,48,2048]{3,2,1,0:T(8,128)(2,1)} fusion(bf16[1,1024,2048]{2,1,0:T(8,128)(2,1)S(1)} %copy-done.5, bf16[32,1,48,1024]{3,2,0,1:T(8,128)(2,1)S(1)} %fusion), kind=kOutput, calls=%fused_computation.15 | convolution fusion | flops 6445596672 | bytes 13631488 | tf_op jit(solution)/shard_map/sjcf,jfd->sjcd/dot_general | solution.py:26
  359.2 0.0 copy-start.1
  359.2 6.1 all-to-all-start.1
  365.3 0.0 copy-done.1
  365.3 0.1 copy.21
  365.5 280.3 %all-to-all-done.1 = bf16[32,1,48,2048]{3,2,1,0:T(8,128)(2,1)} async-done(((bf16[32,1,48,2048]{3,2,1,0:T(8,128)(2,1)}), bf16[32,1,48,2048]{3,2,1,0:T(8,128)(2,1)}, u32[]{:S(2)}, u32[]{:S(2)}) %all-to-all-start.1) | async-done | bytes 6291488 | tf_op jit(solution)/shard_map/all_to_all | solution.py:50
  645.8 12.4 %gather_fusion = bf16[1024,2048]{1,0:T(8,128)(2,1)} fusion(bf16[1536,2048]{1,0:T(8,128)(2,1)} %bitcast.26, s32[1024]{0:T(1024)S(1)} %broadcast_clamp_fusion), kind=kCustom, calls=%fused_computation.1 | custom fusion | bytes 8392704 | tf_op jit(solution)/shard_map/gather | solution.py:51
  658.2 9.6 %reshape.138 = f32[512,2,2048]{2,1,0:T(2,128)} reshape(bf16[1024,2048]{1,0:T(8,128)(2,1)} %gather_fusion) | data formatting | bytes 12582912 | tf_op jit(solution)/shard_map/convert_element_type | solution.py:52
  667.9 15.0 %multiply_reduce_fusion = bf16[512,2048]{1,0:T(8,128)(2,1)} fusion(f32[512,2,2048]{2,1,0:T(2,128)} %reshape.138, f32[512,2]{1,0:T(8,128)S(1)} %copy.21), kind=kLoop, calls=%fused_computation.3 | loop fusion | flops 3145728 | bytes 10489856 | tf_op jit(solution)/shard_map/reduce_sum | solution.py:53
  (11 shorter events, 0.1 us)
Async XLA Ops:
  0.0 14.0 %copy-start = (bf16[512,2048]{1,0:T(8,128)(2,1)S(1)}, bf16[512,2048]{1,0:T(8,128)(2,1)}, u32[]{:S(2)}) copy-start(bf16[512,2048]{1,0:T(8,128)(2,1)} %param.7) | copy-start | bytes 6291460
  0.0 14.0 %copy-start.2 = (f32[2048]{0:T(1024)S(1)}, f32[2048]{0:T(1024)}, u32[]{:S(2)}) copy-start(f32[2048]{0:T(1024)} %param.8) | copy-start | bytes 24580
  37.9 298.1 %copy-start.3 = (bf16[1,2048,1024]{2,1,0:T(8,128)(2,1)S(1)}, bf16[1,2048,1024]{2,1,0:T(8,128)(2,1)}, u32[]{:S(2)}) copy-start(bf16[1,2048,1024]{2,1,0:T(8,128)(2,1)} %param.12) | copy-start | bytes 12582916
  336.0 6.8 copy-start.4
  342.8 7.7 %copy-start.5 = (bf16[1,1024,2048]{2,1,0:T(8,128)(2,1)S(1)}, bf16[1,1024,2048]{2,1,0:T(8,128)(2,1)}, u32[]{:S(2)}) copy-start(bf16[1,1024,2048]{2,1,0:T(8,128)(2,1)} %param.13) | copy-start | bytes 12582916
  359.2 6.1 copy-start.1
  359.2 286.6 %all-to-all-start.1 = ((bf16[32,1,48,2048]{3,2,1,0:T(8,128)(2,1)}), bf16[32,1,48,2048]{3,2,1,0:T(8,128)(2,1)}, u32[]{:S(2)}, u32[]{:S(2)}) async-start(bf16[32,1,48,2048]{3,2,1,0:T(8,128)(2,1)} %convert_bitcast_fusion), calls=%async_computation.1 | async-start | bytes 12582912 | tf_op jit(solution)/shard_map/all_to_all | solution.py:50
where the time goes:
time: 684 us; the launch traced here: 683 us
  blocking collectives  298 us (44%)
  waiting for transfers between devices  280 us (41%)
  local copies, waits for them, and re-layouts  46.2 us (7%)
  other arithmetic  28.9 us (4%)
  matrix products  23.2 us (3%)
    all_to_all x1, blocking collectives, body(): lax.all_to_all(outgoing, 'ep', split_axis=0, concat_axis=0, tiled=True)  298 us
    all_to_all x1, waiting for transfers between devices, body(): lax.all_to_all(finished, 'ep', split_axis=0, concat_axis=0, tiled=True)  280 us
    scatter x1, local copies, waits for them, and re-layouts, body(): jnp.zeros((experts * capacity, width), jnp.bfloat16).at[places]  22 us
    reduce_sum x1, other arithmetic, body(): return jnp.sum(shaped * weights[:, :, None], axis=1).astype(jnp.bfloat16)  15 us
  transfers between devices with their start and end apart: 1, of which 1 were waited for; matrix products, arithmetic and copies ran while one was open for 0% of the time, Pallas kernels for 0%

commit v1 on v0

v1 whole, which is shorter than its diff:
```python
import jax
import jax.numpy as jnp
from jax import lax
from jax.sharding import PartitionSpec as P

EPS = 1e-06
BF16, F32 = jnp.bfloat16, jnp.float32


def rms_norm(tokens, norm_gain):
    floats = tokens.astype(F32)
    scale = lax.rsqrt(jnp.mean(floats * floats, axis=-1, keepdims=True) + EPS)
    return (floats * scale * norm_gain).astype(BF16)


def dot(a, b):
    return jnp.dot(a, b, preferred_element_type=F32)


def ranks_of(route_ids, experts):
    rows = route_ids.shape[0]
    names = route_ids[:, :, None] == jnp.arange(experts, dtype=jnp.int32)
    member = jnp.any(names, axis=1)
    earlier = jnp.arange(rows)[:, None] > jnp.arange(rows)[None, :]
    return names, dot(earlier.astype(BF16), member.astype(BF16)).astype(jnp.int32)


def split_weight(weight):
    high = weight.astype(BF16)
    return high, (weight - high.astype(F32)).astype(BF16)


def expert_rows(rows, w_gate, w_up, w_down):
    gate_pre, up_pre = dot(rows, w_gate[0]), dot(rows, w_up[0])
    hidden = (jax.nn.silu(gate_pre) * up_pre).astype(BF16)
    return dot(hidden, w_down[0]).astype(BF16)


def body(tokens, norm_gain, route_ids, route_gates, w_gate, w_up, w_down):
    tok_rows, width = tokens.shape
    top_count = route_ids.shape[1]
    experts = lax.axis_size("ep") * w_gate.shape[0]
    capacity = 3 * tok_rows * top_count // (2 * experts)
    normed = rms_norm(tokens, norm_gain)
    weights = route_gates / jnp.sum(route_gates, axis=1, keepdims=True)
    names, ranks = ranks_of(route_ids, experts)
    places = route_ids * capacity + jnp.sum(names * ranks[:, None, :], axis=2)
    slots = jnp.arange(experts * capacity, dtype=jnp.int32)
    hits = [slots[:, None] == places[None, :, k] for k in range(top_count)]
    pick = sum(hit.astype(BF16) for hit in hits)
    outgoing = dot(pick, normed).astype(BF16)
    arrived = lax.all_to_all(outgoing.reshape(experts, capacity, width), "ep", split_axis=0, concat_axis=0, tiled=True)
    finished = expert_rows(arrived.reshape(experts * capacity, width), w_gate, w_up, w_down)
    returned = lax.all_to_all(finished.reshape(experts, capacity, width), "ep", split_axis=0, concat_axis=0, tiled=True)
    returned = returned.reshape(experts * capacity, width)
    high, low = split_weight(weights)
    spread = lambda part: sum(
        jnp.where(places[:, k : k + 1] == slots[None, :], part[:, k : k + 1], 0) for k in range(top_count)
    )
    return (dot(spread(high), returned) + dot(spread(low), returned)).astype(BF16)


def solution(mesh):
    rows = P(("grp", "ep"), None)
    by_expert = P("ep", None, None)
    placed = (rows, P(), rows, rows, by_expert, by_expert, by_expert)
    return jax.shard_map(body, mesh=mesh, in_specs=placed, out_specs=rows, check_vma=False)
```

time: 684 us -> 641 us (0.937)
  local copies, waits for them, and re-layouts: 46.2 us -> 2.66 us
  matrix products: 23.2 us -> 49.3 us
  other arithmetic: 28.9 us -> 4.24 us
    dot_general x3 -> x6, matrix products: 23.2 us -> 49.3 us  [dot(): return jnp.dot(a, b, preferred_element_type=F32)]
    scatter x1 -> x0, local copies, waits for them, and re-layouts: 22 us -> none  [body(): jnp.zeros((experts * capacity, width), jnp.bfloat16).at[places]]
    reduce_sum x2 -> x1, other arithmetic: 15.1 us -> 0.72 us  [body(): places = route_ids * capacity + jnp.sum(names * ranks[:, None, :], axis=2)]
    gather x1 -> x0, local copies, waits for them, and re-layouts: 12.4 us -> none  [body(): picked = returned.reshape(experts * capacity, width)[places]]
    convert_element_type x1 -> x0, local copies, waits for them, and re-layouts: 9.65 us -> none  [body(): shaped = picked.astype(jnp.float32).reshape(tok_rows, top_count, width)]
    another operation x3 -> x0, other arithmetic: 9.15 us -> none
where the time goes in v1:
time: 641 us; the launch traced here: 640 us
  blocking collectives  298 us (46%)
  waiting for transfers between devices  280 us (44%)
  matrix products  49.3 us (8%)
    all_to_all x1, blocking collectives, body(): lax.all_to_all(outgoing.reshape(experts, capacity, width), 'ep', split_ax...  298 us
    all_to_all x1, waiting for transfers between devices, body(): lax.all_to_all(finished.reshape(experts, capacity, width), 'ep', split_ax...  280 us
    dot_general x6, matrix products, dot(): return jnp.dot(a, b, preferred_element_type=F32)  49.3 us
  transfers between devices with their start and end apart: 1, of which 1 were waited for; matrix products, arithmetic and copies ran while one was open for 0% of the time, Pallas kernels for 0%

profile of v1, /device:TPU:70, one launch (start us, length us, event | category | flops | bytes accessed | tf_op | source)
XLA Modules:
  0.0 640.4 jit_solution(8372310245475472307)
XLA Ops:
  0.0 0.7 fusion.41
  0.7 0.3 convolution_convert_fusion.2
  1.0 0.7 select_reduce_fusion
  1.7 0.7 multiply_add_fusion
  2.4 2.1 fusion
  4.5 5.7 convolution_convert_fusion.1
  10.2 0.0 copy-start.2
  10.2 297.9 %all_to_all.10 = bf16[32,48,2048]{2,1,0:T(8,128)(2,1)S(1)} all-to-all(bf16[32,48,2048]{2,1,0:T(8,128)(2,1)S(1)} %bitcast.25), channel_id=1, replica_groups=mesh['grp'=4,'ep'=32] {'ep'}, dimensions={0} | all-to-all | bytes 12582912 | tf_op jit(solution)/shard_map/all_to_all | solution.py:52
  308.1 0.0 copy-start
  308.1 2.6 copy-done
  310.7 0.0 copy-done.2
  310.7 8.5 %fusion.7 = f32[1536,1024]{1,0:T(8,128)} fusion(bf16[1536,2048]{1,0:T(8,128)(2,1)S(1)} %bitcast.23, bf16[1,2048,1024]{2,1,0:T(8,128)(2,1)S(1)} %copy-done.2), kind=kOutput, calls=%fused_computation.10 | convolution fusion | flops 6442450944 | bytes 16777216 | tf_op jit(solution)/shard_map/dot_general | solution.py:17
  319.2 20.6 %convolution_convert_fusion = bf16[1536,2048]{1,0:T(8,128)(2,1)} fusion(bf16[1,1024,2048]{2,1,0:T(8,128)(2,1)} %param.13, f32[1536,1024]{1,0:T(8,128)} %fusion.7, bf16[1536,2048]{1,0:T(8,128)(2,1)} %bitcast.24, bf16[1,2048,1024]{2,1,0:T(8,128)(2,1)} %param.12), kind=kOutput, calls=%fused_computation | convolution fusion | flops 12897484800 | bytes 27262976 | tf_op jit(solution)/shard_map/dot_general | solution.py:17
  339.8 0.0 copy-start.1
  339.8 6.0 all-to-all-start.1
  345.8 0.0 copy-done.1
  345.9 280.3 %all-to-all-done.1 = bf16[32,48,2048]{2,1,0:T(8,128)(2,1)} async-done(((bf16[32,48,2048]{2,1,0:T(8,128)(2,1)}), bf16[32,48,2048]{2,1,0:T(8,128)(2,1)}, u32[]{:S(2)}, u32[]{:S(2)}) %all-to-all-start.1) | async-done | bytes 6291488 | tf_op jit(solution)/shard_map/all_to_all | solution.py:54
  626.2 6.4 fusion.23
  632.6 7.8 %add_convert_fusion = bf16[512,2048]{1,0:T(8,128)(2,1)} fusion(f32[512,2048]{1,0:T(8,128)S(1)} %fusion.23, bf16[1536,2048]{1,0:T(8,128)(2,1)} %bitcast.8, s32[512]{0:T(512)S(1)} %bitcast.31, s32[512]{0:T(512)S(1)} %bitcast.28, bf16[512]{0:T(512)(128)(2,1)S(1)} %get-tuple-element.6, bf16[512]{0:T(512)(128)(2,1)S(1)} %get-tuple-element.5), kind=kOutput, calls=%fused_computation.12 | convolution fusion | flops 3229614080 | bytes 12589056 | tf_op jit(solution)/shard_map/dot_general | solution.py:17
  (5 shorter events, 0.1 us)
Async XLA Ops:
  10.2 300.5 %copy-start.2 = (bf16[1,2048,1024]{2,1,0:T(8,128)(2,1)S(1)}, bf16[1,2048,1024]{2,1,0:T(8,128)(2,1)}, u32[]{:S(2)}) copy-start(bf16[1,2048,1024]{2,1,0:T(8,128)(2,1)} %param.11) | copy-start | bytes 12582916
  308.1 2.6 copy-start
  339.8 6.0 copy-start.1
  339.8 286.4 %all-to-all-start.1 = ((bf16[32,48,2048]{2,1,0:T(8,128)(2,1)}), bf16[32,48,2048]{2,1,0:T(8,128)(2,1)}, u32[]{:S(2)}, u32[]{:S(2)}) async-start(bf16[32,48,2048]{2,1,0:T(8,128)(2,1)} %bitcast.22), calls=%async_computation.1 | async-start | bytes 12582912 | tf_op jit(solution)/shard_map/all_to_all | solution.py:54

commit v2 on v1

v2 whole, which is shorter than its diff:
```python
import jax
import jax.numpy as jnp
import numpy as np
from jax import lax
from jax.sharding import PartitionSpec as P


EPS = 1e-06
BF16, F32, I32 = jnp.bfloat16, jnp.float32, jnp.int32
CORES = 2
HOPS = (528, 480, 424, 368, 328, 264, 224, 144, 80)
NEAR = 4
PARTS = 2
HOLD = 8
BATCHES = ((1, 2, 3, 4), (5, 6, 7, 8, 9))
WAYS = (1, -1)


def rms_norm(tokens, norm_gain):
    floats = tokens.astype(F32)
    scale = lax.rsqrt(jnp.mean(floats * floats, axis=-1, keepdims=True) + EPS)
    return (floats * scale * norm_gain).astype(BF16)


def dot(a, b):
    return jnp.dot(a, b, preferred_element_type=F32)


def ranks_of(ids, experts):
    rows = ids.shape[0]
    names = ids[:, :, None] == jnp.arange(experts, dtype=I32)
    member = jnp.any(names, axis=1)
    earlier = jnp.arange(rows)[:, None] > jnp.arange(rows)[None, :]
    return names, member, dot(earlier.astype(BF16), member.astype(BF16)).astype(I32)


def pick_of(places, slots):
    at = jnp.arange(slots, dtype=I32)[:, None]
    return sum((at == places[None, :, k]).astype(BF16) for k in range(places.shape[1]))


def mix(places, weights, values):
    at = jnp.arange(values.shape[0], dtype=I32)[None, :]
    spread = sum(jnp.where(places[:, k : k + 1] == at, weights[:, k : k + 1], 0) for k in range(places.shape[1]))
    return dot(spread.astype(BF16), values)


def expert_rows(rows, w_gate, w_up, w_down):
    gate_pre, up_pre = dot(rows, w_gate[0]), dot(rows, w_up[0])
    hidden = (jax.nn.silu(gate_pre) * up_pre).astype(BF16)
    return dot(hidden, w_down[0]).astype(BF16)


def direct(normed, weights, ids, capacity, w_gate, w_up, w_down):
    width = normed.shape[1]
    experts = lax.axis_size("ep")
    names, _, ranks = ranks_of(ids, experts)
    places = ids * capacity + jnp.sum(names * ranks[:, None, :], axis=2)
    outgoing = dot(pick_of(places, experts * capacity), normed).astype(BF16)
    arrived = lax.all_to_all(outgoing.reshape(experts, capacity, width), "ep", split_axis=0, concat_axis=0, tiled=True)
    finished = expert_rows(arrived.reshape(experts * capacity, width), w_gate, w_up, w_down)
    returned = lax.all_to_all(finished.reshape(experts, capacity, width), "ep", split_axis=0, concat_axis=0, tiled=True)
    return mix(places, weights, returned.reshape(experts * capacity, width)).astype(BF16)


def body(tokens, norm_gain, route_ids, route_gates, w_gate, w_up, w_down):
    tok_rows, width = tokens.shape
    top_count = route_ids.shape[1]
    experts = lax.axis_size("ep")
    chips = experts // CORES
    capacity = 3 * tok_rows * top_count // (2 * experts)
    far = len(HOPS)
    fixed = HOPS[NEAR]
    me = lax.axis_index("ep")
    chip, core = lax.div(me, CORES), lax.rem(me, CORES)
    step = {
        way: [(z * CORES + c, (z + way) % chips * CORES + c) for z in range(chips) for c in range(CORES)]
        for way in WAYS
    }
    swap = [(i, i ^ 1) for i in range(experts)]
    columns = [slice(part * width // PARTS, (part + 1) * width // PARTS) for part in range(PARTS)]
    hop = lambda block, way: lax.ppermute(block, "ep", step[way])

    near = lax.rem(route_ids + (experts - chip * CORES), experts)
    names, member, ranks = ranks_of(near, experts)
    order = jnp.arange(experts)
    count = jnp.sum(member.astype(I32) * (order >= CORES), axis=0)
    after = jnp.sum(jnp.where(order[None, :] <= order[:, None], count[None, :], 0), axis=1)
    before = after - count
    above, below = np.full(experts, 1 << 20, np.int32), np.full(experts, -(1 << 20), np.int32)
    last = lambda chips_on: CORES * chips_on + CORES - 1
    above[last(far)], below[last(chips - 1 - far)] = 0, 0
    for k, rows in enumerate(HOPS, 1):
        above[last(k - 1)], below[last(chips - k)] = rows, -rows
    most, least = jnp.min(after + above), jnp.max(after + below)
    cut = lax.shift_right_logical(least + most, 1)
    spilt = least > most

    rank = jnp.sum(names * ranks[:, None, :], axis=2)
    seat = rank + jnp.sum(names * before, axis=2)
    local = near < CORES
    places = {
        1: jnp.where(~local & (seat < cut), cut - 1 - seat, -1),
        -1: jnp.where(~local & (seat >= cut), seat - cut, -1),
        0: jnp.where(local, jnp.where(near == core, 0, capacity) + rank, -1),
    }

    normed = rms_norm(tokens, norm_gain)
    weights = route_gates / jnp.sum(route_gates, axis=1, keepdims=True)
    first = lambda way, low, high: dot(pick_of(places[way] - low, high - low), normed).astype(BF16)
    near_block = {way: first(way, fixed, HOPS[0]) for way in WAYS}
    far_block = {}
    for way in WAYS:
        block = first(way, 0, fixed)
        for part in range(PARTS):
            far_block[way, part] = block[:, columns[part]]
    here = first(0, 0, 2 * capacity)

    sent = [jnp.maximum(jnp.minimum(after, cut) - before, 0), jnp.maximum(after - jnp.maximum(before, cut), 0)]
    row = jnp.concatenate(sent + [jnp.full((experts,), spilt, I32)]).astype(F32)
    table = lax.all_to_all(
        jnp.broadcast_to(row, (experts, row.shape[0])), "ep", split_axis=0, concat_axis=0, tiled=True
    )
    spilt = jnp.max(table[:, 2 * experts]) > 0
    hops = jnp.arange(1, far + 1, dtype=I32)
    slot = jnp.arange(capacity, dtype=F32)
    wants = {}
    for i, way in enumerate(WAYS):
        source = lax.rem(chip - way * hops + chips, chips) * CORES + core
        mine = (source[:, None] == order[None, :]).astype(F32)
        counts = jnp.dot(mine, table[:, i * experts : (i + 1) * experts], precision=lax.Precision.HIGHEST)
        aim = CORES * hops if way > 0 else CORES * (chips - hops)
        parts = []
        for to in (core, 1 - core):
            ahead = order[None, :] > aim[:, None] + to if way > 0 else order[None, :] < aim[:, None] + to
            start = jnp.sum(jnp.where(ahead, counts, 0), axis=1)
            size = jnp.sum(jnp.where(order[None, :] == aim[:, None] + to, counts, 0), axis=1)
            parts.append(jnp.where(slot[None, :] < size[:, None], start[:, None] + slot[None, :], -1))
        wants[way] = jnp.concatenate(parts, axis=1)

    def run(got):
        own = jnp.concatenate([g[:capacity] for g in got])
        other = jnp.concatenate([g[capacity:] for g in got])
        n = own.shape[0]
        done = expert_rows(jnp.concatenate([own, lax.ppermute(other, "ep", swap)]), w_gate, w_up, w_down)
        back = lax.ppermute(done[n:], "ep", swap)
        span = lambda i: slice(i * capacity, (i + 1) * capacity)
        return [jnp.concatenate([done[span(i)], back[span(i)]]) for i in range(len(got))]

    def pick(way, k, low, high):
        return (wants[way][k - 1][:, None] == jnp.arange(low, high, dtype=F32)[None, :]).astype(BF16)

    far_at, near_at = {}, {}
    for k in range(1, far + 1):
        for way in WAYS:
            if k <= NEAR:
                near_block[way] = near_at[way, k] = hop(near_block[way][: HOPS[k - 1] - fixed], way)
        for part in range(PARTS):
            for way in WAYS:
                block = hop(far_block[way, part][: min(fixed, HOPS[k - 1])], way)
                far_block[way, part] = far_at[way, k, part] = block

    def select(way, k):
        rows = min(fixed, HOPS[k - 1])
        got = []
        for part in range(PARTS):
            got.append(dot(pick(way, k, 0, rows), far_at[way, k, part]))
        got = jnp.concatenate(got, axis=1)
        if k <= NEAR:
            got = got + dot(pick(way, k, fixed, HOPS[k - 1]), near_at[way, k])
        return got.astype(BF16)

    outs = {}
    for batch in BATCHES:
        keys = [(way, k) for k in batch for way in WAYS]
        got = [select(way, k) for way, k in keys]
        if batch is BATCHES[0]:
            keys.append((0, 0))
            got.append(here)
        outs.update(zip(keys, run(got)))

    held, held_near = {}, {}
    for k in range(NEAR, 0, -1):
        for way in WAYS:
            put = dot(pick(way, k, fixed, HOPS[k - 1]).T, outs[way, k]).astype(BF16)
            if k < NEAR:
                put = put + jnp.pad(held_near[way], ((0, HOPS[k - 1] - HOPS[k]), (0, 0)))
            elif HOLD:
                put, _ = lax.optimization_barrier((put, far_at[way, HOLD, 0]))
            held_near[way] = hop(put, -way)
    for k in range(far, 0, -1):
        rows = min(fixed, HOPS[k - 1])
        for part in range(PARTS):
            for way in WAYS:
                put = dot(pick(way, k, 0, rows).T, outs[way, k][:, columns[part]]).astype(BF16)
                if k < far:
                    got = held[way, part]
                    put = put + jnp.pad(got, ((0, rows - got.shape[0]), (0, 0)))
                held[way, part] = hop(put, -way)

    early = mix(places[0], weights, outs[0, 0])
    for way in WAYS:
        early = early + mix(places[way] - fixed, weights, held_near[way])
    total = []
    for part in range(PARTS):
        last_sum = early[:, columns[part]]
        for way in WAYS:
            last_sum = last_sum + mix(places[way], weights, held[way, part])
        total.append(last_sum.astype(BF16))
    quick = jnp.concatenate(total, axis=1)
    return lax.cond(
        spilt,
        lambda: direct(normed, weights, route_ids, capacity, w_gate, w_up, w_down),
        lambda: quick,
    )


def solution(mesh):
    rows = P(("grp", "ep"), None)
    by_expert = P("ep", None, None)
    placed = (rows, P(), rows, rows, by_expert, by_expert, by_expert)

    return jax.shard_map(body, mesh=mesh, in_specs=placed, out_specs=rows, check_vma=False)
```

time: 641 us -> 629 us (0.981); the launches traced: 640 us -> 620 us
  blocking collectives: 298 us -> 0 us
  starting transfers between devices: 6.03 us -> 155 us
  waiting for transfers between devices: 280 us -> 348 us
  matrix products: 49.3 us -> 79.9 us
  local copies, waits for them, and re-layouts: 2.66 us -> 16.6 us
  other arithmetic: 4.24 us -> 16 us
    ppermute x0 -> x92, waiting for transfers between devices: none -> 348 us  [the longest x88 348 us: body(): hop = lambda block, way: lax.ppermute(block, 'ep', step[way])]
    all_to_all x1 -> x0, blocking collectives: 298 us -> none  [body(): lax.all_to_all(outgoing.reshape(experts, capacity, width), 'ep', split_ax...]
    all_to_all x1, waiting for transfers between devices: 280 us -> 0.01 us  [body(): lax.all_to_all(jnp.broadcast_to(row, (experts, row.shape[0])), 'ep', spli...]
    ppermute x0 -> x92, starting transfers between devices: none -> 137 us  [the longest x88 137 us: body(): hop = lambda block, way: lax.ppermute(block, 'ep', step[way])]
    dot_general x6 -> x107, matrix products: 49.3 us -> 79.3 us  [dot(): return jnp.dot(a, b, preferred_element_type=F32)]
    all_to_all x1, starting transfers between devices: 6.03 us -> 17.8 us  [body(): lax.all_to_all(jnp.broadcast_to(row, (experts, row.shape[0])), 'ep', spli...]
    slice x2 -> x34, local copies, waits for them, and re-layouts: 0.04 us -> 9.73 us  [the longest x2 2.41 us: body(): far_block[way, part] = block[:, columns[part]]]
  transfers between devices with their start and end apart: 1 -> 93, of which waited for: 1 -> 40; matrix products, arithmetic and copies ran while one was open for 0% -> 17% of each run, Pallas kernels for 0% -> 0%
where the time goes in v2:
time: 629 us; the launch traced here: 620 us
  waiting for transfers between devices  348 us (55%)
  starting transfers between devices  155 us (25%)
  matrix products  79.9 us (13%)
  local copies, waits for them, and re-layouts  16.6 us (3%)
  other arithmetic  16 us (3%)
    ppermute x88, waiting for transfers between devices, body(): hop = lambda block, way: lax.ppermute(block, 'ep', step[way])  348 us
    ppermute x88, starting transfers between devices, body(): hop = lambda block, way: lax.ppermute(block, 'ep', step[way])  137 us
    dot_general x107, matrix products, dot(): return jnp.dot(a, b, preferred_element_type=F32)  79.3 us
    all_to_all x1, starting transfers between devices, body(): lax.all_to_all(jnp.broadcast_to(row, (experts, row.shape[0])), 'ep', spli...  17.8 us
  transfers between devices with their start and end apart: 93, of which 40 were waited for; matrix products, arithmetic and copies ran while one was open for 17% of the time, Pallas kernels for 0%

profile of v2, /device:TPU:70, one launch (start us, length us, event | category | flops | bytes accessed | tf_op | source)
XLA Modules:
  0.0 620.4 jit_solution(11156918533564036883)
XLA Ops:
  5.7 17.8 %all-to-all-start.2 = ((f32[32,1,96]{2,1,0:T(1,128)}), f32[32,1,96]{2,1,0:T(1,128)S(1)}, u32[]{:S(2)}, u32[]{:S(2)}) async-start(f32[32,1,96]{2,1,0:T(1,128)} %broadcast_in_dim.145), calls=%async_computation.2 | async-start | bytes 32768 | tf_op jit(solution)/shard_map/all_to_all | solution.py:121
  45.3 23.7 %collective-permute-done.4 = bf16[328,1024]{1,0:T(8,128)(2,1)} collective-permute-done((bf16[328,1024]{1,0:T(8,128)(2,1)}, bf16[328,1024]{1,0:T(8,128)(2,1)}, u32[]{:S(2)}, u32[]{:S(2)}) %collective-permute-start.4) | collective-permute-done | bytes 671776 | tf_op jit(solution)/shard_map/ppermute | solution.py:82
  71.9 10.4 %collective-permute-done.3 = bf16[328,1024]{1,0:T(8,128)(2,1)} collective-permute-done((bf16[328,1024]{1,0:T(8,128)(2,1)}, bf16[328,1024]{1,0:T(8,128)(2,1)}, u32[]{:S(2)}, u32[]{:S(2)}) %collective-permute-start.3) | collective-permute-done | bytes 671776 | tf_op jit(solution)/shard_map/ppermute | solution.py:82
  96.0 5.0 collective-permute-done.10
  108.8 13.9 %collective-permute-done.6 = bf16[328,1024]{1,0:T(8,128)(2,1)S(1)} collective-permute-done((bf16[328,1024]{1,0:T(8,128)(2,1)S(1)}, bf16[328,1024]{1,0:T(8,128)(2,1)S(1)}, u32[]{:S(2)}, u32[]{:S(2)}) %collective-permute-start.6) | collective-permute-done | bytes 671776 | tf_op jit(solution)/shard_map/ppermute | solution.py:82
  123.7 12.3 %collective-permute-done.8 = bf16[152,2048]{1,0:T(8,128)(2,1)S(1)} collective-permute-done((bf16[152,2048]{1,0:T(8,128)(2,1)S(1)}, bf16[152,2048]{1,0:T(8,128)(2,1)S(1)}, u32[]{:S(2)}, u32[]{:S(2)}) %collective-permute-start.8) | collective-permute-done | bytes 622624 | tf_op jit(solution)/shard_map/ppermute | solution.py:82
  140.2 30.5 %collective-permute-done.14 = bf16[96,2048]{1,0:T(8,128)(2,1)S(1)} collective-permute-done((bf16[96,2048]{1,0:T(8,128)(2,1)S(1)}, bf16[96,2048]{1,0:T(8,128)(2,1)S(1)}, u32[]{:S(2)}, u32[]{:S(2)}) %collective-permute-start.14) | collective-permute-done | bytes 393248 | tf_op jit(solution)/shard_map/ppermute | solution.py:82
  178.2 10.3 %collective-permute-done.15 = bf16[328,1024]{1,0:T(8,128)(2,1)S(1)} collective-permute-done((bf16[328,1024]{1,0:T(8,128)(2,1)S(1)}, bf16[328,1024]{1,0:T(8,128)(2,1)S(1)}, u32[]{:S(2)}, u32[]{:S(2)}) %collective-permute-start.15) | collective-permute-done | bytes 671776 | tf_op jit(solution)/shard_map/ppermute | solution.py:82
  189.4 14.4 %collective-permute-done.22 = bf16[328,1024]{1,0:T(8,128)(2,1)S(1)} collective-permute-done((bf16[328,1024]{1,0:T(8,128)(2,1)S(1)}, bf16[328,1024]{1,0:T(8,128)(2,1)S(1)}, u32[]{:S(2)}, u32[]{:S(2)}) %collective-permute-start.22) | collective-permute-done | bytes 671776 | tf_op jit(solution)/shard_map/ppermute | solution.py:82
  209.5 12.3 %collective-permute-done.21 = bf16[328,1024]{1,0:T(8,128)(2,1)S(1)} collective-permute-done((bf16[328,1024]{1,0:T(8,128)(2,1)S(1)}, bf16[328,1024]{1,0:T(8,128)(2,1)S(1)}, u32[]{:S(2)}, u32[]{:S(2)}) %collective-permute-start.21) | collective-permute-done | bytes 671776 | tf_op jit(solution)/shard_map/ppermute | solution.py:82
  225.1 11.1 %collective-permute-done.43 = bf16[328,1024]{1,0:T(8,128)(2,1)S(1)} collective-permute-done((bf16[328,1024]{1,0:T(8,128)(2,1)S(1)}, bf16[328,1024]{1,0:T(8,128)(2,1)S(1)}, u32[]{:S(2)}, u32[]{:S(2)}) %collective-permute-start.43) | collective-permute-done | bytes 671776 | tf_op jit(solution)/shard_map/ppermute | solution.py:82
  239.0 11.6 %collective-permute-done.34 = bf16[328,1024]{1,0:T(8,128)(2,1)S(1)} collective-permute-done((bf16[328,1024]{1,0:T(8,128)(2,1)S(1)}, bf16[328,1024]{1,0:T(8,128)(2,1)S(1)}, u32[]{:S(2)}, u32[]{:S(2)}) %collective-permute-start.34) | collective-permute-done | bytes 671776 | tf_op jit(solution)/shard_map/ppermute | solution.py:82
  256.4 5.7 collective-permute-done.45
  264.7 9.0 %collective-permute-done.35 = bf16[264,1024]{1,0:T(8,128)(2,1)S(1)} collective-permute-done((bf16[264,1024]{1,0:T(8,128)(2,1)S(1)}, bf16[264,1024]{1,0:T(8,128)(2,1)S(1)}, u32[]{:S(2)}, u32[]{:S(2)}) %collective-permute-start.35) | collective-permute-done | bytes 540704 | tf_op jit(solution)/shard_map/ppermute | solution.py:82
  279.6 4.0 collective-permute-done.47
  286.1 7.2 %collective-permute-done.36 = bf16[224,1024]{1,0:T(8,128)(2,1)S(1)} collective-permute-done((bf16[224,1024]{1,0:T(8,128)(2,1)S(1)}, bf16[224,1024]{1,0:T(8,128)(2,1)S(1)}, u32[]{:S(2)}, u32[]{:S(2)}) %collective-permute-start.36) | collective-permute-done | bytes 458784 | tf_op jit(solution)/shard_map/ppermute | solution.py:82
  299.7 3.8 fusion.31
  303.6 3.8 fusion.35
  307.4 4.1 fusion.40
  340.7 4.2 collective-permute-done.30
  349.7 6.1 fusion.29
  355.8 6.2 fusion.33
  366.3 7.9 %fusion.37 = bf16[960,2048]{1,0:T(8,128)(2,1)S(1)} fusion(bf16[1,1024,2048]{2,1,0:T(8,128)(2,1)S(1)} %copy-done.10, f32[960,1024]{1,0:T(8,128)} %fusion.29, f32[960,1024]{1,0:T(8,128)} %fusion.33), kind=kOutput, calls=%fused_computation.51 | convolution fusion | flops 4034396160 | bytes 15990784 | tf_op jit(solution)/shard_map/dot_general | solution.py:26
  374.6 5.0 collective-permute-done.32
  385.1 15.2 %collective-permute-done.33 = bf16[200,2048]{1,0:T(8,128)(2,1)S(1)} collective-permute-done((bf16[200,2048]{1,0:T(8,128)(2,1)S(1)}, bf16[200,2048]{1,0:T(8,128)(2,1)S(1)}, u32[]{:S(2)}, u32[]{:S(2)}) %collective-permute-start.33) | collective-permute-done | bytes 819232 | tf_op jit(solution)/shard_map/ppermute | solution.py:82
  421.6 3.9 collective-permute-done.57
  437.5 9.9 %collective-permute-done.76 = bf16[224,1024]{1,0:T(8,128)(2,1)S(1)} collective-permute-done((bf16[224,1024]{1,0:T(8,128)(2,1)S(1)}, bf16[224,1024]{1,0:T(8,128)(2,1)S(1)}, u32[]{:S(2)}, u32[]{:S(2)}) %collective-permute-start.76) | collective-permute-done | bytes 458784 | tf_op jit(solution)/shard_map/ppermute | solution.py:82
  455.5 7.9 %collective-permute-done.77 = bf16[264,1024]{1,0:T(8,128)(2,1)S(1)} collective-permute-done((bf16[264,1024]{1,0:T(8,128)(2,1)S(1)}, bf16[264,1024]{1,0:T(8,128)(2,1)S(1)}, u32[]{:S(2)}, u32[]{:S(2)}) %collective-permute-start.77) | collective-permute-done | bytes 540704 | tf_op jit(solution)/shard_map/ppermute | solution.py:82
  463.8 3.8 collective-permute-start.78
  467.6 7.3 %collective-permute-done.59 = bf16[264,1024]{1,0:T(8,128)(2,1)S(1)} collective-permute-done((bf16[264,1024]{1,0:T(8,128)(2,1)S(1)}, bf16[264,1024]{1,0:T(8,128)(2,1)S(1)}, u32[]{:S(2)}, u32[]{:S(2)}) %collective-permute-start.59) | collective-permute-done | bytes 540704 | tf_op jit(solution)/shard_map/ppermute | solution.py:82
  475.4 3.8 collective-permute-start.60
  480.4 9.0 %collective-permute-done.78 = bf16[328,1024]{1,0:T(8,128)(2,1)S(1)} collective-permute-done((bf16[328,1024]{1,0:T(8,128)(2,1)S(1)}, bf16[328,1024]{1,0:T(8,128)(2,1)S(1)}, u32[]{:S(2)}, u32[]{:S(2)}) %collective-permute-start.78) | collective-permute-done | bytes 671776 | tf_op jit(solution)/shard_map/ppermute | solution.py:82
  489.8 3.8 collective-permute-start.79
  493.6 10.1 %collective-permute-done.60 = bf16[328,1024]{1,0:T(8,128)(2,1)S(1)} collective-permute-done((bf16[328,1024]{1,0:T(8,128)(2,1)S(1)}, bf16[328,1024]{1,0:T(8,128)(2,1)S(1)}, u32[]{:S(2)}, u32[]{:S(2)}) %collective-permute-start.60) | collective-permute-done | bytes 671776 | tf_op jit(solution)/shard_map/ppermute | solution.py:82
  504.2 3.8 collective-permute-start.61
  509.2 9.0 %collective-permute-done.79 = bf16[328,1024]{1,0:T(8,128)(2,1)S(1)} collective-permute-done((bf16[328,1024]{1,0:T(8,128)(2,1)S(1)}, bf16[328,1024]{1,0:T(8,128)(2,1)S(1)}, u32[]{:S(2)}, u32[]{:S(2)}) %collective-permute-start.79) | collective-permute-done | bytes 671776 | tf_op jit(solution)/shard_map/ppermute | solution.py:82
  518.6 3.8 collective-permute-start.80
  522.4 10.1 %collective-permute-done.61 = bf16[328,1024]{1,0:T(8,128)(2,1)S(1)} collective-permute-done((bf16[328,1024]{1,0:T(8,128)(2,1)S(1)}, bf16[328,1024]{1,0:T(8,128)(2,1)S(1)}, u32[]{:S(2)}, u32[]{:S(2)}) %collective-permute-start.61) | collective-permute-done | bytes 671776 | tf_op jit(solution)/shard_map/ppermute | solution.py:82
  538.0 9.0 %collective-permute-done.80 = bf16[328,1024]{1,0:T(8,128)(2,1)S(1)} collective-permute-done((bf16[328,1024]{1,0:T(8,128)(2,1)S(1)}, bf16[328,1024]{1,0:T(8,128)(2,1)S(1)}, u32[]{:S(2)}, u32[]{:S(2)}) %collective-permute-start.80) | collective-permute-done | bytes 671776 | tf_op jit(solution)/shard_map/ppermute | solution.py:82
  547.4 3.8 collective-permute-start.81
  551.2 10.1 %collective-permute-done.62 = bf16[328,1024]{1,0:T(8,128)(2,1)S(1)} collective-permute-done((bf16[328,1024]{1,0:T(8,128)(2,1)S(1)}, bf16[328,1024]{1,0:T(8,128)(2,1)S(1)}, u32[]{:S(2)}, u32[]{:S(2)}) %collective-permute-start.62) | collective-permute-done | bytes 671776 | tf_op jit(solution)/shard_map/ppermute | solution.py:82
  561.8 3.8 collective-permute-start.63
  566.9 8.8 %collective-permute-done.81 = bf16[328,1024]{1,0:T(8,128)(2,1)S(1)} collective-permute-done((bf16[328,1024]{1,0:T(8,128)(2,1)S(1)}, bf16[328,1024]{1,0:T(8,128)(2,1)S(1)}, u32[]{:S(2)}, u32[]{:S(2)}) %collective-permute-start.81) | collective-permute-done | bytes 671776 | tf_op jit(solution)/shard_map/ppermute | solution.py:82
  576.2 3.8 collective-permute-start.82
  580.0 10.1 %collective-permute-done.63 = bf16[328,1024]{1,0:T(8,128)(2,1)S(1)} collective-permute-done((bf16[328,1024]{1,0:T(8,128)(2,1)S(1)}, bf16[328,1024]{1,0:T(8,128)(2,1)S(1)}, u32[]{:S(2)}, u32[]{:S(2)}) %collective-permute-start.63) | collective-permute-done | bytes 671776 | tf_op jit(solution)/shard_map/ppermute | solution.py:82
  590.6 3.8 collective-permute-start.64
  595.5 9.0 %collective-permute-done.82 = bf16[328,1024]{1,0:T(8,128)(2,1)S(1)} collective-permute-done((bf16[328,1024]{1,0:T(8,128)(2,1)S(1)}, bf16[328,1024]{1,0:T(8,128)(2,1)S(1)}, u32[]{:S(2)}, u32[]{:S(2)}) %collective-permute-start.82) | collective-permute-done | bytes 671776 | tf_op jit(solution)/shard_map/ppermute | solution.py:82
  605.4 7.2 %collective-permute-done.64 = bf16[328,1024]{1,0:T(8,128)(2,1)S(1)} collective-permute-done((bf16[328,1024]{1,0:T(8,128)(2,1)S(1)}, bf16[328,1024]{1,0:T(8,128)(2,1)S(1)}, u32[]{:S(2)}, u32[]{:S(2)}) %collective-permute-start.64) | collective-permute-done | bytes 671776 | tf_op jit(solution)/shard_map/ppermute | solution.py:82
  (364 shorter events, 204.4 us)
Async XLA Ops:
  5.7 38.4 %all-to-all-start.2 = ((f32[32,1,96]{2,1,0:T(1,128)}), f32[32,1,96]{2,1,0:T(1,128)S(1)}, u32[]{:S(2)}, u32[]{:S(2)}) async-start(f32[32,1,96]{2,1,0:T(1,128)} %broadcast_in_dim.145), calls=%async_computation.2 | async-start | bytes 32768 | tf_op jit(solution)/shard_map/all_to_all | solution.py:121
  30.4 60.3 %collective-permute-start.2 = (bf16[200,2048]{1,0:T(8,128)(2,1)}, bf16[200,2048]{1,0:T(8,128)(2,1)}, u32[]{:S(2)}, u32[]{:S(2)}) collective-permute-start(bf16[200,2048]{1,0:T(8,128)(2,1)} %convolution_convert_fusion.9), channel_id=1, source_target_pairs={{0,2},{1,3},{2,4},{3,5},{4,6},{5,7},{6,8},{7,9},{8,10},{9,11},{10,... | collective-permute-start | bytes 2457608 | tf_op jit(solution)/shard_map/ppermute | solution.py:82
  33.2 60.3 %collective-permute-start.5 = (bf16[200,2048]{1,0:T(8,128)(2,1)}, bf16[200,2048]{1,0:T(8,128)(2,1)S(1)}, u32[]{:S(2)}, u32[]{:S(2)}) collective-permute-start(bf16[200,2048]{1,0:T(8,128)(2,1)} %convolution_convert_fusion.8), channel_id=1, source_target_pairs={{0,30},{1,31},{2,0},{3,1},{4,2},{5,3},{6,4},{7,5},{8,6},{9,7},{10,... | collective-permute-start | bytes 2457608 | tf_op jit(solution)/shard_map/ppermute | solution.py:82
  37.2 31.8 %collective-permute-start.4 = (bf16[328,1024]{1,0:T(8,128)(2,1)}, bf16[328,1024]{1,0:T(8,128)(2,1)}, u32[]{:S(2)}, u32[]{:S(2)}) collective-permute-start(bf16[328,1024]{1,0:T(8,128)(2,1)} %get-tuple-element.96), channel_id=1, source_target_pairs={{0,30},{1,31},{2,0},{3,1},{4,2},{5,3},{6,4},{7,5},{8,6},{9,7},{10,... | collective-permute-start | bytes 2015240 | tf_op jit(solution)/shard_map/ppermute | solution.py:82
  38.8 43.5 %collective-permute-start.3 = (bf16[328,1024]{1,0:T(8,128)(2,1)}, bf16[328,1024]{1,0:T(8,128)(2,1)}, u32[]{:S(2)}, u32[]{:S(2)}) collective-permute-start(bf16[328,1024]{1,0:T(8,128)(2,1)} %get-tuple-element.97), channel_id=1, source_target_pairs={{0,30},{1,31},{2,0},{3,1},{4,2},{5,3},{6,4},{7,5},{8,6},{9,7},{10,... | collective-permute-start | bytes 2015240 | tf_op jit(solution)/shard_map/ppermute | solution.py:82
  42.3 44.4 %collective-permute-start.1 = (bf16[328,1024]{1,0:T(8,128)(2,1)}, bf16[328,1024]{1,0:T(8,128)(2,1)}, u32[]{:S(2)}, u32[]{:S(2)}) collective-permute-start(bf16[328,1024]{1,0:T(8,128)(2,1)} %get-tuple-element.98), channel_id=1, source_target_pairs={{0,2},{1,3},{2,4},{3,5},{4,6},{5,7},{6,8},{7,9},{8,10},{9,11},{10,... | collective-permute-start | bytes 2015240 | tf_op jit(solution)/shard_map/ppermute | solution.py:82
  86.7 36.5 %collective-permute-start.9 = (bf16[328,1024]{1,0:T(8,128)(2,1)}, bf16[328,1024]{1,0:T(8,128)(2,1)S(1)}, u32[]{:S(2)}, u32[]{:S(2)}) collective-permute-start(bf16[328,1024]{1,0:T(8,128)(2,1)} %collective-permute-done.3), channel_id=1, source_target_pairs={{0,30},{1,31},{2,0},{3,1},{4,2},{5,3},{6,4},{7,5},{8,6},{9,7},{10,... | collective-permute-start | bytes 2015240 | tf_op jit(solution)/shard_map/ppermute | solution.py:82
  90.7 31.9 %collective-permute-start.6 = (bf16[328,1024]{1,0:T(8,128)(2,1)S(1)}, bf16[328,1024]{1,0:T(8,128)(2,1)S(1)}, u32[]{:S(2)}, u32[]{:S(2)}) collective-permute-start(bf16[328,1024]{1,0:T(8,128)(2,1)S(1)} %collective-permute-done), channel_id=1, source_target_pairs={{0,2},{1,3},{2,4},{3,5},{4,6},{5,7},{6,8},{7,9},{8,10},{9,11},{10,... | collective-permute-start | bytes 2015240 | tf_op jit(solution)/shard_map/ppermute | solution.py:82
  93.5 42.5 %collective-permute-start.8 = (bf16[152,2048]{1,0:T(8,128)(2,1)S(1)}, bf16[152,2048]{1,0:T(8,128)(2,1)S(1)}, u32[]{:S(2)}, u32[]{:S(2)}) collective-permute-start(bf16[152,2048]{1,0:T(8,128)(2,1)S(1)} %slice.833), channel_id=1, source_target_pairs={{0,2},{1,3},{2,4},{3,5},{4,6},{5,7},{6,8},{7,9},{8,10},{9,11},{10,... | collective-permute-start | bytes 1867784 | tf_op jit(solution)/shard_map/ppermute | solution.py:82
  101.0 35.3 %collective-permute-start.11 = (bf16[152,2048]{1,0:T(8,128)(2,1)S(1)}, bf16[152,2048]{1,0:T(8,128)(2,1)S(1)}, u32[]{:S(2)}, u32[]{:S(2)}) collective-permute-start(bf16[152,2048]{1,0:T(8,128)(2,1)S(1)} %slice.835), channel_id=1, source_target_pairs={{0,30},{1,31},{2,0},{3,1},{4,2},{5,3},{6,4},{7,5},{8,6},{9,7},{10,... | collective-permute-start | bytes 1867784 | tf_op jit(solution)/shard_map/ppermute | solution.py:82
  108.2 64.6 %collective-permute-start.16 = (bf16[328,1024]{1,0:T(8,128)(2,1)S(1)}, bf16[328,1024]{1,0:T(8,128)(2,1)S(1)}, u32[]{:S(2)}, u32[]{:S(2)}) collective-permute-start(bf16[328,1024]{1,0:T(8,128)(2,1)S(1)} %collective-permute-done.10), channel_id=1, source_target_pairs={{0,30},{1,31},{2,0},{3,1},{4,2},{5,3},{6,4},{7,5},{8,6},{9,7},{10,... | collective-permute-start | bytes 2015240 | tf_op jit(solution)/shard_map/ppermute | solution.py:82
  122.6 52.4 %collective-permute-start.13 = (bf16[328,1024]{1,0:T(8,128)(2,1)S(1)}, bf16[328,1024]{1,0:T(8,128)(2,1)S(1)}, u32[]{:S(2)}, u32[]{:S(2)}) collective-permute-start(bf16[328,1024]{1,0:T(8,128)(2,1)S(1)} %collective-permute-done.7), channel_id=1, source_target_pairs={{0,2},{1,3},{2,4},{3,5},{4,6},{5,7},{6,8},{7,9},{8,10},{9,11},{10,... | collective-permute-start | bytes 2015240 | tf_op jit(solution)/shard_map/ppermute | solution.py:82
  123.2 54.2 %collective-permute-start.12 = (bf16[328,1024]{1,0:T(8,128)(2,1)S(1)}, bf16[328,1024]{1,0:T(8,128)(2,1)S(1)}, u32[]{:S(2)}, u32[]{:S(2)}) collective-permute-start(bf16[328,1024]{1,0:T(8,128)(2,1)S(1)} %collective-permute-done.6), channel_id=1, source_target_pairs={{0,2},{1,3},{2,4},{3,5},{4,6},{5,7},{6,8},{7,9},{8,10},{9,11},{10,... | collective-permute-start | bytes 2015240 | tf_op jit(solution)/shard_map/ppermute | solution.py:82
  136.0 34.7 %collective-permute-start.14 = (bf16[96,2048]{1,0:T(8,128)(2,1)S(1)}, bf16[96,2048]{1,0:T(8,128)(2,1)S(1)}, u32[]{:S(2)}, u32[]{:S(2)}) collective-permute-start(bf16[96,2048]{1,0:T(8,128)(2,1)S(1)} %slice.837), channel_id=1, source_target_pairs={{0,2},{1,3},{2,4},{3,5},{4,6},{5,7},{6,8},{7,9},{8,10},{9,11},{10,... | collective-permute-start | bytes 1179656 | tf_op jit(solution)/shard_map/ppermute | solution.py:82
  136.4 34.5 %collective-permute-start.17 = (bf16[96,2048]{1,0:T(8,128)(2,1)S(1)}, bf16[96,2048]{1,0:T(8,128)(2,1)S(1)}, u32[]{:S(2)}, u32[]{:S(2)}) collective-permute-start(bf16[96,2048]{1,0:T(8,128)(2,1)S(1)} %slice.839), channel_id=1, source_target_pairs={{0,30},{1,31},{2,0},{3,1},{4,2},{5,3},{6,4},{7,5},{8,6},{9,7},{10,... | collective-permute-start | bytes 1179656 | tf_op jit(solution)/shard_map/ppermute | solution.py:82
  170.9 37.9 %collective-permute-start.20 = (bf16[40,2048]{1,0:T(8,128)(2,1)S(1)}, bf16[40,2048]{1,0:T(8,128)(2,1)S(1)}, u32[]{:S(2)}, u32[]{:S(2)}) collective-permute-start(bf16[40,2048]{1,0:T(8,128)(2,1)S(1)} %slice.841), channel_id=1, source_target_pairs={{0,2},{1,3},{2,4},{3,5},{4,6},{5,7},{6,8},{7,9},{8,10},{9,11},{10,... | collective-permute-start | bytes 491528 | tf_op jit(solution)/shard_map/ppermute | solution.py:82
  172.8 51.7 %collective-permute-start.23 = (bf16[40,2048]{1,0:T(8,128)(2,1)S(1)}, bf16[40,2048]{1,0:T(8,128)(2,1)S(1)}, u32[]{:S(2)}, u32[]{:S(2)}) collective-permute-start(bf16[40,2048]{1,0:T(8,128)(2,1)S(1)} %slice.843), channel_id=1, source_target_pairs={{0,30},{1,31},{2,0},{3,1},{4,2},{5,3},{6,4},{7,5},{8,6},{9,7},{10,... | collective-permute-start | bytes 491528 | tf_op jit(solution)/shard_map/ppermute | solution.py:82
  175.0 28.8 %collective-permute-start.22 = (bf16[328,1024]{1,0:T(8,128)(2,1)S(1)}, bf16[328,1024]{1,0:T(8,128)(2,1)S(1)}, u32[]{:S(2)}, u32[]{:S(2)}) collective-permute-start(bf16[328,1024]{1,0:T(8,128)(2,1)S(1)} %collective-permute-done.16), channel_id=1, source_target_pairs={{0,30},{1,31},{2,0},{3,1},{4,2},{5,3},{6,4},{7,5},{8,6},{9,7},{10,... | collective-permute-start | bytes 2015240 | tf_op jit(solution)/shard_map/ppermute | solution.py:82
  177.4 27.9 %collective-permute-start.19 = (bf16[328,1024]{1,0:T(8,128)(2,1)S(1)}, bf16[328,1024]{1,0:T(8,128)(2,1)S(1)}, u32[]{:S(2)}, u32[]{:S(2)}) collective-permute-start(bf16[328,1024]{1,0:T(8,128)(2,1)S(1)} %collective-permute-done.13), channel_id=1, source_target_pairs={{0,2},{1,3},{2,4},{3,5},{4,6},{5,7},{6,8},{7,9},{8,10},{9,11},{10,... | collective-permute-start | bytes 2015240 | tf_op jit(solution)/shard_map/ppermute | solution.py:82
  205.4 30.8 %collective-permute-start.43 = (bf16[328,1024]{1,0:T(8,128)(2,1)S(1)}, bf16[328,1024]{1,0:T(8,128)(2,1)S(1)}, u32[]{:S(2)}, u32[]{:S(2)}) collective-permute-start(bf16[328,1024]{1,0:T(8,128)(2,1)S(1)} %collective-permute-done.22), channel_id=1, source_target_pairs={{0,30},{1,31},{2,0},{3,1},{4,2},{5,3},{6,4},{7,5},{8,6},{9,7},{10,... | collective-permute-start | bytes 2015240 | tf_op jit(solution)/shard_map/ppermute | solution.py:82
  208.3 44.9 %collective-permute-start.42 = (bf16[328,1024]{1,0:T(8,128)(2,1)S(1)}, bf16[328,1024]{1,0:T(8,128)(2,1)S(1)}, u32[]{:S(2)}, u32[]{:S(2)}) collective-permute-start(bf16[328,1024]{1,0:T(8,128)(2,1)S(1)} %collective-permute-done.19), channel_id=1, source_target_pairs={{0,2},{1,3},{2,4},{3,5},{4,6},{5,7},{6,8},{7,9},{8,10},{9,11},{10,... | collective-permute-start | bytes 2015240 | tf_op jit(solution)/shard_map/ppermute | solution.py:82
  208.8 44.6 %collective-permute-start.26 = (bf16[328,1024]{1,0:T(8,128)(2,1)S(1)}, bf16[328,1024]{1,0:T(8,128)(2,1)S(1)}, u32[]{:S(2)}, u32[]{:S(2)}) collective-permute-start(bf16[328,1024]{1,0:T(8,128)(2,1)S(1)} %collective-permute-done.18), channel_id=1, source_target_pairs={{0,2},{1,3},{2,4},{3,5},{4,6},{5,7},{6,8},{7,9},{8,10},{9,11},{10,... | collective-permute-start | bytes 2015240 | tf_op jit(solution)/shard_map/ppermute | solution.py:82
  221.8 28.8 %collective-permute-start.34 = (bf16[328,1024]{1,0:T(8,128)(2,1)S(1)}, bf16[328,1024]{1,0:T(8,128)(2,1)S(1)}, u32[]{:S(2)}, u32[]{:S(2)}) collective-permute-start(bf16[328,1024]{1,0:T(8,128)(2,1)S(1)} %collective-permute-done.21), channel_id=1, source_target_pairs={{0,30},{1,31},{2,0},{3,1},{4,2},{5,3},{6,4},{7,5},{8,6},{9,7},{10,... | collective-permute-start | bytes 2015240 | tf_op jit(solution)/shard_map/ppermute | solution.py:82
  224.9 74.4 %collective-permute-start.24 = (bf16[432,2048]{1,0:T(8,128)(2,1)S(1)}, bf16[432,2048]{1,0:T(8,128)(2,1)S(1)}, u32[]{:S(2)}, u32[]{:S(2)}) collective-permute-start(bf16[432,2048]{1,0:T(8,128)(2,1)S(1)} %get-tuple-element.100), channel_id=1, source_target_pairs={{0,1},{1,0},{2,3},{3,2},{4,5},{5,4},{6,7},{7,6},{8,9},{9,8},{10,11... | collective-permute-start | bytes 5308424 | tf_op jit(solution)/shard_map/ppermute | solution.py:145
  236.2 25.9 %collective-permute-start.45 = (bf16[264,1024]{1,0:T(8,128)(2,1)S(1)}, bf16[264,1024]{1,0:T(8,128)(2,1)S(1)}, u32[]{:S(2)}, u32[]{:S(2)}) collective-permute-start(bf16[264,1024]{1,0:T(8,128)(2,1)S(1)} %slice.896), channel_id=1, source_target_pairs={{0,30},{1,31},{2,0},{3,1},{4,2},{5,3},{6,4},{7,5},{8,6},{9,7},{10,... | collective-permute-start | bytes 1622024 | tf_op jit(solution)/shard_map/ppermute | solution.py:82
  283.6 29.4 %collective-permute-start.49 = (bf16[144,1024]{1,0:T(8,128)(2,1)S(1)}, bf16[144,1024]{1,0:T(8,128)(2,1)S(1)}, u32[]{:S(2)}, u32[]{:S(2)}) collective-permute-start(bf16[144,1024]{1,0:T(8,128)(2,1)S(1)} %slice.908), channel_id=1, source_target_pairs={{0,30},{1,31},{2,0},{3,1},{4,2},{5,3},{6,4},{7,5},{8,6},{9,7},{10,... | collective-permute-start | bytes 884744 | tf_op jit(solution)/shard_map/ppermute | solution.py:82
  374.4 30.3 %collective-permute-start.55 = (bf16[480,2048]{1,0:T(8,128)(2,1)S(1)}, bf16[480,2048]{1,0:T(8,128)(2,1)S(1)}, u32[]{:S(2)}, u32[]{:S(2)}) collective-permute-start(bf16[480,2048]{1,0:T(8,128)(2,1)S(1)} %slice.920), channel_id=1, source_target_pairs={{0,1},{1,0},{2,3},{3,2},{4,5},{5,4},{6,7},{7,6},{8,9},{9,8},{10,11... | collective-permute-start | bytes 5898248 | tf_op jit(solution)/shard_map/ppermute | solution.py:146
  425.9 24.8 %collective-permute-start.58 = (bf16[224,1024]{1,0:T(8,128)(2,1)S(1)}, bf16[224,1024]{1,0:T(8,128)(2,1)S(1)}, u32[]{:S(2)}, u32[]{:S(2)}) collective-permute-start(bf16[224,1024]{1,0:T(8,128)(2,1)S(1)} %fusion.79), channel_id=1, source_target_pairs={{0,30},{1,31},{2,0},{3,1},{4,2},{5,3},{6,4},{7,5},{8,6},{9,7},{10,... | collective-permute-start | bytes 1376264 | tf_op jit(solution)/shard_map/ppermute | solution.py:82
  451.1 23.8 %collective-permute-start.59 = (bf16[264,1024]{1,0:T(8,128)(2,1)S(1)}, bf16[264,1024]{1,0:T(8,128)(2,1)S(1)}, u32[]{:S(2)}, u32[]{:S(2)}) collective-permute-start(bf16[264,1024]{1,0:T(8,128)(2,1)S(1)} %fusion.75), channel_id=1, source_target_pairs={{0,30},{1,31},{2,0},{3,1},{4,2},{5,3},{6,4},{7,5},{8,6},{9,7},{10,... | collective-permute-start | bytes 1622024 | tf_op jit(solution)/shard_map/ppermute | solution.py:82
  454.3 24.9 %collective-permute-start.86 = (bf16[264,1024]{1,0:T(8,128)(2,1)S(1)}, bf16[264,1024]{1,0:T(8,128)(2,1)S(1)}, u32[]{:S(2)}, u32[]{:S(2)}) collective-permute-start(bf16[264,1024]{1,0:T(8,128)(2,1)S(1)} %fusion.78), channel_id=1, source_target_pairs={{0,2},{1,3},{2,4},{3,5},{4,6},{5,7},{6,8},{7,9},{8,10},{9,11},{10,... | collective-permute-start | bytes 1622024 | tf_op jit(solution)/shard_map/ppermute | solution.py:82
  455.4 24.4 %collective-permute-start.68 = (bf16[264,1024]{1,0:T(8,128)(2,1)S(1)}, bf16[264,1024]{1,0:T(8,128)(2,1)S(1)}, u32[]{:S(2)}, u32[]{:S(2)}) collective-permute-start(bf16[264,1024]{1,0:T(8,128)(2,1)S(1)} %fusion.76), channel_id=1, source_target_pairs={{0,2},{1,3},{2,4},{3,5},{4,6},{5,7},{6,8},{7,9},{8,10},{9,11},{10,... | collective-permute-start | bytes 1622024 | tf_op jit(solution)/shard_map/ppermute | solution.py:82
  463.8 25.5 %collective-permute-start.78 = (bf16[328,1024]{1,0:T(8,128)(2,1)S(1)}, bf16[328,1024]{1,0:T(8,128)(2,1)S(1)}, u32[]{:S(2)}, u32[]{:S(2)}) collective-permute-start(bf16[328,1024]{1,0:T(8,128)(2,1)S(1)} %fusion.69), channel_id=1, source_target_pairs={{0,30},{1,31},{2,0},{3,1},{4,2},{5,3},{6,4},{7,5},{8,6},{9,7},{10,... | collective-permute-start | bytes 2015240 | tf_op jit(solution)/shard_map/ppermute | solution.py:82
  475.4 28.3 %collective-permute-start.60 = (bf16[328,1024]{1,0:T(8,128)(2,1)S(1)}, bf16[328,1024]{1,0:T(8,128)(2,1)S(1)}, u32[]{:S(2)}, u32[]{:S(2)}) collective-permute-start(bf16[328,1024]{1,0:T(8,128)(2,1)S(1)} %fusion.59), channel_id=1, source_target_pairs={{0,30},{1,31},{2,0},{3,1},{4,2},{5,3},{6,4},{7,5},{8,6},{9,7},{10,... | collective-permute-start | bytes 2015240 | tf_op jit(solution)/shard_map/ppermute | solution.py:82
  479.6 28.3 %collective-permute-start.87 = (bf16[328,1024]{1,0:T(8,128)(2,1)S(1)}, bf16[328,1024]{1,0:T(8,128)(2,1)S(1)}, u32[]{:S(2)}, u32[]{:S(2)}) collective-permute-start(bf16[328,1024]{1,0:T(8,128)(2,1)S(1)} %fusion.74), channel_id=1, source_target_pairs={{0,2},{1,3},{2,4},{3,5},{4,6},{5,7},{6,8},{7,9},{8,10},{9,11},{10,... | collective-permute-start | bytes 2015240 | tf_op jit(solution)/shard_map/ppermute | solution.py:82
  480.2 28.3 %collective-permute-start.69 = (bf16[328,1024]{1,0:T(8,128)(2,1)S(1)}, bf16[328,1024]{1,0:T(8,128)(2,1)S(1)}, u32[]{:S(2)}, u32[]{:S(2)}) collective-permute-start(bf16[328,1024]{1,0:T(8,128)(2,1)S(1)} %fusion.64), channel_id=1, source_target_pairs={{0,2},{1,3},{2,4},{3,5},{4,6},{5,7},{6,8},{7,9},{8,10},{9,11},{10,... | collective-permute-start | bytes 2015240 | tf_op jit(solution)/shard_map/ppermute | solution.py:82
  489.8 28.3 %collective-permute-start.79 = (bf16[328,1024]{1,0:T(8,128)(2,1)S(1)}, bf16[328,1024]{1,0:T(8,128)(2,1)S(1)}, u32[]{:S(2)}, u32[]{:S(2)}) collective-permute-start(bf16[328,1024]{1,0:T(8,128)(2,1)S(1)} %fusion.68), channel_id=1, source_target_pairs={{0,30},{1,31},{2,0},{3,1},{4,2},{5,3},{6,4},{7,5},{8,6},{9,7},{10,... | collective-permute-start | bytes 2015240 | tf_op jit(solution)/shard_map/ppermute | solution.py:82
  504.2 28.3 %collective-permute-start.61 = (bf16[328,1024]{1,0:T(8,128)(2,1)S(1)}, bf16[328,1024]{1,0:T(8,128)(2,1)S(1)}, u32[]{:S(2)}, u32[]{:S(2)}) collective-permute-start(bf16[328,1024]{1,0:T(8,128)(2,1)S(1)} %fusion.58), channel_id=1, source_target_pairs={{0,30},{1,31},{2,0},{3,1},{4,2},{5,3},{6,4},{7,5},{8,6},{9,7},{10,... | collective-permute-start | bytes 2015240 | tf_op jit(solution)/shard_map/ppermute | solution.py:82
  508.4 28.3 %collective-permute-start.88 = (bf16[328,1024]{1,0:T(8,128)(2,1)S(1)}, bf16[328,1024]{1,0:T(8,128)(2,1)S(1)}, u32[]{:S(2)}, u32[]{:S(2)}) collective-permute-start(bf16[328,1024]{1,0:T(8,128)(2,1)S(1)} %fusion.73), channel_id=1, source_target_pairs={{0,2},{1,3},{2,4},{3,5},{4,6},{5,7},{6,8},{7,9},{8,10},{9,11},{10,... | collective-permute-start | bytes 2015240 | tf_op jit(solution)/shard_map/ppermute | solution.py:82
  509.0 28.3 %collective-permute-start.70 = (bf16[328,1024]{1,0:T(8,128)(2,1)S(1)}, bf16[328,1024]{1,0:T(8,128)(2,1)S(1)}, u32[]{:S(2)}, u32[]{:S(2)}) collective-permute-start(bf16[328,1024]{1,0:T(8,128)(2,1)S(1)} %fusion.63), channel_id=1, source_target_pairs={{0,2},{1,3},{2,4},{3,5},{4,6},{5,7},{6,8},{7,9},{8,10},{9,11},{10,... | collective-permute-start | bytes 2015240 | tf_op jit(solution)/shard_map/ppermute | solution.py:82
  518.6 28.3 %collective-permute-start.80 = (bf16[328,1024]{1,0:T(8,128)(2,1)S(1)}, bf16[328,1024]{1,0:T(8,128)(2,1)S(1)}, u32[]{:S(2)}, u32[]{:S(2)}) collective-permute-start(bf16[328,1024]{1,0:T(8,128)(2,1)S(1)} %fusion.67), channel_id=1, source_target_pairs={{0,30},{1,31},{2,0},{3,1},{4,2},{5,3},{6,4},{7,5},{8,6},{9,7},{10,... | collective-permute-start | bytes 2015240 | tf_op jit(solution)/shard_map/ppermute | solution.py:82
  533.0 28.3 %collective-permute-start.62 = (bf16[328,1024]{1,0:T(8,128)(2,1)S(1)}, bf16[328,1024]{1,0:T(8,128)(2,1)S(1)}, u32[]{:S(2)}, u32[]{:S(2)}) collective-permute-start(bf16[328,1024]{1,0:T(8,128)(2,1)S(1)} %fusion.57), channel_id=1, source_target_pairs={{0,30},{1,31},{2,0},{3,1},{4,2},{5,3},{6,4},{7,5},{8,6},{9,7},{10,... | collective-permute-start | bytes 2015240 | tf_op jit(solution)/shard_map/ppermute | solution.py:82
  537.2 28.3 %collective-permute-start.89 = (bf16[328,1024]{1,0:T(8,128)(2,1)S(1)}, bf16[328,1024]{1,0:T(8,128)(2,1)S(1)}, u32[]{:S(2)}, u32[]{:S(2)}) collective-permute-start(bf16[328,1024]{1,0:T(8,128)(2,1)S(1)} %fusion.72), channel_id=1, source_target_pairs={{0,2},{1,3},{2,4},{3,5},{4,6},{5,7},{6,8},{7,9},{8,10},{9,11},{10,... | collective-permute-start | bytes 2015240 | tf_op jit(solution)/shard_map/ppermute | solution.py:82
  537.8 28.3 %collective-permute-start.71 = (bf16[328,1024]{1,0:T(8,128)(2,1)S(1)}, bf16[328,1024]{1,0:T(8,128)(2,1)S(1)}, u32[]{:S(2)}, u32[]{:S(2)}) collective-permute-start(bf16[328,1024]{1,0:T(8,128)(2,1)S(1)} %fusion.62), channel_id=1, source_target_pairs={{0,2},{1,3},{2,4},{3,5},{4,6},{5,7},{6,8},{7,9},{8,10},{9,11},{10,... | collective-permute-start | bytes 2015240 | tf_op jit(solution)/shard_map/ppermute | solution.py:82
  547.4 28.3 %collective-permute-start.81 = (bf16[328,1024]{1,0:T(8,128)(2,1)S(1)}, bf16[328,1024]{1,0:T(8,128)(2,1)S(1)}, u32[]{:S(2)}, u32[]{:S(2)}) collective-permute-start(bf16[328,1024]{1,0:T(8,128)(2,1)S(1)} %fusion.66), channel_id=1, source_target_pairs={{0,30},{1,31},{2,0},{3,1},{4,2},{5,3},{6,4},{7,5},{8,6},{9,7},{10,... | collective-permute-start | bytes 2015240 | tf_op jit(solution)/shard_map/ppermute | solution.py:82
  561.8 28.3 %collective-permute-start.63 = (bf16[328,1024]{1,0:T(8,128)(2,1)S(1)}, bf16[328,1024]{1,0:T(8,128)(2,1)S(1)}, u32[]{:S(2)}, u32[]{:S(2)}) collective-permute-start(bf16[328,1024]{1,0:T(8,128)(2,1)S(1)} %fusion.56), channel_id=1, source_target_pairs={{0,30},{1,31},{2,0},{3,1},{4,2},{5,3},{6,4},{7,5},{8,6},{9,7},{10,... | collective-permute-start | bytes 2015240 | tf_op jit(solution)/shard_map/ppermute | solution.py:82
  566.0 28.3 %collective-permute-start.90 = (bf16[328,1024]{1,0:T(8,128)(2,1)S(1)}, bf16[328,1024]{1,0:T(8,128)(2,1)S(1)}, u32[]{:S(2)}, u32[]{:S(2)}) collective-permute-start(bf16[328,1024]{1,0:T(8,128)(2,1)S(1)} %fusion.71), channel_id=1, source_target_pairs={{0,2},{1,3},{2,4},{3,5},{4,6},{5,7},{6,8},{7,9},{8,10},{9,11},{10,... | collective-permute-start | bytes 2015240 | tf_op jit(solution)/shard_map/ppermute | solution.py:82
  566.6 28.3 %collective-permute-start.72 = (bf16[328,1024]{1,0:T(8,128)(2,1)S(1)}, bf16[328,1024]{1,0:T(8,128)(2,1)S(1)}, u32[]{:S(2)}, u32[]{:S(2)}) collective-permute-start(bf16[328,1024]{1,0:T(8,128)(2,1)S(1)} %fusion.61), channel_id=1, source_target_pairs={{0,2},{1,3},{2,4},{3,5},{4,6},{5,7},{6,8},{7,9},{8,10},{9,11},{10,... | collective-permute-start | bytes 2015240 | tf_op jit(solution)/shard_map/ppermute | solution.py:82
  576.2 28.3 %collective-permute-start.82 = (bf16[328,1024]{1,0:T(8,128)(2,1)S(1)}, bf16[328,1024]{1,0:T(8,128)(2,1)S(1)}, u32[]{:S(2)}, u32[]{:S(2)}) collective-permute-start(bf16[328,1024]{1,0:T(8,128)(2,1)S(1)} %fusion.65), channel_id=1, source_target_pairs={{0,30},{1,31},{2,0},{3,1},{4,2},{5,3},{6,4},{7,5},{8,6},{9,7},{10,... | collective-permute-start | bytes 2015240 | tf_op jit(solution)/shard_map/ppermute | solution.py:82
  (59 other events, 836.7 us)

commit v3 on v2

--- a/solution.py
+++ b/solution.py
@@ -11,7 +11,7 @@
 HOPS = (528, 480, 424, 368, 328, 264, 224, 144, 80)
 NEAR = 4
 PARTS = 2
-HOLD = 8
+HOLD = 7
 BATCHES = ((1, 2, 3, 4), (5, 6, 7, 8, 9))
 WAYS = (1, -1)
 
@@ -46,7 +46,8 @@
 
 
 def expert_rows(rows, w_gate, w_up, w_down):
-    gate_pre, up_pre = dot(rows, w_gate[0]), dot(rows, w_up[0])
+    gate_pre = dot(rows, w_gate[0])
+    up_pre = dot(rows, w_up[0])
     hidden = (jax.nn.silu(gate_pre) * up_pre).astype(BF16)
     return dot(hidden, w_down[0]).astype(BF16)
 
@@ -116,11 +117,20 @@
             far_block[way, part] = block[:, columns[part]]
     here = first(0, 0, 2 * capacity)
 
+    far_at, near_at = {}, {}
+    for k in range(1, far + 1):
+        for way in WAYS:
+            if k <= NEAR:
+                near_block[way] = near_at[way, k] = hop(near_block[way][: HOPS[k - 1] - fixed], way)
+        for part in range(PARTS):
+            for way in WAYS:
+                block = hop(far_block[way, part][: min(fixed, HOPS[k - 1])], way)
+                far_block[way, part] = far_at[way, k, part] = block
+
     sent = [jnp.maximum(jnp.minimum(after, cut) - before, 0), jnp.maximum(after - jnp.maximum(before, cut), 0)]
     row = jnp.concatenate(sent + [jnp.full((experts,), spilt, I32)]).astype(F32)
-    table = lax.all_to_all(
-        jnp.broadcast_to(row, (experts, row.shape[0])), "ep", split_axis=0, concat_axis=0, tiled=True
-    )
+    row, _ = lax.optimization_barrier((jnp.broadcast_to(row, (experts, row.shape[0])), near_at[1, 1]))
+    table = lax.all_to_all(row, "ep", split_axis=0, concat_axis=0, tiled=True)
     spilt = jnp.max(table[:, 2 * experts]) > 0
     hops = jnp.arange(1, far + 1, dtype=I32)
     slot = jnp.arange(capacity, dtype=F32)
@@ -142,23 +152,14 @@
         own = jnp.concatenate([g[:capacity] for g in got])
         other = jnp.concatenate([g[capacity:] for g in got])
         n = own.shape[0]
-        done = expert_rows(jnp.concatenate([own, lax.ppermute(other, "ep", swap)]), w_gate, w_up, w_down)
+        other = lax.ppermute(other, "ep", swap)
+        done = expert_rows(jnp.concatenate([own, other]), w_gate, w_up, w_down)
         back = lax.ppermute(done[n:], "ep", swap)
         span = lambda i: slice(i * capacity, (i + 1) * capacity)
         return [jnp.concatenate([done[span(i)], back[span(i)]]) for i in range(len(got))]
 
     def pick(way, k, low, high):
         return (wants[way][k - 1][:, None] == jnp.arange(low, high, dtype=F32)[None, :]).astype(BF16)
-
-    far_at, near_at = {}, {}
-    for k in range(1, far + 1):
-        for way in WAYS:
-            if k <= NEAR:
-                near_block[way] = near_at[way, k] = hop(near_block[way][: HOPS[k - 1] - fixed], way)
-        for part in range(PARTS):
-            for way in WAYS:
-                block = hop(far_block[way, part][: min(fixed, HOPS[k - 1])], way)
-                far_block[way, part] = far_at[way, k, part] = block
 
     def select(way, k):
         rows = min(fixed, HOPS[k - 1])

time: 629 us -> 616 us (0.979)
  starting transfers between devices: 155 us -> 137 us
  waiting for transfers between devices: 348 us -> 338 us
  matrix products: 79.9 us -> 87.7 us
    ppermute x88, waiting for transfers between devices: 348 us -> 338 us  [body(): hop = lambda block, way: lax.ppermute(block, 'ep', step[way])]
    ppermute x88, starting transfers between devices: 137 us -> 128 us  [body(): hop = lambda block, way: lax.ppermute(block, 'ep', step[way])]
    all_to_all x1, starting transfers between devices: 17.8 us -> 9.08 us  [body(): table = lax.all_to_all(row, 'ep', split_axis=0, concat_axis=0, tiled=True)]
    dot_general x107, matrix products: 79.3 us -> 85.6 us  [dot(): return jnp.dot(a, b, preferred_element_type=F32)]
  transfers between devices with their start and end apart: 93 -> 93, of which waited for: 40 -> 41; matrix products, arithmetic and copies ran while one was open for 17% -> 18% of each run, Pallas kernels for 0% -> 0%
where the time goes in v3:
time: 616 us; the launch traced here: 607 us
  waiting for transfers between devices  338 us (55%)
  starting transfers between devices  137 us (22%)
  matrix products  87.7 us (14%)
  other arithmetic  20 us (3%)
  local copies, waits for them, and re-layouts  18.4 us (3%)
    ppermute x88, waiting for transfers between devices, body(): hop = lambda block, way: lax.ppermute(block, 'ep', step[way])  338 us
    ppermute x88, starting transfers between devices, body(): hop = lambda block, way: lax.ppermute(block, 'ep', step[way])  128 us
    dot_general x107, matrix products, dot(): return jnp.dot(a, b, preferred_element_type=F32)  85.6 us
  transfers between devices with their start and end apart: 93, of which 41 were waited for; matrix products, arithmetic and copies ran while one was open for 18% of the time, Pallas kernels for 0%

profile of v3, /device:TPU:70, one launch (start us, length us, event | category | flops | bytes accessed | tf_op | source)
XLA Modules:
  0.0 607.1 jit_solution(10460620374432446549)
XLA Ops:
  14.1 10.4 %collective-permute-start.5 = (bf16[200,2048]{1,0:T(8,128)(2,1)}, bf16[200,2048]{1,0:T(8,128)(2,1)S(1)}, u32[]{:S(2)}, u32[]{:S(2)}) collective-permute-start(bf16[200,2048]{1,0:T(8,128)(2,1)} %convolution_convert_fusion.8), channel_id=1, source_target_pairs={{0,30},{1,31},{2,0},{3,1},{4,2},{5,3},{6,4},{7,5},{8,6},{9,7},{10,... | collective-permute-start | bytes 2457608 | tf_op jit(solution)/shard_map/ppermute | solution.py:83
  37.0 5.4 collective-permute-done
  44.3 9.1 %all-to-all-start.2 = ((f32[32,1,96]{2,1,0:T(1,128)}), f32[32,1,96]{2,1,0:T(1,128)}, u32[]{:S(2)}, u32[]{:S(2)}) async-start(f32[32,1,96]{2,1,0:T(1,128)} %bitcast.13), calls=%async_computation.2 | async-start | bytes 32768 | tf_op jit(solution)/shard_map/all_to_all | solution.py:133
  53.9 3.9 collective-permute-done.4
  57.9 3.7 collective-permute-start.10
  61.6 11.1 %collective-permute-done.3 = bf16[328,1024]{1,0:T(8,128)(2,1)} collective-permute-done((bf16[328,1024]{1,0:T(8,128)(2,1)}, bf16[328,1024]{1,0:T(8,128)(2,1)}, u32[]{:S(2)}, u32[]{:S(2)}) %collective-permute-start.3) | collective-permute-done | bytes 671776 | tf_op jit(solution)/shard_map/ppermute | solution.py:83
  72.6 3.8 collective-permute-start.9
  90.1 3.3 collective-permute-start.11
  98.4 12.0 %collective-permute-done.6 = bf16[328,1024]{1,0:T(8,128)(2,1)} collective-permute-done((bf16[328,1024]{1,0:T(8,128)(2,1)}, bf16[328,1024]{1,0:T(8,128)(2,1)}, u32[]{:S(2)}, u32[]{:S(2)}) %collective-permute-start.6) | collective-permute-done | bytes 671776 | tf_op jit(solution)/shard_map/ppermute | solution.py:83
  113.3 10.3 %collective-permute-done.8 = bf16[152,2048]{1,0:T(8,128)(2,1)S(1)} collective-permute-done((bf16[152,2048]{1,0:T(8,128)(2,1)}, bf16[152,2048]{1,0:T(8,128)(2,1)S(1)}, u32[]{:S(2)}, u32[]{:S(2)}) %collective-permute-start.8) | collective-permute-done | bytes 622624 | tf_op jit(solution)/shard_map/ppermute | solution.py:83
  123.8 3.3 collective-permute-start.17
  127.8 29.6 %collective-permute-done.14 = bf16[96,2048]{1,0:T(8,128)(2,1)S(1)} collective-permute-done((bf16[96,2048]{1,0:T(8,128)(2,1)S(1)}, bf16[96,2048]{1,0:T(8,128)(2,1)S(1)}, u32[]{:S(2)}, u32[]{:S(2)}) %collective-permute-start.14) | collective-permute-done | bytes 393248 | tf_op jit(solution)/shard_map/ppermute | solution.py:83
  164.6 11.1 %collective-permute-done.15 = bf16[328,1024]{1,0:T(8,128)(2,1)S(1)} collective-permute-done((bf16[328,1024]{1,0:T(8,128)(2,1)}, bf16[328,1024]{1,0:T(8,128)(2,1)S(1)}, u32[]{:S(2)}, u32[]{:S(2)}) %collective-permute-start.15) | collective-permute-done | bytes 671776 | tf_op jit(solution)/shard_map/ppermute | solution.py:83
  176.3 14.5 %collective-permute-done.22 = bf16[328,1024]{1,0:T(8,128)(2,1)S(1)} collective-permute-done((bf16[328,1024]{1,0:T(8,128)(2,1)S(1)}, bf16[328,1024]{1,0:T(8,128)(2,1)S(1)}, u32[]{:S(2)}, u32[]{:S(2)}) %collective-permute-start.22) | collective-permute-done | bytes 671776 | tf_op jit(solution)/shard_map/ppermute | solution.py:83
  196.8 12.0 %collective-permute-done.21 = bf16[328,1024]{1,0:T(8,128)(2,1)S(1)} collective-permute-done((bf16[328,1024]{1,0:T(8,128)(2,1)S(1)}, bf16[328,1024]{1,0:T(8,128)(2,1)S(1)}, u32[]{:S(2)}, u32[]{:S(2)}) %collective-permute-start.21) | collective-permute-done | bytes 671776 | tf_op jit(solution)/shard_map/ppermute | solution.py:83
  210.9 12.3 %collective-permute-done.41 = bf16[328,1024]{1,0:T(8,128)(2,1)S(1)} collective-permute-done((bf16[328,1024]{1,0:T(8,128)(2,1)S(1)}, bf16[328,1024]{1,0:T(8,128)(2,1)S(1)}, u32[]{:S(2)}, u32[]{:S(2)}) %collective-permute-start.41) | collective-permute-done | bytes 671776 | tf_op jit(solution)/shard_map/ppermute | solution.py:83
  224.6 13.0 %collective-permute-done.33 = bf16[328,1024]{1,0:T(8,128)(2,1)S(1)} collective-permute-done((bf16[328,1024]{1,0:T(8,128)(2,1)S(1)}, bf16[328,1024]{1,0:T(8,128)(2,1)S(1)}, u32[]{:S(2)}, u32[]{:S(2)}) %collective-permute-start.33) | collective-permute-done | bytes 671776 | tf_op jit(solution)/shard_map/ppermute | solution.py:83
  242.8 6.4 %collective-permute-done.43 = bf16[264,1024]{1,0:T(8,128)(2,1)S(1)} collective-permute-done((bf16[264,1024]{1,0:T(8,128)(2,1)S(1)}, bf16[264,1024]{1,0:T(8,128)(2,1)S(1)}, u32[]{:S(2)}, u32[]{:S(2)}) %collective-permute-start.43) | collective-permute-done | bytes 540704 | tf_op jit(solution)/shard_map/ppermute | solution.py:83
  250.5 10.2 %collective-permute-done.34 = bf16[264,1024]{1,0:T(8,128)(2,1)S(1)} collective-permute-done((bf16[264,1024]{1,0:T(8,128)(2,1)S(1)}, bf16[264,1024]{1,0:T(8,128)(2,1)S(1)}, u32[]{:S(2)}, u32[]{:S(2)}) %collective-permute-start.34) | collective-permute-done | bytes 540704 | tf_op jit(solution)/shard_map/ppermute | solution.py:83
  266.0 4.6 collective-permute-done.45
  271.9 8.5 %collective-permute-done.35 = bf16[224,1024]{1,0:T(8,128)(2,1)S(1)} collective-permute-done((bf16[224,1024]{1,0:T(8,128)(2,1)S(1)}, bf16[224,1024]{1,0:T(8,128)(2,1)S(1)}, u32[]{:S(2)}, u32[]{:S(2)}) %collective-permute-start.35) | collective-permute-done | bytes 458784 | tf_op jit(solution)/shard_map/ppermute | solution.py:83
  286.1 3.8 fusion.31
  290.0 3.8 fusion.35
  293.8 4.1 fusion.40
  299.5 3.3 collective-permute-start.53
  327.3 4.2 collective-permute-done.29
  336.2 6.2 %fusion.29 = f32[960,1024]{1,0:T(8,128)} fusion(bf16[960,2048]{1,0:T(8,128)(2,1)S(1)} %constant_dynamic-update-slice_fusion.1, bf16[1,2048,1024]{2,1,0:T(8,128)(2,1)S(1)} %copy-done.73), kind=kOutput, calls=%fused_computation.41 | convolution fusion | flops 4026531840 | bytes 12058624 | tf_op jit(solution)/shard_map/dot_general | solution.py:26
  342.3 6.2 %fusion.33 = f32[960,1024]{1,0:T(8,128)} fusion(bf16[960,2048]{1,0:T(8,128)(2,1)S(1)} %constant_dynamic-update-slice_fusion.1, bf16[1,2048,1024]{2,1,0:T(8,128)(2,1)S(1)} %copy-done.75), kind=kOutput, calls=%fused_computation.45 | convolution fusion | flops 4026531840 | bytes 12058624 | tf_op jit(solution)/shard_map/dot_general | solution.py:26
  352.9 7.9 %fusion.37 = bf16[960,2048]{1,0:T(8,128)(2,1)S(1)} fusion(bf16[1,1024,2048]{2,1,0:T(8,128)(2,1)S(1)} %copy-done.70, f32[960,1024]{1,0:T(8,128)} %fusion.29, f32[960,1024]{1,0:T(8,128)} %fusion.33), kind=kOutput, calls=%fused_computation.51 | convolution fusion | flops 4034396160 | bytes 15990784 | tf_op jit(solution)/shard_map/dot_general | solution.py:26
  361.2 4.1 collective-permute-done.31
  365.7 4.2 collective-permute-start.32
  371.7 13.9 %collective-permute-done.32 = bf16[200,2048]{1,0:T(8,128)(2,1)S(1)} collective-permute-done((bf16[200,2048]{1,0:T(8,128)(2,1)S(1)}, bf16[200,2048]{1,0:T(8,128)(2,1)S(1)}, u32[]{:S(2)}, u32[]{:S(2)}) %collective-permute-start.32) | collective-permute-done | bytes 819232 | tf_op jit(solution)/shard_map/ppermute | solution.py:83
  386.5 4.0 collective-permute-done.39
  407.1 5.8 collective-permute-done.57
  415.6 3.6 collective-permute-done.75
  424.8 9.9 %collective-permute-done.76 = bf16[224,1024]{1,0:T(8,128)(2,1)S(1)} collective-permute-done((bf16[224,1024]{1,0:T(8,128)(2,1)S(1)}, bf16[224,1024]{1,0:T(8,128)(2,1)S(1)}, u32[]{:S(2)}, u32[]{:S(2)}) %collective-permute-start.76) | collective-permute-done | bytes 458784 | tf_op jit(solution)/shard_map/ppermute | solution.py:83
  442.0 9.3 %collective-permute-done.77 = bf16[264,1024]{1,0:T(8,128)(2,1)S(1)} collective-permute-done((bf16[264,1024]{1,0:T(8,128)(2,1)S(1)}, bf16[264,1024]{1,0:T(8,128)(2,1)S(1)}, u32[]{:S(2)}, u32[]{:S(2)}) %collective-permute-start.77) | collective-permute-done | bytes 540704 | tf_op jit(solution)/shard_map/ppermute | solution.py:83
  454.1 8.8 %collective-permute-done.59 = bf16[264,1024]{1,0:T(8,128)(2,1)S(1)} collective-permute-done((bf16[264,1024]{1,0:T(8,128)(2,1)S(1)}, bf16[264,1024]{1,0:T(8,128)(2,1)S(1)}, u32[]{:S(2)}, u32[]{:S(2)}) %collective-permute-start.59) | collective-permute-done | bytes 540704 | tf_op jit(solution)/shard_map/ppermute | solution.py:83
  468.6 8.7 %collective-permute-done.78 = bf16[328,1024]{1,0:T(8,128)(2,1)S(1)} collective-permute-done((bf16[328,1024]{1,0:T(8,128)(2,1)S(1)}, bf16[328,1024]{1,0:T(8,128)(2,1)S(1)}, u32[]{:S(2)}, u32[]{:S(2)}) %collective-permute-start.78) | collective-permute-done | bytes 671776 | tf_op jit(solution)/shard_map/ppermute | solution.py:83
  480.1 11.7 %collective-permute-done.60 = bf16[328,1024]{1,0:T(8,128)(2,1)S(1)} collective-permute-done((bf16[328,1024]{1,0:T(8,128)(2,1)S(1)}, bf16[328,1024]{1,0:T(8,128)(2,1)S(1)}, u32[]{:S(2)}, u32[]{:S(2)}) %collective-permute-start.60) | collective-permute-done | bytes 671776 | tf_op jit(solution)/shard_map/ppermute | solution.py:83
  497.4 8.7 %collective-permute-done.79 = bf16[328,1024]{1,0:T(8,128)(2,1)S(1)} collective-permute-done((bf16[328,1024]{1,0:T(8,128)(2,1)S(1)}, bf16[328,1024]{1,0:T(8,128)(2,1)S(1)}, u32[]{:S(2)}, u32[]{:S(2)}) %collective-permute-start.79) | collective-permute-done | bytes 671776 | tf_op jit(solution)/shard_map/ppermute | solution.py:83
  508.9 11.7 %collective-permute-done.61 = bf16[328,1024]{1,0:T(8,128)(2,1)S(1)} collective-permute-done((bf16[328,1024]{1,0:T(8,128)(2,1)S(1)}, bf16[328,1024]{1,0:T(8,128)(2,1)S(1)}, u32[]{:S(2)}, u32[]{:S(2)}) %collective-permute-start.61) | collective-permute-done | bytes 671776 | tf_op jit(solution)/shard_map/ppermute | solution.py:83
  526.2 8.7 %collective-permute-done.80 = bf16[328,1024]{1,0:T(8,128)(2,1)S(1)} collective-permute-done((bf16[328,1024]{1,0:T(8,128)(2,1)S(1)}, bf16[328,1024]{1,0:T(8,128)(2,1)S(1)}, u32[]{:S(2)}, u32[]{:S(2)}) %collective-permute-start.80) | collective-permute-done | bytes 671776 | tf_op jit(solution)/shard_map/ppermute | solution.py:83
  537.6 11.7 %collective-permute-done.62 = bf16[328,1024]{1,0:T(8,128)(2,1)S(1)} collective-permute-done((bf16[328,1024]{1,0:T(8,128)(2,1)S(1)}, bf16[328,1024]{1,0:T(8,128)(2,1)S(1)}, u32[]{:S(2)}, u32[]{:S(2)}) %collective-permute-start.62) | collective-permute-done | bytes 671776 | tf_op jit(solution)/shard_map/ppermute | solution.py:83
  555.3 8.4 %collective-permute-done.81 = bf16[328,1024]{1,0:T(8,128)(2,1)S(1)} collective-permute-done((bf16[328,1024]{1,0:T(8,128)(2,1)S(1)}, bf16[328,1024]{1,0:T(8,128)(2,1)S(1)}, u32[]{:S(2)}, u32[]{:S(2)}) %collective-permute-start.81) | collective-permute-done | bytes 671776 | tf_op jit(solution)/shard_map/ppermute | solution.py:83
  566.4 11.7 %collective-permute-done.63 = bf16[328,1024]{1,0:T(8,128)(2,1)S(1)} collective-permute-done((bf16[328,1024]{1,0:T(8,128)(2,1)S(1)}, bf16[328,1024]{1,0:T(8,128)(2,1)S(1)}, u32[]{:S(2)}, u32[]{:S(2)}) %collective-permute-start.63) | collective-permute-done | bytes 671776 | tf_op jit(solution)/shard_map/ppermute | solution.py:83
  583.8 8.4 %collective-permute-done.82 = bf16[328,1024]{1,0:T(8,128)(2,1)S(1)} collective-permute-done((bf16[328,1024]{1,0:T(8,128)(2,1)S(1)}, bf16[328,1024]{1,0:T(8,128)(2,1)S(1)}, u32[]{:S(2)}, u32[]{:S(2)}) %collective-permute-start.82) | collective-permute-done | bytes 671776 | tf_op jit(solution)/shard_map/ppermute | solution.py:83
  593.1 6.3 %collective-permute-done.64 = bf16[328,1024]{1,0:T(8,128)(2,1)S(1)} collective-permute-done((bf16[328,1024]{1,0:T(8,128)(2,1)S(1)}, bf16[328,1024]{1,0:T(8,128)(2,1)S(1)}, u32[]{:S(2)}, u32[]{:S(2)}) %collective-permute-start.64) | collective-permute-done | bytes 671776 | tf_op jit(solution)/shard_map/ppermute | solution.py:83
  (484 shorter events, 204.0 us)
Async XLA Ops:
  10.4 31.9 %collective-permute-start = (bf16[200,2048]{1,0:T(8,128)(2,1)}, bf16[200,2048]{1,0:T(8,128)(2,1)}, u32[]{:S(2)}, u32[]{:S(2)}) collective-permute-start(bf16[200,2048]{1,0:T(8,128)(2,1)} %convolution_convert_fusion.9), channel_id=1, source_target_pairs={{0,2},{1,3},{2,4},{3,5},{4,6},{5,7},{6,8},{7,9},{8,10},{9,11},{10,... | collective-permute-start | bytes 2457608 | tf_op jit(solution)/shard_map/ppermute | solution.py:83
  14.1 64.5 %collective-permute-start.5 = (bf16[200,2048]{1,0:T(8,128)(2,1)}, bf16[200,2048]{1,0:T(8,128)(2,1)S(1)}, u32[]{:S(2)}, u32[]{:S(2)}) collective-permute-start(bf16[200,2048]{1,0:T(8,128)(2,1)} %convolution_convert_fusion.8), channel_id=1, source_target_pairs={{0,30},{1,31},{2,0},{3,1},{4,2},{5,3},{6,4},{7,5},{8,6},{9,7},{10,... | collective-permute-start | bytes 2457608 | tf_op jit(solution)/shard_map/ppermute | solution.py:83
  26.7 31.2 %collective-permute-start.4 = (bf16[328,1024]{1,0:T(8,128)(2,1)}, bf16[328,1024]{1,0:T(8,128)(2,1)}, u32[]{:S(2)}, u32[]{:S(2)}) collective-permute-start(bf16[328,1024]{1,0:T(8,128)(2,1)} %get-tuple-element.98), channel_id=1, source_target_pairs={{0,30},{1,31},{2,0},{3,1},{4,2},{5,3},{6,4},{7,5},{8,6},{9,7},{10,... | collective-permute-start | bytes 2015240 | tf_op jit(solution)/shard_map/ppermute | solution.py:83
  28.7 44.0 %collective-permute-start.3 = (bf16[328,1024]{1,0:T(8,128)(2,1)}, bf16[328,1024]{1,0:T(8,128)(2,1)}, u32[]{:S(2)}, u32[]{:S(2)}) collective-permute-start(bf16[328,1024]{1,0:T(8,128)(2,1)} %get-tuple-element.99), channel_id=1, source_target_pairs={{0,30},{1,31},{2,0},{3,1},{4,2},{5,3},{6,4},{7,5},{8,6},{9,7},{10,... | collective-permute-start | bytes 2015240 | tf_op jit(solution)/shard_map/ppermute | solution.py:83
  31.7 44.8 %collective-permute-start.2 = (bf16[328,1024]{1,0:T(8,128)(2,1)}, bf16[328,1024]{1,0:T(8,128)(2,1)}, u32[]{:S(2)}, u32[]{:S(2)}) collective-permute-start(bf16[328,1024]{1,0:T(8,128)(2,1)} %get-tuple-element.100), channel_id=1, source_target_pairs={{0,2},{1,3},{2,4},{3,5},{4,6},{5,7},{6,8},{7,9},{8,10},{9,11},{10,... | collective-permute-start | bytes 2015240 | tf_op jit(solution)/shard_map/ppermute | solution.py:83
  42.3 34.1 %collective-permute-start.1 = (bf16[328,1024]{1,0:T(8,128)(2,1)}, bf16[328,1024]{1,0:T(8,128)(2,1)}, u32[]{:S(2)}, u32[]{:S(2)}) collective-permute-start(bf16[328,1024]{1,0:T(8,128)(2,1)} %get-tuple-element.101), channel_id=1, source_target_pairs={{0,2},{1,3},{2,4},{3,5},{4,6},{5,7},{6,8},{7,9},{8,10},{9,11},{10,... | collective-permute-start | bytes 2015240 | tf_op jit(solution)/shard_map/ppermute | solution.py:83
  44.3 35.4 %all-to-all-start.2 = ((f32[32,1,96]{2,1,0:T(1,128)}), f32[32,1,96]{2,1,0:T(1,128)}, u32[]{:S(2)}, u32[]{:S(2)}) async-start(f32[32,1,96]{2,1,0:T(1,128)} %bitcast.13), calls=%async_computation.2 | async-start | bytes 32768 | tf_op jit(solution)/shard_map/all_to_all | solution.py:133
  57.9 32.2 %collective-permute-start.10 = (bf16[328,1024]{1,0:T(8,128)(2,1)}, bf16[328,1024]{1,0:T(8,128)(2,1)}, u32[]{:S(2)}, u32[]{:S(2)}) collective-permute-start(bf16[328,1024]{1,0:T(8,128)(2,1)} %collective-permute-done.4), channel_id=1, source_target_pairs={{0,30},{1,31},{2,0},{3,1},{4,2},{5,3},{6,4},{7,5},{8,6},{9,7},{10,... | collective-permute-start | bytes 2015240 | tf_op jit(solution)/shard_map/ppermute | solution.py:83
  72.6 39.1 %collective-permute-start.9 = (bf16[328,1024]{1,0:T(8,128)(2,1)}, bf16[328,1024]{1,0:T(8,128)(2,1)}, u32[]{:S(2)}, u32[]{:S(2)}) collective-permute-start(bf16[328,1024]{1,0:T(8,128)(2,1)} %collective-permute-done.3), channel_id=1, source_target_pairs={{0,30},{1,31},{2,0},{3,1},{4,2},{5,3},{6,4},{7,5},{8,6},{9,7},{10,... | collective-permute-start | bytes 2015240 | tf_op jit(solution)/shard_map/ppermute | solution.py:83
  76.5 33.9 %collective-permute-start.6 = (bf16[328,1024]{1,0:T(8,128)(2,1)}, bf16[328,1024]{1,0:T(8,128)(2,1)}, u32[]{:S(2)}, u32[]{:S(2)}) collective-permute-start(bf16[328,1024]{1,0:T(8,128)(2,1)} %collective-permute-done.1), channel_id=1, source_target_pairs={{0,2},{1,3},{2,4},{3,5},{4,6},{5,7},{6,8},{7,9},{8,10},{9,11},{10,... | collective-permute-start | bytes 2015240 | tf_op jit(solution)/shard_map/ppermute | solution.py:83
  78.6 45.0 %collective-permute-start.8 = (bf16[152,2048]{1,0:T(8,128)(2,1)}, bf16[152,2048]{1,0:T(8,128)(2,1)S(1)}, u32[]{:S(2)}, u32[]{:S(2)}) collective-permute-start(bf16[152,2048]{1,0:T(8,128)(2,1)} %slice.833), channel_id=1, source_target_pairs={{0,2},{1,3},{2,4},{3,5},{4,6},{5,7},{6,8},{7,9},{8,10},{9,11},{10,... | collective-permute-start | bytes 1867784 | tf_op jit(solution)/shard_map/ppermute | solution.py:83
  90.1 33.7 %collective-permute-start.11 = (bf16[152,2048]{1,0:T(8,128)(2,1)S(1)}, bf16[152,2048]{1,0:T(8,128)(2,1)S(1)}, u32[]{:S(2)}, u32[]{:S(2)}) collective-permute-start(bf16[152,2048]{1,0:T(8,128)(2,1)S(1)} %copy-done.4), channel_id=1, source_target_pairs={{0,30},{1,31},{2,0},{3,1},{4,2},{5,3},{6,4},{7,5},{8,6},{9,7},{10,... | collective-permute-start | bytes 1867784 | tf_op jit(solution)/shard_map/ppermute | solution.py:83
  96.0 63.7 %collective-permute-start.16 = (bf16[328,1024]{1,0:T(8,128)(2,1)}, bf16[328,1024]{1,0:T(8,128)(2,1)S(1)}, u32[]{:S(2)}, u32[]{:S(2)}) collective-permute-start(bf16[328,1024]{1,0:T(8,128)(2,1)} %collective-permute-done.10), channel_id=1, source_target_pairs={{0,30},{1,31},{2,0},{3,1},{4,2},{5,3},{6,4},{7,5},{8,6},{9,7},{10,... | collective-permute-start | bytes 2015240 | tf_op jit(solution)/shard_map/ppermute | solution.py:83
  110.4 50.9 %collective-permute-start.13 = (bf16[328,1024]{1,0:T(8,128)(2,1)}, bf16[328,1024]{1,0:T(8,128)(2,1)S(1)}, u32[]{:S(2)}, u32[]{:S(2)}) collective-permute-start(bf16[328,1024]{1,0:T(8,128)(2,1)} %collective-permute-done.7), channel_id=1, source_target_pairs={{0,2},{1,3},{2,4},{3,5},{4,6},{5,7},{6,8},{7,9},{8,10},{9,11},{10,... | collective-permute-start | bytes 2015240 | tf_op jit(solution)/shard_map/ppermute | solution.py:83
  111.8 50.0 %collective-permute-start.12 = (bf16[328,1024]{1,0:T(8,128)(2,1)}, bf16[328,1024]{1,0:T(8,128)(2,1)S(1)}, u32[]{:S(2)}, u32[]{:S(2)}) collective-permute-start(bf16[328,1024]{1,0:T(8,128)(2,1)} %collective-permute-done.6), channel_id=1, source_target_pairs={{0,2},{1,3},{2,4},{3,5},{4,6},{5,7},{6,8},{7,9},{8,10},{9,11},{10,... | collective-permute-start | bytes 2015240 | tf_op jit(solution)/shard_map/ppermute | solution.py:83
  123.6 33.9 %collective-permute-start.14 = (bf16[96,2048]{1,0:T(8,128)(2,1)S(1)}, bf16[96,2048]{1,0:T(8,128)(2,1)S(1)}, u32[]{:S(2)}, u32[]{:S(2)}) collective-permute-start(bf16[96,2048]{1,0:T(8,128)(2,1)S(1)} %slice.837), channel_id=1, source_target_pairs={{0,2},{1,3},{2,4},{3,5},{4,6},{5,7},{6,8},{7,9},{8,10},{9,11},{10,... | collective-permute-start | bytes 1179656 | tf_op jit(solution)/shard_map/ppermute | solution.py:83
  123.8 33.7 %collective-permute-start.17 = (bf16[96,2048]{1,0:T(8,128)(2,1)S(1)}, bf16[96,2048]{1,0:T(8,128)(2,1)S(1)}, u32[]{:S(2)}, u32[]{:S(2)}) collective-permute-start(bf16[96,2048]{1,0:T(8,128)(2,1)S(1)} %slice.839), channel_id=1, source_target_pairs={{0,30},{1,31},{2,0},{3,1},{4,2},{5,3},{6,4},{7,5},{8,6},{9,7},{10,... | collective-permute-start | bytes 1179656 | tf_op jit(solution)/shard_map/ppermute | solution.py:83
  157.5 36.6 %collective-permute-start.20 = (bf16[40,2048]{1,0:T(8,128)(2,1)S(1)}, bf16[40,2048]{1,0:T(8,128)(2,1)S(1)}, u32[]{:S(2)}, u32[]{:S(2)}) collective-permute-start(bf16[40,2048]{1,0:T(8,128)(2,1)S(1)} %slice.841), channel_id=1, source_target_pairs={{0,2},{1,3},{2,4},{3,5},{4,6},{5,7},{6,8},{7,9},{8,10},{9,11},{10,... | collective-permute-start | bytes 491528 | tf_op jit(solution)/shard_map/ppermute | solution.py:83
  159.7 50.7 %collective-permute-start.23 = (bf16[40,2048]{1,0:T(8,128)(2,1)S(1)}, bf16[40,2048]{1,0:T(8,128)(2,1)S(1)}, u32[]{:S(2)}, u32[]{:S(2)}) collective-permute-start(bf16[40,2048]{1,0:T(8,128)(2,1)S(1)} %slice.843), channel_id=1, source_target_pairs={{0,30},{1,31},{2,0},{3,1},{4,2},{5,3},{6,4},{7,5},{8,6},{9,7},{10,... | collective-permute-start | bytes 491528 | tf_op jit(solution)/shard_map/ppermute | solution.py:83
  161.3 29.5 %collective-permute-start.22 = (bf16[328,1024]{1,0:T(8,128)(2,1)S(1)}, bf16[328,1024]{1,0:T(8,128)(2,1)S(1)}, u32[]{:S(2)}, u32[]{:S(2)}) collective-permute-start(bf16[328,1024]{1,0:T(8,128)(2,1)S(1)} %collective-permute-done.16), channel_id=1, source_target_pairs={{0,30},{1,31},{2,0},{3,1},{4,2},{5,3},{6,4},{7,5},{8,6},{9,7},{10,... | collective-permute-start | bytes 2015240 | tf_op jit(solution)/shard_map/ppermute | solution.py:83
  161.8 29.4 %collective-permute-start.19 = (bf16[328,1024]{1,0:T(8,128)(2,1)S(1)}, bf16[328,1024]{1,0:T(8,128)(2,1)S(1)}, u32[]{:S(2)}, u32[]{:S(2)}) collective-permute-start(bf16[328,1024]{1,0:T(8,128)(2,1)S(1)} %collective-permute-done.13), channel_id=1, source_target_pairs={{0,2},{1,3},{2,4},{3,5},{4,6},{5,7},{6,8},{7,9},{8,10},{9,11},{10,... | collective-permute-start | bytes 2015240 | tf_op jit(solution)/shard_map/ppermute | solution.py:83
  191.2 32.0 %collective-permute-start.41 = (bf16[328,1024]{1,0:T(8,128)(2,1)S(1)}, bf16[328,1024]{1,0:T(8,128)(2,1)S(1)}, u32[]{:S(2)}, u32[]{:S(2)}) collective-permute-start(bf16[328,1024]{1,0:T(8,128)(2,1)S(1)} %collective-permute-done.22), channel_id=1, source_target_pairs={{0,30},{1,31},{2,0},{3,1},{4,2},{5,3},{6,4},{7,5},{8,6},{9,7},{10,... | collective-permute-start | bytes 2015240 | tf_op jit(solution)/shard_map/ppermute | solution.py:83
  192.4 46.5 %collective-permute-start.40 = (bf16[328,1024]{1,0:T(8,128)(2,1)S(1)}, bf16[328,1024]{1,0:T(8,128)(2,1)S(1)}, u32[]{:S(2)}, u32[]{:S(2)}) collective-permute-start(bf16[328,1024]{1,0:T(8,128)(2,1)S(1)} %collective-permute-done.19), channel_id=1, source_target_pairs={{0,2},{1,3},{2,4},{3,5},{4,6},{5,7},{6,8},{7,9},{8,10},{9,11},{10,... | collective-permute-start | bytes 2015240 | tf_op jit(solution)/shard_map/ppermute | solution.py:83
  194.1 45.8 %collective-permute-start.26 = (bf16[328,1024]{1,0:T(8,128)(2,1)S(1)}, bf16[328,1024]{1,0:T(8,128)(2,1)S(1)}, u32[]{:S(2)}, u32[]{:S(2)}) collective-permute-start(bf16[328,1024]{1,0:T(8,128)(2,1)S(1)} %collective-permute-done.18), channel_id=1, source_target_pairs={{0,2},{1,3},{2,4},{3,5},{4,6},{5,7},{6,8},{7,9},{8,10},{9,11},{10,... | collective-permute-start | bytes 2015240 | tf_op jit(solution)/shard_map/ppermute | solution.py:83
  208.8 28.8 %collective-permute-start.33 = (bf16[328,1024]{1,0:T(8,128)(2,1)S(1)}, bf16[328,1024]{1,0:T(8,128)(2,1)S(1)}, u32[]{:S(2)}, u32[]{:S(2)}) collective-permute-start(bf16[328,1024]{1,0:T(8,128)(2,1)S(1)} %collective-permute-done.21), channel_id=1, source_target_pairs={{0,30},{1,31},{2,0},{3,1},{4,2},{5,3},{6,4},{7,5},{8,6},{9,7},{10,... | collective-permute-start | bytes 2015240 | tf_op jit(solution)/shard_map/ppermute | solution.py:83
  210.8 75.0 %collective-permute-start.24 = (bf16[432,2048]{1,0:T(8,128)(2,1)S(1)}, bf16[432,2048]{1,0:T(8,128)(2,1)S(1)}, u32[]{:S(2)}, u32[]{:S(2)}) collective-permute-start(bf16[432,2048]{1,0:T(8,128)(2,1)S(1)} %get-tuple-element.102), channel_id=1, source_target_pairs={{0,1},{1,0},{2,3},{3,2},{4,5},{5,4},{6,7},{7,6},{8,9},{9,8},{10,11... | collective-permute-start | bytes 5308424 | tf_op jit(solution)/shard_map/ppermute | solution.py:155
  223.2 25.9 %collective-permute-start.43 = (bf16[264,1024]{1,0:T(8,128)(2,1)S(1)}, bf16[264,1024]{1,0:T(8,128)(2,1)S(1)}, u32[]{:S(2)}, u32[]{:S(2)}) collective-permute-start(bf16[264,1024]{1,0:T(8,128)(2,1)S(1)} %slice.894), channel_id=1, source_target_pairs={{0,30},{1,31},{2,0},{3,1},{4,2},{5,3},{6,4},{7,5},{8,6},{9,7},{10,... | collective-permute-start | bytes 1622024 | tf_op jit(solution)/shard_map/ppermute | solution.py:83
  270.6 28.9 %collective-permute-start.49 = (bf16[144,1024]{1,0:T(8,128)(2,1)S(1)}, bf16[144,1024]{1,0:T(8,128)(2,1)S(1)}, u32[]{:S(2)}, u32[]{:S(2)}) collective-permute-start(bf16[144,1024]{1,0:T(8,128)(2,1)S(1)} %slice.908), channel_id=1, source_target_pairs={{0,30},{1,31},{2,0},{3,1},{4,2},{5,3},{6,4},{7,5},{8,6},{9,7},{10,... | collective-permute-start | bytes 884744 | tf_op jit(solution)/shard_map/ppermute | solution.py:83
  361.0 30.5 %collective-permute-start.55 = (bf16[480,2048]{1,0:T(8,128)(2,1)S(1)}, bf16[480,2048]{1,0:T(8,128)(2,1)S(1)}, u32[]{:S(2)}, u32[]{:S(2)}) collective-permute-start(bf16[480,2048]{1,0:T(8,128)(2,1)S(1)} %slice.920), channel_id=1, source_target_pairs={{0,1},{1,0},{2,3},{3,2},{4,5},{5,4},{6,7},{7,6},{8,9},{9,8},{10,11... | collective-permute-start | bytes 5898248 | tf_op jit(solution)/shard_map/ppermute | solution.py:157
  439.1 26.6 %collective-permute-start.86 = (bf16[264,1024]{1,0:T(8,128)(2,1)S(1)}, bf16[264,1024]{1,0:T(8,128)(2,1)S(1)}, u32[]{:S(2)}, u32[]{:S(2)}) collective-permute-start(bf16[264,1024]{1,0:T(8,128)(2,1)S(1)} %fusion.78), channel_id=1, source_target_pairs={{0,2},{1,3},{2,4},{3,5},{4,6},{5,7},{6,8},{7,9},{8,10},{9,11},{10,... | collective-permute-start | bytes 1622024 | tf_op jit(solution)/shard_map/ppermute | solution.py:83
  440.9 25.4 %collective-permute-start.68 = (bf16[264,1024]{1,0:T(8,128)(2,1)S(1)}, bf16[264,1024]{1,0:T(8,128)(2,1)S(1)}, u32[]{:S(2)}, u32[]{:S(2)}) collective-permute-start(bf16[264,1024]{1,0:T(8,128)(2,1)S(1)} %fusion.76), channel_id=1, source_target_pairs={{0,2},{1,3},{2,4},{3,5},{4,6},{5,7},{6,8},{7,9},{8,10},{9,11},{10,... | collective-permute-start | bytes 1622024 | tf_op jit(solution)/shard_map/ppermute | solution.py:83
  451.8 25.5 %collective-permute-start.78 = (bf16[328,1024]{1,0:T(8,128)(2,1)S(1)}, bf16[328,1024]{1,0:T(8,128)(2,1)S(1)}, u32[]{:S(2)}, u32[]{:S(2)}) collective-permute-start(bf16[328,1024]{1,0:T(8,128)(2,1)S(1)} %fusion.69), channel_id=1, source_target_pairs={{0,30},{1,31},{2,0},{3,1},{4,2},{5,3},{6,4},{7,5},{8,6},{9,7},{10,... | collective-permute-start | bytes 2015240 | tf_op jit(solution)/shard_map/ppermute | solution.py:83
  463.4 28.3 %collective-permute-start.60 = (bf16[328,1024]{1,0:T(8,128)(2,1)S(1)}, bf16[328,1024]{1,0:T(8,128)(2,1)S(1)}, u32[]{:S(2)}, u32[]{:S(2)}) collective-permute-start(bf16[328,1024]{1,0:T(8,128)(2,1)S(1)} %fusion.59), channel_id=1, source_target_pairs={{0,30},{1,31},{2,0},{3,1},{4,2},{5,3},{6,4},{7,5},{8,6},{9,7},{10,... | collective-permute-start | bytes 2015240 | tf_op jit(solution)/shard_map/ppermute | solution.py:83
  466.1 28.3 %collective-permute-start.87 = (bf16[328,1024]{1,0:T(8,128)(2,1)S(1)}, bf16[328,1024]{1,0:T(8,128)(2,1)S(1)}, u32[]{:S(2)}, u32[]{:S(2)}) collective-permute-start(bf16[328,1024]{1,0:T(8,128)(2,1)S(1)} %fusion.74), channel_id=1, source_target_pairs={{0,2},{1,3},{2,4},{3,5},{4,6},{5,7},{6,8},{7,9},{8,10},{9,11},{10,... | collective-permute-start | bytes 2015240 | tf_op jit(solution)/shard_map/ppermute | solution.py:83
  466.7 28.3 %collective-permute-start.69 = (bf16[328,1024]{1,0:T(8,128)(2,1)S(1)}, bf16[328,1024]{1,0:T(8,128)(2,1)S(1)}, u32[]{:S(2)}, u32[]{:S(2)}) collective-permute-start(bf16[328,1024]{1,0:T(8,128)(2,1)S(1)} %fusion.64), channel_id=1, source_target_pairs={{0,2},{1,3},{2,4},{3,5},{4,6},{5,7},{6,8},{7,9},{8,10},{9,11},{10,... | collective-permute-start | bytes 2015240 | tf_op jit(solution)/shard_map/ppermute | solution.py:83
  477.8 28.3 %collective-permute-start.79 = (bf16[328,1024]{1,0:T(8,128)(2,1)S(1)}, bf16[328,1024]{1,0:T(8,128)(2,1)S(1)}, u32[]{:S(2)}, u32[]{:S(2)}) collective-permute-start(bf16[328,1024]{1,0:T(8,128)(2,1)S(1)} %fusion.68), channel_id=1, source_target_pairs={{0,30},{1,31},{2,0},{3,1},{4,2},{5,3},{6,4},{7,5},{8,6},{9,7},{10,... | collective-permute-start | bytes 2015240 | tf_op jit(solution)/shard_map/ppermute | solution.py:83
  492.2 28.3 %collective-permute-start.61 = (bf16[328,1024]{1,0:T(8,128)(2,1)S(1)}, bf16[328,1024]{1,0:T(8,128)(2,1)S(1)}, u32[]{:S(2)}, u32[]{:S(2)}) collective-permute-start(bf16[328,1024]{1,0:T(8,128)(2,1)S(1)} %fusion.58), channel_id=1, source_target_pairs={{0,30},{1,31},{2,0},{3,1},{4,2},{5,3},{6,4},{7,5},{8,6},{9,7},{10,... | collective-permute-start | bytes 2015240 | tf_op jit(solution)/shard_map/ppermute | solution.py:83
  494.9 28.3 %collective-permute-start.88 = (bf16[328,1024]{1,0:T(8,128)(2,1)S(1)}, bf16[328,1024]{1,0:T(8,128)(2,1)S(1)}, u32[]{:S(2)}, u32[]{:S(2)}) collective-permute-start(bf16[328,1024]{1,0:T(8,128)(2,1)S(1)} %fusion.73), channel_id=1, source_target_pairs={{0,2},{1,3},{2,4},{3,5},{4,6},{5,7},{6,8},{7,9},{8,10},{9,11},{10,... | collective-permute-start | bytes 2015240 | tf_op jit(solution)/shard_map/ppermute | solution.py:83
  495.5 28.3 %collective-permute-start.70 = (bf16[328,1024]{1,0:T(8,128)(2,1)S(1)}, bf16[328,1024]{1,0:T(8,128)(2,1)S(1)}, u32[]{:S(2)}, u32[]{:S(2)}) collective-permute-start(bf16[328,1024]{1,0:T(8,128)(2,1)S(1)} %fusion.63), channel_id=1, source_target_pairs={{0,2},{1,3},{2,4},{3,5},{4,6},{5,7},{6,8},{7,9},{8,10},{9,11},{10,... | collective-permute-start | bytes 2015240 | tf_op jit(solution)/shard_map/ppermute | solution.py:83
  506.6 28.3 %collective-permute-start.80 = (bf16[328,1024]{1,0:T(8,128)(2,1)S(1)}, bf16[328,1024]{1,0:T(8,128)(2,1)S(1)}, u32[]{:S(2)}, u32[]{:S(2)}) collective-permute-start(bf16[328,1024]{1,0:T(8,128)(2,1)S(1)} %fusion.67), channel_id=1, source_target_pairs={{0,30},{1,31},{2,0},{3,1},{4,2},{5,3},{6,4},{7,5},{8,6},{9,7},{10,... | collective-permute-start | bytes 2015240 | tf_op jit(solution)/shard_map/ppermute | solution.py:83
  521.0 28.3 %collective-permute-start.62 = (bf16[328,1024]{1,0:T(8,128)(2,1)S(1)}, bf16[328,1024]{1,0:T(8,128)(2,1)S(1)}, u32[]{:S(2)}, u32[]{:S(2)}) collective-permute-start(bf16[328,1024]{1,0:T(8,128)(2,1)S(1)} %fusion.57), channel_id=1, source_target_pairs={{0,30},{1,31},{2,0},{3,1},{4,2},{5,3},{6,4},{7,5},{8,6},{9,7},{10,... | collective-permute-start | bytes 2015240 | tf_op jit(solution)/shard_map/ppermute | solution.py:83
  523.7 28.3 %collective-permute-start.89 = (bf16[328,1024]{1,0:T(8,128)(2,1)S(1)}, bf16[328,1024]{1,0:T(8,128)(2,1)S(1)}, u32[]{:S(2)}, u32[]{:S(2)}) collective-permute-start(bf16[328,1024]{1,0:T(8,128)(2,1)S(1)} %fusion.72), channel_id=1, source_target_pairs={{0,2},{1,3},{2,4},{3,5},{4,6},{5,7},{6,8},{7,9},{8,10},{9,11},{10,... | collective-permute-start | bytes 2015240 | tf_op jit(solution)/shard_map/ppermute | solution.py:83
  524.3 28.3 %collective-permute-start.71 = (bf16[328,1024]{1,0:T(8,128)(2,1)S(1)}, bf16[328,1024]{1,0:T(8,128)(2,1)S(1)}, u32[]{:S(2)}, u32[]{:S(2)}) collective-permute-start(bf16[328,1024]{1,0:T(8,128)(2,1)S(1)} %fusion.62), channel_id=1, source_target_pairs={{0,2},{1,3},{2,4},{3,5},{4,6},{5,7},{6,8},{7,9},{8,10},{9,11},{10,... | collective-permute-start | bytes 2015240 | tf_op jit(solution)/shard_map/ppermute | solution.py:83
  535.4 28.3 %collective-permute-start.81 = (bf16[328,1024]{1,0:T(8,128)(2,1)S(1)}, bf16[328,1024]{1,0:T(8,128)(2,1)S(1)}, u32[]{:S(2)}, u32[]{:S(2)}) collective-permute-start(bf16[328,1024]{1,0:T(8,128)(2,1)S(1)} %fusion.66), channel_id=1, source_target_pairs={{0,30},{1,31},{2,0},{3,1},{4,2},{5,3},{6,4},{7,5},{8,6},{9,7},{10,... | collective-permute-start | bytes 2015240 | tf_op jit(solution)/shard_map/ppermute | solution.py:83
  549.8 28.3 %collective-permute-start.63 = (bf16[328,1024]{1,0:T(8,128)(2,1)S(1)}, bf16[328,1024]{1,0:T(8,128)(2,1)S(1)}, u32[]{:S(2)}, u32[]{:S(2)}) collective-permute-start(bf16[328,1024]{1,0:T(8,128)(2,1)S(1)} %fusion.56), channel_id=1, source_target_pairs={{0,30},{1,31},{2,0},{3,1},{4,2},{5,3},{6,4},{7,5},{8,6},{9,7},{10,... | collective-permute-start | bytes 2015240 | tf_op jit(solution)/shard_map/ppermute | solution.py:83
  552.5 28.3 %collective-permute-start.90 = (bf16[328,1024]{1,0:T(8,128)(2,1)S(1)}, bf16[328,1024]{1,0:T(8,128)(2,1)S(1)}, u32[]{:S(2)}, u32[]{:S(2)}) collective-permute-start(bf16[328,1024]{1,0:T(8,128)(2,1)S(1)} %fusion.71), channel_id=1, source_target_pairs={{0,2},{1,3},{2,4},{3,5},{4,6},{5,7},{6,8},{7,9},{8,10},{9,11},{10,... | collective-permute-start | bytes 2015240 | tf_op jit(solution)/shard_map/ppermute | solution.py:83
  553.1 28.3 %collective-permute-start.72 = (bf16[328,1024]{1,0:T(8,128)(2,1)S(1)}, bf16[328,1024]{1,0:T(8,128)(2,1)S(1)}, u32[]{:S(2)}, u32[]{:S(2)}) collective-permute-start(bf16[328,1024]{1,0:T(8,128)(2,1)S(1)} %fusion.61), channel_id=1, source_target_pairs={{0,2},{1,3},{2,4},{3,5},{4,6},{5,7},{6,8},{7,9},{8,10},{9,11},{10,... | collective-permute-start | bytes 2015240 | tf_op jit(solution)/shard_map/ppermute | solution.py:83
  564.2 28.1 %collective-permute-start.82 = (bf16[328,1024]{1,0:T(8,128)(2,1)S(1)}, bf16[328,1024]{1,0:T(8,128)(2,1)S(1)}, u32[]{:S(2)}, u32[]{:S(2)}) collective-permute-start(bf16[328,1024]{1,0:T(8,128)(2,1)S(1)} %fusion.65), channel_id=1, source_target_pairs={{0,30},{1,31},{2,0},{3,1},{4,2},{5,3},{6,4},{7,5},{8,6},{9,7},{10,... | collective-permute-start | bytes 2015240 | tf_op jit(solution)/shard_map/ppermute | solution.py:83
  (119 other events, 3909.2 us)

commit v4 on v3

--- a/solution.py
+++ b/solution.py
@@ -11,7 +11,6 @@
 HOPS = (528, 480, 424, 368, 328, 264, 224, 144, 80)
 NEAR = 4
 PARTS = 2
-HOLD = 7
 BATCHES = ((1, 2, 3, 4), (5, 6, 7, 8, 9))
 WAYS = (1, -1)
 
@@ -129,8 +128,9 @@
 
     sent = [jnp.maximum(jnp.minimum(after, cut) - before, 0), jnp.maximum(after - jnp.maximum(before, cut), 0)]
     row = jnp.concatenate(sent + [jnp.full((experts,), spilt, I32)]).astype(F32)
-    row, _ = lax.optimization_barrier((jnp.broadcast_to(row, (experts, row.shape[0])), near_at[1, 1]))
+    row = jnp.broadcast_to(row, (experts, row.shape[0]))
     table = lax.all_to_all(row, "ep", split_axis=0, concat_axis=0, tiled=True)
+    table, _ = lax.optimization_barrier((table, far_at[1, 2, 0]))
     spilt = jnp.max(table[:, 2 * experts]) > 0
     hops = jnp.arange(1, far + 1, dtype=I32)
     slot = jnp.arange(capacity, dtype=F32)
@@ -186,8 +186,6 @@
             put = dot(pick(way, k, fixed, HOPS[k - 1]).T, outs[way, k]).astype(BF16)
             if k < NEAR:
                 put = put + jnp.pad(held_near[way], ((0, HOPS[k - 1] - HOPS[k]), (0, 0)))
-            elif HOLD:
-                put, _ = lax.optimization_barrier((put, far_at[way, HOLD, 0]))
             held_near[way] = hop(put, -way)
     for k in range(far, 0, -1):
         rows = min(fixed, HOPS[k - 1])
@@ -198,6 +196,8 @@
                     got = held[way, part]
                     put = put + jnp.pad(got, ((0, rows - got.shape[0]), (0, 0)))
                 held[way, part] = hop(put, -way)
+        if k == NEAR:
+            held_near, _ = lax.optimization_barrier((held_near, held[1, 0]))
 
     early = mix(places[0], weights, outs[0, 0])
     for way in WAYS:

time: 616 us -> 628 us (1.019)
  starting transfers between devices: 137 us -> 152 us
  matrix products: 87.7 us -> 81.4 us
    all_to_all x1, starting transfers between devices: 9.08 us -> 17.8 us  [body(): table = lax.all_to_all(row, 'ep', split_axis=0, concat_axis=0, tiled=True)]
  transfers between devices with their start and end apart: 93 -> 93, of which waited for: 41 -> 50; matrix products, arithmetic and copies ran while one was open for 18% -> 18% of each run, Pallas kernels for 0% -> 0%
where the time goes in v4:
time: 628 us; the launch traced here: 620 us
  waiting for transfers between devices  340 us (54%)
  starting transfers between devices  152 us (24%)
  matrix products  81.4 us (13%)
  other arithmetic  20.2 us (3%)
  local copies, waits for them, and re-layouts  19.2 us (3%)
    ppermute x88, waiting for transfers between devices, body(): hop = lambda block, way: lax.ppermute(block, 'ep', step[way])  340 us
    ppermute x88, starting transfers between devices, body(): hop = lambda block, way: lax.ppermute(block, 'ep', step[way])  134 us
    dot_general x107, matrix products, dot(): return jnp.dot(a, b, preferred_element_type=F32)  79.4 us
    all_to_all x1, starting transfers between devices, body(): table = lax.all_to_all(row, 'ep', split_axis=0, concat_axis=0, tiled=True)  17.8 us
  transfers between devices with their start and end apart: 93, of which 50 were waited for; matrix products, arithmetic and copies ran while one was open for 18% of the time, Pallas kernels for 0%

profile of v4, /device:TPU:70, one launch (start us, length us, event | category | flops | bytes accessed | tf_op | source)
XLA Modules:
  0.0 619.6 jit_solution(11258308297561018525)
XLA Ops:
  5.5 17.8 %all-to-all-start.2 = ((f32[32,1,96]{2,1,0:T(1,128)}), f32[32,1,96]{2,1,0:T(1,128)S(1)}, u32[]{:S(2)}, u32[]{:S(2)}) async-start(f32[32,1,96]{2,1,0:T(1,128)} %broadcast_in_dim.145), calls=%async_computation.2 | async-start | bytes 32768 | tf_op jit(solution)/shard_map/all_to_all | solution.py:132
  45.6 6.3 %collective-permute-done.5 = bf16[328,1024]{1,0:T(8,128)(2,1)} collective-permute-done((bf16[328,1024]{1,0:T(8,128)(2,1)}, bf16[328,1024]{1,0:T(8,128)(2,1)}, u32[]{:S(2)}, u32[]{:S(2)}) %collective-permute-start.5) | collective-permute-done | bytes 671776 | tf_op jit(solution)/shard_map/ppermute | solution.py:82
  53.4 13.8 %collective-permute-done = bf16[328,1024]{1,0:T(8,128)(2,1)} collective-permute-done((bf16[328,1024]{1,0:T(8,128)(2,1)}, bf16[328,1024]{1,0:T(8,128)(2,1)}, u32[]{:S(2)}, u32[]{:S(2)}) %collective-permute-start) | collective-permute-done | bytes 671776 | tf_op jit(solution)/shard_map/ppermute | solution.py:82
  70.2 12.5 %collective-permute-done.4 = bf16[328,1024]{1,0:T(8,128)(2,1)} collective-permute-done((bf16[328,1024]{1,0:T(8,128)(2,1)}, bf16[328,1024]{1,0:T(8,128)(2,1)}, u32[]{:S(2)}, u32[]{:S(2)}) %collective-permute-start.4) | collective-permute-done | bytes 671776 | tf_op jit(solution)/shard_map/ppermute | solution.py:82
  90.7 5.3 collective-permute-done.1
  103.2 7.2 %collective-permute-done.7 = bf16[328,1024]{1,0:T(8,128)(2,1)} collective-permute-done((bf16[328,1024]{1,0:T(8,128)(2,1)}, bf16[328,1024]{1,0:T(8,128)(2,1)}, u32[]{:S(2)}, u32[]{:S(2)}) %collective-permute-start.7) | collective-permute-done | bytes 671776 | tf_op jit(solution)/shard_map/ppermute | solution.py:82
  134.8 25.1 %collective-permute-done.14 = bf16[96,2048]{1,0:T(8,128)(2,1)S(1)} collective-permute-done((bf16[96,2048]{1,0:T(8,128)(2,1)S(1)}, bf16[96,2048]{1,0:T(8,128)(2,1)S(1)}, u32[]{:S(2)}, u32[]{:S(2)}) %collective-permute-start.14) | collective-permute-done | bytes 393248 | tf_op jit(solution)/shard_map/ppermute | solution.py:82
  168.7 9.3 %collective-permute-done.15 = bf16[328,1024]{1,0:T(8,128)(2,1)S(1)} collective-permute-done((bf16[328,1024]{1,0:T(8,128)(2,1)}, bf16[328,1024]{1,0:T(8,128)(2,1)S(1)}, u32[]{:S(2)}, u32[]{:S(2)}) %collective-permute-start.15) | collective-permute-done | bytes 671776 | tf_op jit(solution)/shard_map/ppermute | solution.py:82
  179.0 6.3 %collective-permute-done.19 = bf16[328,1024]{1,0:T(8,128)(2,1)S(1)} collective-permute-done((bf16[328,1024]{1,0:T(8,128)(2,1)S(1)}, bf16[328,1024]{1,0:T(8,128)(2,1)S(1)}, u32[]{:S(2)}, u32[]{:S(2)}) %collective-permute-start.19) | collective-permute-done | bytes 671776 | tf_op jit(solution)/shard_map/ppermute | solution.py:82
  186.5 10.5 %collective-permute-done.18 = bf16[328,1024]{1,0:T(8,128)(2,1)S(1)} collective-permute-done((bf16[328,1024]{1,0:T(8,128)(2,1)S(1)}, bf16[328,1024]{1,0:T(8,128)(2,1)S(1)}, u32[]{:S(2)}, u32[]{:S(2)}) %collective-permute-start.18) | collective-permute-done | bytes 671776 | tf_op jit(solution)/shard_map/ppermute | solution.py:82
  201.7 8.7 %collective-permute-done.21 = bf16[328,1024]{1,0:T(8,128)(2,1)S(1)} collective-permute-done((bf16[328,1024]{1,0:T(8,128)(2,1)S(1)}, bf16[328,1024]{1,0:T(8,128)(2,1)S(1)}, u32[]{:S(2)}, u32[]{:S(2)}) %collective-permute-start.21) | collective-permute-done | bytes 671776 | tf_op jit(solution)/shard_map/ppermute | solution.py:82
  214.9 9.9 %collective-permute-done.37 = bf16[328,1024]{1,0:T(8,128)(2,1)S(1)} collective-permute-done((bf16[328,1024]{1,0:T(8,128)(2,1)S(1)}, bf16[328,1024]{1,0:T(8,128)(2,1)S(1)}, u32[]{:S(2)}, u32[]{:S(2)}) %collective-permute-start.37) | collective-permute-done | bytes 671776 | tf_op jit(solution)/shard_map/ppermute | solution.py:82
  227.8 11.3 %collective-permute-done.36 = bf16[328,1024]{1,0:T(8,128)(2,1)S(1)} collective-permute-done((bf16[328,1024]{1,0:T(8,128)(2,1)S(1)}, bf16[328,1024]{1,0:T(8,128)(2,1)S(1)}, u32[]{:S(2)}, u32[]{:S(2)}) %collective-permute-start.36) | collective-permute-done | bytes 671776 | tf_op jit(solution)/shard_map/ppermute | solution.py:82
  245.3 5.4 collective-permute-done.41
  253.8 8.5 %collective-permute-done.40 = bf16[264,1024]{1,0:T(8,128)(2,1)S(1)} collective-permute-done((bf16[264,1024]{1,0:T(8,128)(2,1)S(1)}, bf16[264,1024]{1,0:T(8,128)(2,1)S(1)}, u32[]{:S(2)}, u32[]{:S(2)}) %collective-permute-start.40) | collective-permute-done | bytes 540704 | tf_op jit(solution)/shard_map/ppermute | solution.py:82
  275.2 6.8 %collective-permute-done.44 = bf16[224,1024]{1,0:T(8,128)(2,1)S(1)} collective-permute-done((bf16[224,1024]{1,0:T(8,128)(2,1)S(1)}, bf16[224,1024]{1,0:T(8,128)(2,1)S(1)}, u32[]{:S(2)}, u32[]{:S(2)}) %collective-permute-start.44) | collective-permute-done | bytes 458784 | tf_op jit(solution)/shard_map/ppermute | solution.py:82
  288.7 3.8 fusion.31
  292.5 3.8 fusion.35
  296.3 4.1 fusion.40
  330.8 4.2 collective-permute-done.26
  337.2 4.2 fusion.29
  341.5 4.3 fusion.33
  345.7 4.6 fusion.37
  356.2 7.3 %collective-permute-done.31 = bf16[96,2048]{1,0:T(8,128)(2,1)S(1)} collective-permute-done((bf16[96,2048]{1,0:T(8,128)(2,1)S(1)}, bf16[96,2048]{1,0:T(8,128)(2,1)S(1)}, u32[]{:S(2)}, u32[]{:S(2)}) %collective-permute-start.31) | collective-permute-done | bytes 393248 | tf_op jit(solution)/shard_map/ppermute | solution.py:82
  363.9 4.2 collective-permute-start.32
  368.3 5.0 collective-permute-done.28
  373.9 7.0 %collective-permute-done.32 = bf16[152,2048]{1,0:T(8,128)(2,1)S(1)} collective-permute-done((bf16[152,2048]{1,0:T(8,128)(2,1)S(1)}, bf16[152,2048]{1,0:T(8,128)(2,1)S(1)}, u32[]{:S(2)}, u32[]{:S(2)}) %collective-permute-start.32) | collective-permute-done | bytes 622624 | tf_op jit(solution)/shard_map/ppermute | solution.py:82
  381.5 3.8 collective-permute-start.33
  389.1 8.7 %collective-permute-done.83 = bf16[80,1024]{1,0:T(8,128)(2,1)S(1)} collective-permute-done((bf16[80,1024]{1,0:T(8,128)(2,1)S(1)}, bf16[80,1024]{1,0:T(8,128)(2,1)S(1)}, u32[]{:S(2)}, u32[]{:S(2)}) %collective-permute-start.83) | collective-permute-done | bytes 163872 | tf_op jit(solution)/shard_map/ppermute | solution.py:82
  398.2 8.5 %collective-permute-done.56 = bf16[80,1024]{1,0:T(8,128)(2,1)S(1)} collective-permute-done((bf16[80,1024]{1,0:T(8,128)(2,1)S(1)}, bf16[80,1024]{1,0:T(8,128)(2,1)S(1)}, u32[]{:S(2)}, u32[]{:S(2)}) %collective-permute-start.56) | collective-permute-done | bytes 163872 | tf_op jit(solution)/shard_map/ppermute | solution.py:82
  413.7 5.7 collective-permute-done.57
  428.0 4.1 collective-permute-start.76
  433.0 4.2 collective-permute-done.58
  437.6 5.5 collective-permute-done.76
  450.3 9.1 %collective-permute-done.59 = bf16[264,1024]{1,0:T(8,128)(2,1)S(1)} collective-permute-done((bf16[264,1024]{1,0:T(8,128)(2,1)S(1)}, bf16[264,1024]{1,0:T(8,128)(2,1)S(1)}, u32[]{:S(2)}, u32[]{:S(2)}) %collective-permute-start.59) | collective-permute-done | bytes 540704 | tf_op jit(solution)/shard_map/ppermute | solution.py:82
  459.9 7.0 %collective-permute-done.77 = bf16[264,1024]{1,0:T(8,128)(2,1)S(1)} collective-permute-done((bf16[264,1024]{1,0:T(8,128)(2,1)S(1)}, bf16[264,1024]{1,0:T(8,128)(2,1)S(1)}, u32[]{:S(2)}, u32[]{:S(2)}) %collective-permute-start.77) | collective-permute-done | bytes 540704 | tf_op jit(solution)/shard_map/ppermute | solution.py:82
  467.0 3.9 collective-permute-start.60
  474.4 11.9 %collective-permute-done.60 = bf16[328,1024]{1,0:T(8,128)(2,1)S(1)} collective-permute-done((bf16[328,1024]{1,0:T(8,128)(2,1)S(1)}, bf16[328,1024]{1,0:T(8,128)(2,1)S(1)}, u32[]{:S(2)}, u32[]{:S(2)}) %collective-permute-start.60) | collective-permute-done | bytes 671776 | tf_op jit(solution)/shard_map/ppermute | solution.py:82
  486.8 10.0 %collective-permute-done.78 = bf16[328,1024]{1,0:T(8,128)(2,1)S(1)} collective-permute-done((bf16[328,1024]{1,0:T(8,128)(2,1)S(1)}, bf16[328,1024]{1,0:T(8,128)(2,1)S(1)}, u32[]{:S(2)}, u32[]{:S(2)}) %collective-permute-start.78) | collective-permute-done | bytes 671776 | tf_op jit(solution)/shard_map/ppermute | solution.py:82
  507.5 8.4 %collective-permute-done.61 = bf16[328,1024]{1,0:T(8,128)(2,1)S(1)} collective-permute-done((bf16[328,1024]{1,0:T(8,128)(2,1)S(1)}, bf16[328,1024]{1,0:T(8,128)(2,1)S(1)}, u32[]{:S(2)}, u32[]{:S(2)}) %collective-permute-start.61) | collective-permute-done | bytes 671776 | tf_op jit(solution)/shard_map/ppermute | solution.py:82
  520.2 10.1 %collective-permute-done.79 = bf16[328,1024]{1,0:T(8,128)(2,1)S(1)} collective-permute-done((bf16[328,1024]{1,0:T(8,128)(2,1)S(1)}, bf16[328,1024]{1,0:T(8,128)(2,1)S(1)}, u32[]{:S(2)}, u32[]{:S(2)}) %collective-permute-start.79) | collective-permute-done | bytes 671776 | tf_op jit(solution)/shard_map/ppermute | solution.py:82
  537.7 17.0 %collective-permute-done.80 = bf16[328,1024]{1,0:T(8,128)(2,1)S(1)} collective-permute-done((bf16[328,1024]{1,0:T(8,128)(2,1)S(1)}, bf16[328,1024]{1,0:T(8,128)(2,1)S(1)}, u32[]{:S(2)}, u32[]{:S(2)}) %collective-permute-start.80) | collective-permute-done | bytes 671776 | tf_op jit(solution)/shard_map/ppermute | solution.py:82
  555.1 3.8 collective-permute-start.81
  565.3 9.1 %collective-permute-done.81 = bf16[328,1024]{1,0:T(8,128)(2,1)S(1)} collective-permute-done((bf16[328,1024]{1,0:T(8,128)(2,1)S(1)}, bf16[328,1024]{1,0:T(8,128)(2,1)S(1)}, u32[]{:S(2)}, u32[]{:S(2)}) %collective-permute-start.81) | collective-permute-done | bytes 671776 | tf_op jit(solution)/shard_map/ppermute | solution.py:82
  578.6 10.1 %collective-permute-done.63 = bf16[328,1024]{1,0:T(8,128)(2,1)S(1)} collective-permute-done((bf16[328,1024]{1,0:T(8,128)(2,1)S(1)}, bf16[328,1024]{1,0:T(8,128)(2,1)S(1)}, u32[]{:S(2)}, u32[]{:S(2)}) %collective-permute-start.63) | collective-permute-done | bytes 671776 | tf_op jit(solution)/shard_map/ppermute | solution.py:82
  589.2 3.8 collective-permute-start.64
  594.2 8.6 %collective-permute-done.82 = bf16[328,1024]{1,0:T(8,128)(2,1)S(1)} collective-permute-done((bf16[328,1024]{1,0:T(8,128)(2,1)S(1)}, bf16[328,1024]{1,0:T(8,128)(2,1)S(1)}, u32[]{:S(2)}, u32[]{:S(2)}) %collective-permute-start.82) | collective-permute-done | bytes 671776 | tf_op jit(solution)/shard_map/ppermute | solution.py:82
  603.7 6.3 %collective-permute-done.64 = bf16[328,1024]{1,0:T(8,128)(2,1)S(1)} collective-permute-done((bf16[328,1024]{1,0:T(8,128)(2,1)S(1)}, bf16[328,1024]{1,0:T(8,128)(2,1)S(1)}, u32[]{:S(2)}, u32[]{:S(2)}) %collective-permute-start.64) | collective-permute-done | bytes 671776 | tf_op jit(solution)/shard_map/ppermute | solution.py:82
  (488 shorter events, 236.8 us)
Async XLA Ops:
  5.5 92.3 %all-to-all-start.2 = ((f32[32,1,96]{2,1,0:T(1,128)}), f32[32,1,96]{2,1,0:T(1,128)S(1)}, u32[]{:S(2)}, u32[]{:S(2)}) async-start(f32[32,1,96]{2,1,0:T(1,128)} %broadcast_in_dim.145), calls=%async_computation.2 | async-start | bytes 32768 | tf_op jit(solution)/shard_map/all_to_all | solution.py:132
  30.2 56.0 %collective-permute-start.3 = (bf16[200,2048]{1,0:T(8,128)(2,1)}, bf16[200,2048]{1,0:T(8,128)(2,1)S(1)}, u32[]{:S(2)}, u32[]{:S(2)}) collective-permute-start(bf16[200,2048]{1,0:T(8,128)(2,1)} %convolution_convert_fusion.9), channel_id=1, source_target_pairs={{0,2},{1,3},{2,4},{3,5},{4,6},{5,7},{6,8},{7,9},{8,10},{9,11},{10,... | collective-permute-start | bytes 2457608 | tf_op jit(solution)/shard_map/ppermute | solution.py:82
  37.7 29.5 %collective-permute-start = (bf16[328,1024]{1,0:T(8,128)(2,1)}, bf16[328,1024]{1,0:T(8,128)(2,1)}, u32[]{:S(2)}, u32[]{:S(2)}) collective-permute-start(bf16[328,1024]{1,0:T(8,128)(2,1)} %get-tuple-element.101), channel_id=1, source_target_pairs={{0,2},{1,3},{2,4},{3,5},{4,6},{5,7},{6,8},{7,9},{8,10},{9,11},{10,... | collective-permute-start | bytes 2015240 | tf_op jit(solution)/shard_map/ppermute | solution.py:82
  39.4 49.2 %collective-permute-start.6 = (bf16[200,2048]{1,0:T(8,128)(2,1)}, bf16[200,2048]{1,0:T(8,128)(2,1)}, u32[]{:S(2)}, u32[]{:S(2)}) collective-permute-start(bf16[200,2048]{1,0:T(8,128)(2,1)} %convolution_convert_fusion.8), channel_id=1, source_target_pairs={{0,30},{1,31},{2,0},{3,1},{4,2},{5,3},{6,4},{7,5},{8,6},{9,7},{10,... | collective-permute-start | bytes 2457608 | tf_op jit(solution)/shard_map/ppermute | solution.py:82
  42.5 40.2 %collective-permute-start.4 = (bf16[328,1024]{1,0:T(8,128)(2,1)}, bf16[328,1024]{1,0:T(8,128)(2,1)}, u32[]{:S(2)}, u32[]{:S(2)}) collective-permute-start(bf16[328,1024]{1,0:T(8,128)(2,1)} %get-tuple-element.99), channel_id=1, source_target_pairs={{0,30},{1,31},{2,0},{3,1},{4,2},{5,3},{6,4},{7,5},{8,6},{9,7},{10,... | collective-permute-start | bytes 2015240 | tf_op jit(solution)/shard_map/ppermute | solution.py:82
  51.9 33.8 %collective-permute-start.2 = (bf16[328,1024]{1,0:T(8,128)(2,1)}, bf16[328,1024]{1,0:T(8,128)(2,1)}, u32[]{:S(2)}, u32[]{:S(2)}) collective-permute-start(bf16[328,1024]{1,0:T(8,128)(2,1)} %get-tuple-element.100), channel_id=1, source_target_pairs={{0,2},{1,3},{2,4},{3,5},{4,6},{5,7},{6,8},{7,9},{8,10},{9,11},{10,... | collective-permute-start | bytes 2015240 | tf_op jit(solution)/shard_map/ppermute | solution.py:82
  67.2 28.8 %collective-permute-start.1 = (bf16[328,1024]{1,0:T(8,128)(2,1)}, bf16[328,1024]{1,0:T(8,128)(2,1)}, u32[]{:S(2)}, u32[]{:S(2)}) collective-permute-start(bf16[328,1024]{1,0:T(8,128)(2,1)} %collective-permute-done), channel_id=1, source_target_pairs={{0,2},{1,3},{2,4},{3,5},{4,6},{5,7},{6,8},{7,9},{8,10},{9,11},{10,... | collective-permute-start | bytes 2015240 | tf_op jit(solution)/shard_map/ppermute | solution.py:82
  82.7 33.5 %collective-permute-start.10 = (bf16[328,1024]{1,0:T(8,128)(2,1)}, bf16[328,1024]{1,0:T(8,128)(2,1)}, u32[]{:S(2)}, u32[]{:S(2)}) collective-permute-start(bf16[328,1024]{1,0:T(8,128)(2,1)} %collective-permute-done.5), channel_id=1, source_target_pairs={{0,30},{1,31},{2,0},{3,1},{4,2},{5,3},{6,4},{7,5},{8,6},{9,7},{10,... | collective-permute-start | bytes 2015240 | tf_op jit(solution)/shard_map/ppermute | solution.py:82
  85.7 37.0 %collective-permute-start.9 = (bf16[328,1024]{1,0:T(8,128)(2,1)}, bf16[328,1024]{1,0:T(8,128)(2,1)}, u32[]{:S(2)}, u32[]{:S(2)}) collective-permute-start(bf16[328,1024]{1,0:T(8,128)(2,1)} %collective-permute-done.4), channel_id=1, source_target_pairs={{0,30},{1,31},{2,0},{3,1},{4,2},{5,3},{6,4},{7,5},{8,6},{9,7},{10,... | collective-permute-start | bytes 2015240 | tf_op jit(solution)/shard_map/ppermute | solution.py:82
  86.2 24.2 %collective-permute-start.7 = (bf16[328,1024]{1,0:T(8,128)(2,1)}, bf16[328,1024]{1,0:T(8,128)(2,1)}, u32[]{:S(2)}, u32[]{:S(2)}) collective-permute-start(bf16[328,1024]{1,0:T(8,128)(2,1)} %collective-permute-done.2), channel_id=1, source_target_pairs={{0,2},{1,3},{2,4},{3,5},{4,6},{5,7},{6,8},{7,9},{8,10},{9,11},{10,... | collective-permute-start | bytes 2015240 | tf_op jit(solution)/shard_map/ppermute | solution.py:82
  88.6 35.7 %collective-permute-start.8 = (bf16[152,2048]{1,0:T(8,128)(2,1)}, bf16[152,2048]{1,0:T(8,128)(2,1)}, u32[]{:S(2)}, u32[]{:S(2)}) collective-permute-start(bf16[152,2048]{1,0:T(8,128)(2,1)} %slice.830), channel_id=1, source_target_pairs={{0,2},{1,3},{2,4},{3,5},{4,6},{5,7},{6,8},{7,9},{8,10},{9,11},{10,... | collective-permute-start | bytes 1867784 | tf_op jit(solution)/shard_map/ppermute | solution.py:82
  96.0 33.2 %collective-permute-start.11 = (bf16[152,2048]{1,0:T(8,128)(2,1)}, bf16[152,2048]{1,0:T(8,128)(2,1)S(1)}, u32[]{:S(2)}, u32[]{:S(2)}) collective-permute-start(bf16[152,2048]{1,0:T(8,128)(2,1)} %slice.832), channel_id=1, source_target_pairs={{0,30},{1,31},{2,0},{3,1},{4,2},{5,3},{6,4},{7,5},{8,6},{9,7},{10,... | collective-permute-start | bytes 1867784 | tf_op jit(solution)/shard_map/ppermute | solution.py:82
  110.4 55.0 %collective-permute-start.13 = (bf16[328,1024]{1,0:T(8,128)(2,1)}, bf16[328,1024]{1,0:T(8,128)(2,1)S(1)}, u32[]{:S(2)}, u32[]{:S(2)}) collective-permute-start(bf16[328,1024]{1,0:T(8,128)(2,1)} %collective-permute-done.7), channel_id=1, source_target_pairs={{0,2},{1,3},{2,4},{3,5},{4,6},{5,7},{6,8},{7,9},{8,10},{9,11},{10,... | collective-permute-start | bytes 2015240 | tf_op jit(solution)/shard_map/ppermute | solution.py:82
  116.2 45.8 %collective-permute-start.16 = (bf16[328,1024]{1,0:T(8,128)(2,1)}, bf16[328,1024]{1,0:T(8,128)(2,1)S(1)}, u32[]{:S(2)}, u32[]{:S(2)}) collective-permute-start(bf16[328,1024]{1,0:T(8,128)(2,1)} %collective-permute-done.10), channel_id=1, source_target_pairs={{0,30},{1,31},{2,0},{3,1},{4,2},{5,3},{6,4},{7,5},{8,6},{9,7},{10,... | collective-permute-start | bytes 2015240 | tf_op jit(solution)/shard_map/ppermute | solution.py:82
  122.7 43.3 %collective-permute-start.12 = (bf16[328,1024]{1,0:T(8,128)(2,1)}, bf16[328,1024]{1,0:T(8,128)(2,1)S(1)}, u32[]{:S(2)}, u32[]{:S(2)}) collective-permute-start(bf16[328,1024]{1,0:T(8,128)(2,1)} %collective-permute-done.1), channel_id=1, source_target_pairs={{0,2},{1,3},{2,4},{3,5},{4,6},{5,7},{6,8},{7,9},{8,10},{9,11},{10,... | collective-permute-start | bytes 2015240 | tf_op jit(solution)/shard_map/ppermute | solution.py:82
  125.4 34.5 %collective-permute-start.14 = (bf16[96,2048]{1,0:T(8,128)(2,1)S(1)}, bf16[96,2048]{1,0:T(8,128)(2,1)S(1)}, u32[]{:S(2)}, u32[]{:S(2)}) collective-permute-start(bf16[96,2048]{1,0:T(8,128)(2,1)S(1)} %slice.834), channel_id=1, source_target_pairs={{0,2},{1,3},{2,4},{3,5},{4,6},{5,7},{6,8},{7,9},{8,10},{9,11},{10,... | collective-permute-start | bytes 1179656 | tf_op jit(solution)/shard_map/ppermute | solution.py:82
  129.3 32.4 %collective-permute-start.17 = (bf16[96,2048]{1,0:T(8,128)(2,1)S(1)}, bf16[96,2048]{1,0:T(8,128)(2,1)S(1)}, u32[]{:S(2)}, u32[]{:S(2)}) collective-permute-start(bf16[96,2048]{1,0:T(8,128)(2,1)S(1)} %slice.836), channel_id=1, source_target_pairs={{0,30},{1,31},{2,0},{3,1},{4,2},{5,3},{6,4},{7,5},{8,6},{9,7},{10,... | collective-permute-start | bytes 1179656 | tf_op jit(solution)/shard_map/ppermute | solution.py:82
  161.6 36.4 %collective-permute-start.20 = (bf16[40,2048]{1,0:T(8,128)(2,1)S(1)}, bf16[40,2048]{1,0:T(8,128)(2,1)S(1)}, u32[]{:S(2)}, u32[]{:S(2)}) collective-permute-start(bf16[40,2048]{1,0:T(8,128)(2,1)S(1)} %slice.838), channel_id=1, source_target_pairs={{0,2},{1,3},{2,4},{3,5},{4,6},{5,7},{6,8},{7,9},{8,10},{9,11},{10,... | collective-permute-start | bytes 491528 | tf_op jit(solution)/shard_map/ppermute | solution.py:82
  162.1 52.3 %collective-permute-start.23 = (bf16[40,2048]{1,0:T(8,128)(2,1)S(1)}, bf16[40,2048]{1,0:T(8,128)(2,1)S(1)}, u32[]{:S(2)}, u32[]{:S(2)}) collective-permute-start(bf16[40,2048]{1,0:T(8,128)(2,1)S(1)} %slice.840), channel_id=1, source_target_pairs={{0,30},{1,31},{2,0},{3,1},{4,2},{5,3},{6,4},{7,5},{8,6},{9,7},{10,... | collective-permute-start | bytes 491528 | tf_op jit(solution)/shard_map/ppermute | solution.py:82
  165.4 32.9 %collective-permute-start.22 = (bf16[328,1024]{1,0:T(8,128)(2,1)S(1)}, bf16[328,1024]{1,0:T(8,128)(2,1)S(1)}, u32[]{:S(2)}, u32[]{:S(2)}) collective-permute-start(bf16[328,1024]{1,0:T(8,128)(2,1)S(1)} %collective-permute-done.16), channel_id=1, source_target_pairs={{0,30},{1,31},{2,0},{3,1},{4,2},{5,3},{6,4},{7,5},{8,6},{9,7},{10,... | collective-permute-start | bytes 2015240 | tf_op jit(solution)/shard_map/ppermute | solution.py:82
  185.3 25.0 %collective-permute-start.21 = (bf16[328,1024]{1,0:T(8,128)(2,1)S(1)}, bf16[328,1024]{1,0:T(8,128)(2,1)S(1)}, u32[]{:S(2)}, u32[]{:S(2)}) collective-permute-start(bf16[328,1024]{1,0:T(8,128)(2,1)S(1)} %collective-permute-done.15), channel_id=1, source_target_pairs={{0,30},{1,31},{2,0},{3,1},{4,2},{5,3},{6,4},{7,5},{8,6},{9,7},{10,... | collective-permute-start | bytes 2015240 | tf_op jit(solution)/shard_map/ppermute | solution.py:82
  197.0 45.2 %collective-permute-start.35 = (bf16[328,1024]{1,0:T(8,128)(2,1)S(1)}, bf16[328,1024]{1,0:T(8,128)(2,1)S(1)}, u32[]{:S(2)}, u32[]{:S(2)}) collective-permute-start(bf16[328,1024]{1,0:T(8,128)(2,1)S(1)} %collective-permute-done.19), channel_id=1, source_target_pairs={{0,2},{1,3},{2,4},{3,5},{4,6},{5,7},{6,8},{7,9},{8,10},{9,11},{10,... | collective-permute-start | bytes 2015240 | tf_op jit(solution)/shard_map/ppermute | solution.py:82
  198.0 44.4 %collective-permute-start.34 = (bf16[328,1024]{1,0:T(8,128)(2,1)S(1)}, bf16[328,1024]{1,0:T(8,128)(2,1)S(1)}, u32[]{:S(2)}, u32[]{:S(2)}) collective-permute-start(bf16[328,1024]{1,0:T(8,128)(2,1)S(1)} %collective-permute-done.18), channel_id=1, source_target_pairs={{0,2},{1,3},{2,4},{3,5},{4,6},{5,7},{6,8},{7,9},{8,10},{9,11},{10,... | collective-permute-start | bytes 2015240 | tf_op jit(solution)/shard_map/ppermute | solution.py:82
  198.3 26.5 %collective-permute-start.37 = (bf16[328,1024]{1,0:T(8,128)(2,1)S(1)}, bf16[328,1024]{1,0:T(8,128)(2,1)S(1)}, u32[]{:S(2)}, u32[]{:S(2)}) collective-permute-start(bf16[328,1024]{1,0:T(8,128)(2,1)S(1)} %collective-permute-done.22), channel_id=1, source_target_pairs={{0,30},{1,31},{2,0},{3,1},{4,2},{5,3},{6,4},{7,5},{8,6},{9,7},{10,... | collective-permute-start | bytes 2015240 | tf_op jit(solution)/shard_map/ppermute | solution.py:82
  210.3 28.8 %collective-permute-start.36 = (bf16[328,1024]{1,0:T(8,128)(2,1)S(1)}, bf16[328,1024]{1,0:T(8,128)(2,1)S(1)}, u32[]{:S(2)}, u32[]{:S(2)}) collective-permute-start(bf16[328,1024]{1,0:T(8,128)(2,1)S(1)} %collective-permute-done.21), channel_id=1, source_target_pairs={{0,30},{1,31},{2,0},{3,1},{4,2},{5,3},{6,4},{7,5},{8,6},{9,7},{10,... | collective-permute-start | bytes 2015240 | tf_op jit(solution)/shard_map/ppermute | solution.py:82
  214.7 73.5 %collective-permute-start.24 = (bf16[432,2048]{1,0:T(8,128)(2,1)S(1)}, bf16[432,2048]{1,0:T(8,128)(2,1)S(1)}, u32[]{:S(2)}, u32[]{:S(2)}) collective-permute-start(bf16[432,2048]{1,0:T(8,128)(2,1)S(1)} %get-tuple-element.102), channel_id=1, source_target_pairs={{0,1},{1,0},{2,3},{3,2},{4,5},{5,4},{6,7},{7,6},{8,9},{9,8},{10,11... | collective-permute-start | bytes 5308424 | tf_op jit(solution)/shard_map/ppermute | solution.py:155
  224.8 25.9 %collective-permute-start.41 = (bf16[264,1024]{1,0:T(8,128)(2,1)S(1)}, bf16[264,1024]{1,0:T(8,128)(2,1)S(1)}, u32[]{:S(2)}, u32[]{:S(2)}) collective-permute-start(bf16[264,1024]{1,0:T(8,128)(2,1)S(1)} %slice.882), channel_id=1, source_target_pairs={{0,30},{1,31},{2,0},{3,1},{4,2},{5,3},{6,4},{7,5},{8,6},{9,7},{10,... | collective-permute-start | bytes 1622024 | tf_op jit(solution)/shard_map/ppermute | solution.py:82
  242.4 23.4 %collective-permute-start.38 = (bf16[264,1024]{1,0:T(8,128)(2,1)S(1)}, bf16[264,1024]{1,0:T(8,128)(2,1)S(1)}, u32[]{:S(2)}, u32[]{:S(2)}) collective-permute-start(bf16[264,1024]{1,0:T(8,128)(2,1)S(1)} %slice.877), channel_id=1, source_target_pairs={{0,2},{1,3},{2,4},{3,5},{4,6},{5,7},{6,8},{7,9},{8,10},{9,11},{10,... | collective-permute-start | bytes 1622024 | tf_op jit(solution)/shard_map/ppermute | solution.py:82
  272.2 29.8 %collective-permute-start.49 = (bf16[144,1024]{1,0:T(8,128)(2,1)S(1)}, bf16[144,1024]{1,0:T(8,128)(2,1)S(1)}, u32[]{:S(2)}, u32[]{:S(2)}) collective-permute-start(bf16[144,1024]{1,0:T(8,128)(2,1)S(1)} %slice.898), channel_id=1, source_target_pairs={{0,30},{1,31},{2,0},{3,1},{4,2},{5,3},{6,4},{7,5},{8,6},{9,7},{10,... | collective-permute-start | bytes 884744 | tf_op jit(solution)/shard_map/ppermute | solution.py:82
  282.0 23.3 %collective-permute-start.48 = (bf16[144,1024]{1,0:T(8,128)(2,1)S(1)}, bf16[144,1024]{1,0:T(8,128)(2,1)S(1)}, u32[]{:S(2)}, u32[]{:S(2)}) collective-permute-start(bf16[144,1024]{1,0:T(8,128)(2,1)S(1)} %slice.897), channel_id=1, source_target_pairs={{0,30},{1,31},{2,0},{3,1},{4,2},{5,3},{6,4},{7,5},{8,6},{9,7},{10,... | collective-permute-start | bytes 884744 | tf_op jit(solution)/shard_map/ppermute | solution.py:82
  327.5 23.2 %collective-permute-start.30 = (bf16[40,2048]{1,0:T(8,128)(2,1)S(1)}, bf16[40,2048]{1,0:T(8,128)(2,1)S(1)}, u32[]{:S(2)}, u32[]{:S(2)}) collective-permute-start(bf16[40,2048]{1,0:T(8,128)(2,1)S(1)} %convolution_convert_fusion.15), channel_id=1, source_target_pairs={{0,30},{1,31},{2,0},{3,1},{4,2},{5,3},{6,4},{7,5},{8,6},{9,7},{10,... | collective-permute-start | bytes 491528 | tf_op jit(solution)/shard_map/ppermute | solution.py:82
  350.6 34.7 %collective-permute-start.55 = (bf16[480,2048]{1,0:T(8,128)(2,1)S(1)}, bf16[480,2048]{1,0:T(8,128)(2,1)S(1)}, u32[]{:S(2)}, u32[]{:S(2)}) collective-permute-start(bf16[480,2048]{1,0:T(8,128)(2,1)S(1)} %slice.910), channel_id=1, source_target_pairs={{0,1},{1,0},{2,3},{3,2},{4,5},{5,4},{6,7},{7,6},{8,9},{9,8},{10,11... | collective-permute-start | bytes 5898248 | tf_op jit(solution)/shard_map/ppermute | solution.py:157
  373.8 130.3 %collective-permute-start.29 = (bf16[200,2048]{1,0:T(8,128)(2,1)S(1)}, bf16[200,2048]{1,0:T(8,128)(2,1)S(1)}, u32[]{:S(2)}, u32[]{:S(2)}) collective-permute-start(bf16[200,2048]{1,0:T(8,128)(2,1)S(1)} %fusion.43), channel_id=1, source_target_pairs={{0,2},{1,3},{2,4},{3,5},{4,6},{5,7},{6,8},{7,9},{8,10},{9,11},{10,... | collective-permute-start | bytes 2457608 | tf_op jit(solution)/shard_map/ppermute | solution.py:82
  381.5 126.1 %collective-permute-start.33 = (bf16[200,2048]{1,0:T(8,128)(2,1)S(1)}, bf16[200,2048]{1,0:T(8,128)(2,1)S(1)}, u32[]{:S(2)}, u32[]{:S(2)}) collective-permute-start(bf16[200,2048]{1,0:T(8,128)(2,1)S(1)} %fusion.44), channel_id=1, source_target_pairs={{0,30},{1,31},{2,0},{3,1},{4,2},{5,3},{6,4},{7,5},{8,6},{9,7},{10,... | collective-permute-start | bytes 2457608 | tf_op jit(solution)/shard_map/ppermute | solution.py:82
  406.7 25.8 %collective-permute-start.84 = (bf16[144,1024]{1,0:T(8,128)(2,1)S(1)}, bf16[144,1024]{1,0:T(8,128)(2,1)S(1)}, u32[]{:S(2)}, u32[]{:S(2)}) collective-permute-start(bf16[144,1024]{1,0:T(8,128)(2,1)S(1)} %fusion.86), channel_id=1, source_target_pairs={{0,2},{1,3},{2,4},{3,5},{4,6},{5,7},{6,8},{7,9},{8,10},{9,11},{10,... | collective-permute-start | bytes 884744 | tf_op jit(solution)/shard_map/ppermute | solution.py:82
  471.3 25.5 %collective-permute-start.78 = (bf16[328,1024]{1,0:T(8,128)(2,1)S(1)}, bf16[328,1024]{1,0:T(8,128)(2,1)S(1)}, u32[]{:S(2)}, u32[]{:S(2)}) collective-permute-start(bf16[328,1024]{1,0:T(8,128)(2,1)S(1)} %fusion.69), channel_id=1, source_target_pairs={{0,30},{1,31},{2,0},{3,1},{4,2},{5,3},{6,4},{7,5},{8,6},{9,7},{10,... | collective-permute-start | bytes 2015240 | tf_op jit(solution)/shard_map/ppermute | solution.py:82
  473.3 27.7 %collective-permute-start.69 = (bf16[328,1024]{1,0:T(8,128)(2,1)S(1)}, bf16[328,1024]{1,0:T(8,128)(2,1)S(1)}, u32[]{:S(2)}, u32[]{:S(2)}) collective-permute-start(bf16[328,1024]{1,0:T(8,128)(2,1)S(1)} %fusion.64), channel_id=1, source_target_pairs={{0,2},{1,3},{2,4},{3,5},{4,6},{5,7},{6,8},{7,9},{8,10},{9,11},{10,... | collective-permute-start | bytes 2015240 | tf_op jit(solution)/shard_map/ppermute | solution.py:82
  500.9 29.4 %collective-permute-start.79 = (bf16[328,1024]{1,0:T(8,128)(2,1)S(1)}, bf16[328,1024]{1,0:T(8,128)(2,1)S(1)}, u32[]{:S(2)}, u32[]{:S(2)}) collective-permute-start(bf16[328,1024]{1,0:T(8,128)(2,1)S(1)} %fusion.68), channel_id=1, source_target_pairs={{0,30},{1,31},{2,0},{3,1},{4,2},{5,3},{6,4},{7,5},{8,6},{9,7},{10,... | collective-permute-start | bytes 2015240 | tf_op jit(solution)/shard_map/ppermute | solution.py:82
  503.0 31.6 %collective-permute-start.70 = (bf16[328,1024]{1,0:T(8,128)(2,1)S(1)}, bf16[328,1024]{1,0:T(8,128)(2,1)S(1)}, u32[]{:S(2)}, u32[]{:S(2)}) collective-permute-start(bf16[328,1024]{1,0:T(8,128)(2,1)S(1)} %fusion.63), channel_id=1, source_target_pairs={{0,2},{1,3},{2,4},{3,5},{4,6},{5,7},{6,8},{7,9},{8,10},{9,11},{10,... | collective-permute-start | bytes 2015240 | tf_op jit(solution)/shard_map/ppermute | solution.py:82
  504.1 31.1 %collective-permute-start.88 = (bf16[328,1024]{1,0:T(8,128)(2,1)S(1)}, bf16[328,1024]{1,0:T(8,128)(2,1)S(1)}, u32[]{:S(2)}, u32[]{:S(2)}) collective-permute-start(bf16[328,1024]{1,0:T(8,128)(2,1)S(1)} %fusion.73), channel_id=1, source_target_pairs={{0,2},{1,3},{2,4},{3,5},{4,6},{5,7},{6,8},{7,9},{8,10},{9,11},{10,... | collective-permute-start | bytes 2015240 | tf_op jit(solution)/shard_map/ppermute | solution.py:82
  516.4 42.5 %collective-permute-start.62 = (bf16[328,1024]{1,0:T(8,128)(2,1)S(1)}, bf16[328,1024]{1,0:T(8,128)(2,1)S(1)}, u32[]{:S(2)}, u32[]{:S(2)}) collective-permute-start(bf16[328,1024]{1,0:T(8,128)(2,1)S(1)} %fusion.59), channel_id=1, source_target_pairs={{0,30},{1,31},{2,0},{3,1},{4,2},{5,3},{6,4},{7,5},{8,6},{9,7},{10,... | collective-permute-start | bytes 2015240 | tf_op jit(solution)/shard_map/ppermute | solution.py:82
  530.8 23.9 %collective-permute-start.80 = (bf16[328,1024]{1,0:T(8,128)(2,1)S(1)}, bf16[328,1024]{1,0:T(8,128)(2,1)S(1)}, u32[]{:S(2)}, u32[]{:S(2)}) collective-permute-start(bf16[328,1024]{1,0:T(8,128)(2,1)S(1)} %fusion.67), channel_id=1, source_target_pairs={{0,30},{1,31},{2,0},{3,1},{4,2},{5,3},{6,4},{7,5},{8,6},{9,7},{10,... | collective-permute-start | bytes 2015240 | tf_op jit(solution)/shard_map/ppermute | solution.py:82
  535.1 27.0 %collective-permute-start.71 = (bf16[328,1024]{1,0:T(8,128)(2,1)S(1)}, bf16[328,1024]{1,0:T(8,128)(2,1)S(1)}, u32[]{:S(2)}, u32[]{:S(2)}) collective-permute-start(bf16[328,1024]{1,0:T(8,128)(2,1)S(1)} %fusion.62), channel_id=1, source_target_pairs={{0,2},{1,3},{2,4},{3,5},{4,6},{5,7},{6,8},{7,9},{8,10},{9,11},{10,... | collective-permute-start | bytes 2015240 | tf_op jit(solution)/shard_map/ppermute | solution.py:82
  535.7 25.3 %collective-permute-start.89 = (bf16[328,1024]{1,0:T(8,128)(2,1)S(1)}, bf16[328,1024]{1,0:T(8,128)(2,1)S(1)}, u32[]{:S(2)}, u32[]{:S(2)}) collective-permute-start(bf16[328,1024]{1,0:T(8,128)(2,1)S(1)} %fusion.72), channel_id=1, source_target_pairs={{0,2},{1,3},{2,4},{3,5},{4,6},{5,7},{6,8},{7,9},{8,10},{9,11},{10,... | collective-permute-start | bytes 2015240 | tf_op jit(solution)/shard_map/ppermute | solution.py:82
  559.4 29.4 %collective-permute-start.63 = (bf16[328,1024]{1,0:T(8,128)(2,1)S(1)}, bf16[328,1024]{1,0:T(8,128)(2,1)S(1)}, u32[]{:S(2)}, u32[]{:S(2)}) collective-permute-start(bf16[328,1024]{1,0:T(8,128)(2,1)S(1)} %fusion.58), channel_id=1, source_target_pairs={{0,30},{1,31},{2,0},{3,1},{4,2},{5,3},{6,4},{7,5},{8,6},{9,7},{10,... | collective-permute-start | bytes 2015240 | tf_op jit(solution)/shard_map/ppermute | solution.py:82
  561.4 31.6 %collective-permute-start.90 = (bf16[328,1024]{1,0:T(8,128)(2,1)S(1)}, bf16[328,1024]{1,0:T(8,128)(2,1)S(1)}, u32[]{:S(2)}, u32[]{:S(2)}) collective-permute-start(bf16[328,1024]{1,0:T(8,128)(2,1)S(1)} %fusion.71), channel_id=1, source_target_pairs={{0,2},{1,3},{2,4},{3,5},{4,6},{5,7},{6,8},{7,9},{8,10},{9,11},{10,... | collective-permute-start | bytes 2015240 | tf_op jit(solution)/shard_map/ppermute | solution.py:82
  562.5 31.1 %collective-permute-start.72 = (bf16[328,1024]{1,0:T(8,128)(2,1)S(1)}, bf16[328,1024]{1,0:T(8,128)(2,1)S(1)}, u32[]{:S(2)}, u32[]{:S(2)}) collective-permute-start(bf16[328,1024]{1,0:T(8,128)(2,1)S(1)} %fusion.61), channel_id=1, source_target_pairs={{0,2},{1,3},{2,4},{3,5},{4,6},{5,7},{6,8},{7,9},{8,10},{9,11},{10,... | collective-permute-start | bytes 2015240 | tf_op jit(solution)/shard_map/ppermute | solution.py:82
  574.8 28.0 %collective-permute-start.82 = (bf16[328,1024]{1,0:T(8,128)(2,1)S(1)}, bf16[328,1024]{1,0:T(8,128)(2,1)S(1)}, u32[]{:S(2)}, u32[]{:S(2)}) collective-permute-start(bf16[328,1024]{1,0:T(8,128)(2,1)S(1)} %fusion.65), channel_id=1, source_target_pairs={{0,30},{1,31},{2,0},{3,1},{4,2},{5,3},{6,4},{7,5},{8,6},{9,7},{10,... | collective-permute-start | bytes 2015240 | tf_op jit(solution)/shard_map/ppermute | solution.py:82
  (121 other events, 4027.8 us)

commit v5 on v4

--- a/solution.py
+++ b/solution.py
@@ -107,13 +107,15 @@
 
     normed = rms_norm(tokens, norm_gain)
     weights = route_gates / jnp.sum(route_gates, axis=1, keepdims=True)
-    first = lambda way, low, high: dot(pick_of(places[way] - low, high - low), normed).astype(BF16)
+
+    def first(way, low, high, span=slice(None)):
+        return dot(pick_of(places[way] - low, high - low), normed[:, span]).astype(BF16)
+
     near_block = {way: first(way, fixed, HOPS[0]) for way in WAYS}
     far_block = {}
     for way in WAYS:
-        block = first(way, 0, fixed)
-        for part in range(PARTS):
-            far_block[way, part] = block[:, columns[part]]
+        for part in range(PARTS):
+            far_block[way, part] = first(way, 0, fixed, columns[part])
     here = first(0, 0, 2 * capacity)
 
     far_at, near_at = {}, {}

time: 628 us -> 625 us (level)
  waiting for transfers between devices: 340 us -> 328 us
  starting transfers between devices: 152 us -> 159 us
    ppermute x88, waiting for transfers between devices: 340 us -> 328 us  [body(): hop = lambda block, way: lax.ppermute(block, 'ep', step[way])]
    ppermute x88, starting transfers between devices: 134 us -> 141 us  [body(): hop = lambda block, way: lax.ppermute(block, 'ep', step[way])]
    dot_general x107 -> x109, matrix products: 79.4 us -> 83.3 us  [dot(): return jnp.dot(a, b, preferred_element_type=F32)]
where the time goes in v5:
time: 625 us; the launch traced here: 617 us
  waiting for transfers between devices  328 us (52%)
  starting transfers between devices  159 us (25%)
  matrix products  85.2 us (14%)
  other arithmetic  20.4 us (3%)
  local copies, waits for them, and re-layouts  16.7 us (3%)
    ppermute x88, waiting for transfers between devices, body(): hop = lambda block, way: lax.ppermute(block, 'ep', step[way])  328 us
    ppermute x88, starting transfers between devices, body(): hop = lambda block, way: lax.ppermute(block, 'ep', step[way])  141 us
    dot_general x109, matrix products, dot(): return jnp.dot(a, b, preferred_element_type=F32)  83.3 us
    all_to_all x1, starting transfers between devices, body(): table = lax.all_to_all(row, 'ep', split_axis=0, concat_axis=0, tiled=True)  17.8 us
  transfers between devices with their start and end apart: 93, of which 50 were waited for; matrix products, arithmetic and copies ran while one was open for 18% of the time, Pallas kernels for 0%

profile of v5, /device:TPU:70, one launch (start us, length us, event | category | flops | bytes accessed | tf_op | source)
XLA Modules:
  0.0 616.6 jit_solution(11248507895239726674)
XLA Ops:
  5.7 17.8 %all-to-all-start.2 = ((f32[32,1,96]{2,1,0:T(1,128)}), f32[32,1,96]{2,1,0:T(1,128)S(1)}, u32[]{:S(2)}, u32[]{:S(2)}) async-start(f32[32,1,96]{2,1,0:T(1,128)} %broadcast_in_dim.145), calls=%async_computation.2 | async-start | bytes 32768 | tf_op jit(solution)/shard_map/all_to_all | solution.py:134
  51.3 12.8 %collective-permute-done.2 = bf16[328,1024]{1,0:T(8,128)(2,1)} collective-permute-done((bf16[328,1024]{1,0:T(8,128)(2,1)}, bf16[328,1024]{1,0:T(8,128)(2,1)}, u32[]{:S(2)}, u32[]{:S(2)}) %collective-permute-start.2) | collective-permute-done | bytes 671776 | tf_op jit(solution)/shard_map/ppermute | solution.py:82
  68.6 16.0 %collective-permute-done.4 = bf16[328,1024]{1,0:T(8,128)(2,1)} collective-permute-done((bf16[328,1024]{1,0:T(8,128)(2,1)}, bf16[328,1024]{1,0:T(8,128)(2,1)}, u32[]{:S(2)}, u32[]{:S(2)}) %collective-permute-start.4) | collective-permute-done | bytes 671776 | tf_op jit(solution)/shard_map/ppermute | solution.py:82
  125.0 6.2 collective-permute-done.11
  136.7 23.2 %collective-permute-done.14 = bf16[96,2048]{1,0:T(8,128)(2,1)S(1)} collective-permute-done((bf16[96,2048]{1,0:T(8,128)(2,1)S(1)}, bf16[96,2048]{1,0:T(8,128)(2,1)S(1)}, u32[]{:S(2)}, u32[]{:S(2)}) %collective-permute-start.14) | collective-permute-done | bytes 393248 | tf_op jit(solution)/shard_map/ppermute | solution.py:82
  166.8 11.3 %collective-permute-done.15 = bf16[328,1024]{1,0:T(8,128)(2,1)S(1)} collective-permute-done((bf16[328,1024]{1,0:T(8,128)(2,1)}, bf16[328,1024]{1,0:T(8,128)(2,1)S(1)}, u32[]{:S(2)}, u32[]{:S(2)}) %collective-permute-start.15) | collective-permute-done | bytes 671776 | tf_op jit(solution)/shard_map/ppermute | solution.py:82
  185.0 12.0 %collective-permute-done.19 = bf16[328,1024]{1,0:T(8,128)(2,1)S(1)} collective-permute-done((bf16[328,1024]{1,0:T(8,128)(2,1)S(1)}, bf16[328,1024]{1,0:T(8,128)(2,1)S(1)}, u32[]{:S(2)}, u32[]{:S(2)}) %collective-permute-start.19) | collective-permute-done | bytes 671776 | tf_op jit(solution)/shard_map/ppermute | solution.py:82
  202.0 8.9 %collective-permute-done.21 = bf16[328,1024]{1,0:T(8,128)(2,1)S(1)} collective-permute-done((bf16[328,1024]{1,0:T(8,128)(2,1)S(1)}, bf16[328,1024]{1,0:T(8,128)(2,1)S(1)}, u32[]{:S(2)}, u32[]{:S(2)}) %collective-permute-start.21) | collective-permute-done | bytes 671776 | tf_op jit(solution)/shard_map/ppermute | solution.py:82
  216.4 14.2 %collective-permute-done.35 = bf16[328,1024]{1,0:T(8,128)(2,1)S(1)} collective-permute-done((bf16[328,1024]{1,0:T(8,128)(2,1)S(1)}, bf16[328,1024]{1,0:T(8,128)(2,1)S(1)}, u32[]{:S(2)}, u32[]{:S(2)}) %collective-permute-start.35) | collective-permute-done | bytes 671776 | tf_op jit(solution)/shard_map/ppermute | solution.py:82
  234.2 5.5 collective-permute-done.36
  239.7 3.8 collective-permute-start.40
  246.4 7.4 %collective-permute-done.39 = bf16[264,1024]{1,0:T(8,128)(2,1)S(1)} collective-permute-done((bf16[264,1024]{1,0:T(8,128)(2,1)S(1)}, bf16[264,1024]{1,0:T(8,128)(2,1)S(1)}, u32[]{:S(2)}, u32[]{:S(2)}) %collective-permute-start.39) | collective-permute-done | bytes 540704 | tf_op jit(solution)/shard_map/ppermute | solution.py:82
  257.3 5.5 collective-permute-done.40
  262.9 3.8 collective-permute-start.44
  269.6 3.9 collective-permute-done.43
  277.0 5.5 collective-permute-done.44
  282.5 4.0 collective-permute-start.48
  289.3 3.8 fusion.31
  293.2 3.8 fusion.35
  297.0 4.1 fusion.40
  327.6 4.2 collective-permute-done.26
  334.3 4.2 fusion.29
  338.6 4.3 fusion.33
  342.9 4.6 fusion.37
  352.9 7.3 %collective-permute-done.31 = bf16[96,2048]{1,0:T(8,128)(2,1)S(1)} collective-permute-done((bf16[96,2048]{1,0:T(8,128)(2,1)S(1)}, bf16[96,2048]{1,0:T(8,128)(2,1)S(1)}, u32[]{:S(2)}, u32[]{:S(2)}) %collective-permute-start.31) | collective-permute-done | bytes 393248 | tf_op jit(solution)/shard_map/ppermute | solution.py:82
  360.7 4.2 collective-permute-start.32
  365.1 5.0 collective-permute-done.28
  370.7 7.1 %collective-permute-done.32 = bf16[152,2048]{1,0:T(8,128)(2,1)S(1)} collective-permute-done((bf16[152,2048]{1,0:T(8,128)(2,1)S(1)}, bf16[152,2048]{1,0:T(8,128)(2,1)S(1)}, u32[]{:S(2)}, u32[]{:S(2)}) %collective-permute-start.32) | collective-permute-done | bytes 622624 | tf_op jit(solution)/shard_map/ppermute | solution.py:82
  378.3 3.8 collective-permute-start.33
  386.0 8.7 %collective-permute-done.83 = bf16[80,1024]{1,0:T(8,128)(2,1)S(1)} collective-permute-done((bf16[80,1024]{1,0:T(8,128)(2,1)S(1)}, bf16[80,1024]{1,0:T(8,128)(2,1)S(1)}, u32[]{:S(2)}, u32[]{:S(2)}) %collective-permute-start.83) | collective-permute-done | bytes 163872 | tf_op jit(solution)/shard_map/ppermute | solution.py:82
  395.0 8.6 %collective-permute-done.56 = bf16[80,1024]{1,0:T(8,128)(2,1)S(1)} collective-permute-done((bf16[80,1024]{1,0:T(8,128)(2,1)S(1)}, bf16[80,1024]{1,0:T(8,128)(2,1)S(1)}, u32[]{:S(2)}, u32[]{:S(2)}) %collective-permute-start.56) | collective-permute-done | bytes 163872 | tf_op jit(solution)/shard_map/ppermute | solution.py:82
  410.6 5.7 collective-permute-done.57
  424.8 4.1 collective-permute-start.76
  429.8 4.3 collective-permute-done.58
  434.5 5.5 collective-permute-done.76
  447.2 9.1 %collective-permute-done.59 = bf16[264,1024]{1,0:T(8,128)(2,1)S(1)} collective-permute-done((bf16[264,1024]{1,0:T(8,128)(2,1)S(1)}, bf16[264,1024]{1,0:T(8,128)(2,1)S(1)}, u32[]{:S(2)}, u32[]{:S(2)}) %collective-permute-start.59) | collective-permute-done | bytes 540704 | tf_op jit(solution)/shard_map/ppermute | solution.py:82
  456.8 7.0 %collective-permute-done.77 = bf16[264,1024]{1,0:T(8,128)(2,1)S(1)} collective-permute-done((bf16[264,1024]{1,0:T(8,128)(2,1)S(1)}, bf16[264,1024]{1,0:T(8,128)(2,1)S(1)}, u32[]{:S(2)}, u32[]{:S(2)}) %collective-permute-start.77) | collective-permute-done | bytes 540704 | tf_op jit(solution)/shard_map/ppermute | solution.py:82
  463.9 3.9 collective-permute-start.60
  471.4 11.9 %collective-permute-done.60 = bf16[328,1024]{1,0:T(8,128)(2,1)S(1)} collective-permute-done((bf16[328,1024]{1,0:T(8,128)(2,1)S(1)}, bf16[328,1024]{1,0:T(8,128)(2,1)S(1)}, u32[]{:S(2)}, u32[]{:S(2)}) %collective-permute-start.60) | collective-permute-done | bytes 671776 | tf_op jit(solution)/shard_map/ppermute | solution.py:82
  483.7 10.0 %collective-permute-done.78 = bf16[328,1024]{1,0:T(8,128)(2,1)S(1)} collective-permute-done((bf16[328,1024]{1,0:T(8,128)(2,1)S(1)}, bf16[328,1024]{1,0:T(8,128)(2,1)S(1)}, u32[]{:S(2)}, u32[]{:S(2)}) %collective-permute-start.78) | collective-permute-done | bytes 671776 | tf_op jit(solution)/shard_map/ppermute | solution.py:82
  504.6 8.3 %collective-permute-done.61 = bf16[328,1024]{1,0:T(8,128)(2,1)S(1)} collective-permute-done((bf16[328,1024]{1,0:T(8,128)(2,1)S(1)}, bf16[328,1024]{1,0:T(8,128)(2,1)S(1)}, u32[]{:S(2)}, u32[]{:S(2)}) %collective-permute-start.61) | collective-permute-done | bytes 671776 | tf_op jit(solution)/shard_map/ppermute | solution.py:82
  517.1 10.1 %collective-permute-done.79 = bf16[328,1024]{1,0:T(8,128)(2,1)S(1)} collective-permute-done((bf16[328,1024]{1,0:T(8,128)(2,1)S(1)}, bf16[328,1024]{1,0:T(8,128)(2,1)S(1)}, u32[]{:S(2)}, u32[]{:S(2)}) %collective-permute-start.79) | collective-permute-done | bytes 671776 | tf_op jit(solution)/shard_map/ppermute | solution.py:82
  534.6 16.9 %collective-permute-done.80 = bf16[328,1024]{1,0:T(8,128)(2,1)S(1)} collective-permute-done((bf16[328,1024]{1,0:T(8,128)(2,1)S(1)}, bf16[328,1024]{1,0:T(8,128)(2,1)S(1)}, u32[]{:S(2)}, u32[]{:S(2)}) %collective-permute-start.80) | collective-permute-done | bytes 671776 | tf_op jit(solution)/shard_map/ppermute | solution.py:82
  562.3 9.0 %collective-permute-done.81 = bf16[328,1024]{1,0:T(8,128)(2,1)S(1)} collective-permute-done((bf16[328,1024]{1,0:T(8,128)(2,1)S(1)}, bf16[328,1024]{1,0:T(8,128)(2,1)S(1)}, u32[]{:S(2)}, u32[]{:S(2)}) %collective-permute-start.81) | collective-permute-done | bytes 671776 | tf_op jit(solution)/shard_map/ppermute | solution.py:82
  575.6 10.1 %collective-permute-done.63 = bf16[328,1024]{1,0:T(8,128)(2,1)S(1)} collective-permute-done((bf16[328,1024]{1,0:T(8,128)(2,1)S(1)}, bf16[328,1024]{1,0:T(8,128)(2,1)S(1)}, u32[]{:S(2)}, u32[]{:S(2)}) %collective-permute-start.63) | collective-permute-done | bytes 671776 | tf_op jit(solution)/shard_map/ppermute | solution.py:82
  586.1 3.8 collective-permute-start.64
  591.3 8.5 %collective-permute-done.82 = bf16[328,1024]{1,0:T(8,128)(2,1)S(1)} collective-permute-done((bf16[328,1024]{1,0:T(8,128)(2,1)S(1)}, bf16[328,1024]{1,0:T(8,128)(2,1)S(1)}, u32[]{:S(2)}, u32[]{:S(2)}) %collective-permute-start.82) | collective-permute-done | bytes 671776 | tf_op jit(solution)/shard_map/ppermute | solution.py:82
  600.7 6.3 %collective-permute-done.64 = bf16[328,1024]{1,0:T(8,128)(2,1)S(1)} collective-permute-done((bf16[328,1024]{1,0:T(8,128)(2,1)S(1)}, bf16[328,1024]{1,0:T(8,128)(2,1)S(1)}, u32[]{:S(2)}, u32[]{:S(2)}) %collective-permute-start.64) | collective-permute-done | bytes 671776 | tf_op jit(solution)/shard_map/ppermute | solution.py:82
  (486 shorter events, 240.5 us)
Async XLA Ops:
  5.7 92.2 %all-to-all-start.2 = ((f32[32,1,96]{2,1,0:T(1,128)}), f32[32,1,96]{2,1,0:T(1,128)S(1)}, u32[]{:S(2)}, u32[]{:S(2)}) async-start(f32[32,1,96]{2,1,0:T(1,128)} %broadcast_in_dim.145), calls=%async_computation.2 | async-start | bytes 32768 | tf_op jit(solution)/shard_map/all_to_all | solution.py:134
  32.9 31.2 %collective-permute-start.2 = (bf16[328,1024]{1,0:T(8,128)(2,1)}, bf16[328,1024]{1,0:T(8,128)(2,1)}, u32[]{:S(2)}, u32[]{:S(2)}) collective-permute-start(bf16[328,1024]{1,0:T(8,128)(2,1)} %convolution_convert_fusion.37), channel_id=1, source_target_pairs={{0,2},{1,3},{2,4},{3,5},{4,6},{5,7},{6,8},{7,9},{8,10},{9,11},{10,... | collective-permute-start | bytes 2015240 | tf_op jit(solution)/shard_map/ppermute | solution.py:82
  35.9 31.3 %collective-permute-start.5 = (bf16[328,1024]{1,0:T(8,128)(2,1)}, bf16[328,1024]{1,0:T(8,128)(2,1)}, u32[]{:S(2)}, u32[]{:S(2)}) collective-permute-start(bf16[328,1024]{1,0:T(8,128)(2,1)} %convolution_convert_fusion.35), channel_id=1, source_target_pairs={{0,30},{1,31},{2,0},{3,1},{4,2},{5,3},{6,4},{7,5},{8,6},{9,7},{10,... | collective-permute-start | bytes 2015240 | tf_op jit(solution)/shard_map/ppermute | solution.py:82
  39.1 48.5 %collective-permute-start.3 = (bf16[200,2048]{1,0:T(8,128)(2,1)}, bf16[200,2048]{1,0:T(8,128)(2,1)S(1)}, u32[]{:S(2)}, u32[]{:S(2)}) collective-permute-start(bf16[200,2048]{1,0:T(8,128)(2,1)} %convolution_convert_fusion.7), channel_id=1, source_target_pairs={{0,2},{1,3},{2,4},{3,5},{4,6},{5,7},{6,8},{7,9},{8,10},{9,11},{10,... | collective-permute-start | bytes 2457608 | tf_op jit(solution)/shard_map/ppermute | solution.py:82
  41.0 47.6 %collective-permute-start.6 = (bf16[200,2048]{1,0:T(8,128)(2,1)}, bf16[200,2048]{1,0:T(8,128)(2,1)}, u32[]{:S(2)}, u32[]{:S(2)}) collective-permute-start(bf16[200,2048]{1,0:T(8,128)(2,1)} %convolution_convert_fusion.6), channel_id=1, source_target_pairs={{0,30},{1,31},{2,0},{3,1},{4,2},{5,3},{6,4},{7,5},{8,6},{9,7},{10,... | collective-permute-start | bytes 2457608 | tf_op jit(solution)/shard_map/ppermute | solution.py:82
  49.7 35.0 %collective-permute-start.4 = (bf16[328,1024]{1,0:T(8,128)(2,1)}, bf16[328,1024]{1,0:T(8,128)(2,1)}, u32[]{:S(2)}, u32[]{:S(2)}) collective-permute-start(bf16[328,1024]{1,0:T(8,128)(2,1)} %convolution_convert_fusion.36), channel_id=1, source_target_pairs={{0,30},{1,31},{2,0},{3,1},{4,2},{5,3},{6,4},{7,5},{8,6},{9,7},{10,... | collective-permute-start | bytes 2015240 | tf_op jit(solution)/shard_map/ppermute | solution.py:82
  64.1 31.9 %collective-permute-start.1 = (bf16[328,1024]{1,0:T(8,128)(2,1)}, bf16[328,1024]{1,0:T(8,128)(2,1)}, u32[]{:S(2)}, u32[]{:S(2)}) collective-permute-start(bf16[328,1024]{1,0:T(8,128)(2,1)} %collective-permute-done), channel_id=1, source_target_pairs={{0,2},{1,3},{2,4},{3,5},{4,6},{5,7},{6,8},{7,9},{8,10},{9,11},{10,... | collective-permute-start | bytes 2015240 | tf_op jit(solution)/shard_map/ppermute | solution.py:82
  67.2 43.3 %collective-permute-start.7 = (bf16[328,1024]{1,0:T(8,128)(2,1)}, bf16[328,1024]{1,0:T(8,128)(2,1)}, u32[]{:S(2)}, u32[]{:S(2)}) collective-permute-start(bf16[328,1024]{1,0:T(8,128)(2,1)} %collective-permute-done.2), channel_id=1, source_target_pairs={{0,2},{1,3},{2,4},{3,5},{4,6},{5,7},{6,8},{7,9},{8,10},{9,11},{10,... | collective-permute-start | bytes 2015240 | tf_op jit(solution)/shard_map/ppermute | solution.py:82
  84.7 29.2 %collective-permute-start.10 = (bf16[328,1024]{1,0:T(8,128)(2,1)}, bf16[328,1024]{1,0:T(8,128)(2,1)}, u32[]{:S(2)}, u32[]{:S(2)}) collective-permute-start(bf16[328,1024]{1,0:T(8,128)(2,1)} %collective-permute-done.5), channel_id=1, source_target_pairs={{0,30},{1,31},{2,0},{3,1},{4,2},{5,3},{6,4},{7,5},{8,6},{9,7},{10,... | collective-permute-start | bytes 2015240 | tf_op jit(solution)/shard_map/ppermute | solution.py:82
  87.7 30.2 %collective-permute-start.9 = (bf16[328,1024]{1,0:T(8,128)(2,1)}, bf16[328,1024]{1,0:T(8,128)(2,1)}, u32[]{:S(2)}, u32[]{:S(2)}) collective-permute-start(bf16[328,1024]{1,0:T(8,128)(2,1)} %collective-permute-done.4), channel_id=1, source_target_pairs={{0,30},{1,31},{2,0},{3,1},{4,2},{5,3},{6,4},{7,5},{8,6},{9,7},{10,... | collective-permute-start | bytes 2015240 | tf_op jit(solution)/shard_map/ppermute | solution.py:82
  88.5 35.2 %collective-permute-start.8 = (bf16[152,2048]{1,0:T(8,128)(2,1)}, bf16[152,2048]{1,0:T(8,128)(2,1)}, u32[]{:S(2)}, u32[]{:S(2)}) collective-permute-start(bf16[152,2048]{1,0:T(8,128)(2,1)} %slice.826), channel_id=1, source_target_pairs={{0,2},{1,3},{2,4},{3,5},{4,6},{5,7},{6,8},{7,9},{8,10},{9,11},{10,... | collective-permute-start | bytes 1867784 | tf_op jit(solution)/shard_map/ppermute | solution.py:82
  96.0 35.1 %collective-permute-start.11 = (bf16[152,2048]{1,0:T(8,128)(2,1)}, bf16[152,2048]{1,0:T(8,128)(2,1)S(1)}, u32[]{:S(2)}, u32[]{:S(2)}) collective-permute-start(bf16[152,2048]{1,0:T(8,128)(2,1)} %slice.828), channel_id=1, source_target_pairs={{0,30},{1,31},{2,0},{3,1},{4,2},{5,3},{6,4},{7,5},{8,6},{9,7},{10,... | collective-permute-start | bytes 1867784 | tf_op jit(solution)/shard_map/ppermute | solution.py:82
  110.4 51.6 %collective-permute-start.12 = (bf16[328,1024]{1,0:T(8,128)(2,1)}, bf16[328,1024]{1,0:T(8,128)(2,1)S(1)}, u32[]{:S(2)}, u32[]{:S(2)}) collective-permute-start(bf16[328,1024]{1,0:T(8,128)(2,1)} %collective-permute-done.1), channel_id=1, source_target_pairs={{0,2},{1,3},{2,4},{3,5},{4,6},{5,7},{6,8},{7,9},{8,10},{9,11},{10,... | collective-permute-start | bytes 2015240 | tf_op jit(solution)/shard_map/ppermute | solution.py:82
  113.8 51.6 %collective-permute-start.13 = (bf16[328,1024]{1,0:T(8,128)(2,1)}, bf16[328,1024]{1,0:T(8,128)(2,1)S(1)}, u32[]{:S(2)}, u32[]{:S(2)}) collective-permute-start(bf16[328,1024]{1,0:T(8,128)(2,1)} %collective-permute-done.7), channel_id=1, source_target_pairs={{0,2},{1,3},{2,4},{3,5},{4,6},{5,7},{6,8},{7,9},{8,10},{9,11},{10,... | collective-permute-start | bytes 2015240 | tf_op jit(solution)/shard_map/ppermute | solution.py:82
  117.8 48.1 %collective-permute-start.16 = (bf16[328,1024]{1,0:T(8,128)(2,1)}, bf16[328,1024]{1,0:T(8,128)(2,1)S(1)}, u32[]{:S(2)}, u32[]{:S(2)}) collective-permute-start(bf16[328,1024]{1,0:T(8,128)(2,1)} %collective-permute-done.10), channel_id=1, source_target_pairs={{0,30},{1,31},{2,0},{3,1},{4,2},{5,3},{6,4},{7,5},{8,6},{9,7},{10,... | collective-permute-start | bytes 2015240 | tf_op jit(solution)/shard_map/ppermute | solution.py:82
  124.8 35.1 %collective-permute-start.14 = (bf16[96,2048]{1,0:T(8,128)(2,1)S(1)}, bf16[96,2048]{1,0:T(8,128)(2,1)S(1)}, u32[]{:S(2)}, u32[]{:S(2)}) collective-permute-start(bf16[96,2048]{1,0:T(8,128)(2,1)S(1)} %slice.830), channel_id=1, source_target_pairs={{0,2},{1,3},{2,4},{3,5},{4,6},{5,7},{6,8},{7,9},{8,10},{9,11},{10,... | collective-permute-start | bytes 1179656 | tf_op jit(solution)/shard_map/ppermute | solution.py:82
  131.2 30.4 %collective-permute-start.17 = (bf16[96,2048]{1,0:T(8,128)(2,1)S(1)}, bf16[96,2048]{1,0:T(8,128)(2,1)S(1)}, u32[]{:S(2)}, u32[]{:S(2)}) collective-permute-start(bf16[96,2048]{1,0:T(8,128)(2,1)S(1)} %slice.832), channel_id=1, source_target_pairs={{0,30},{1,31},{2,0},{3,1},{4,2},{5,3},{6,4},{7,5},{8,6},{9,7},{10,... | collective-permute-start | bytes 1179656 | tf_op jit(solution)/shard_map/ppermute | solution.py:82
  161.6 36.2 %collective-permute-start.20 = (bf16[40,2048]{1,0:T(8,128)(2,1)S(1)}, bf16[40,2048]{1,0:T(8,128)(2,1)S(1)}, u32[]{:S(2)}, u32[]{:S(2)}) collective-permute-start(bf16[40,2048]{1,0:T(8,128)(2,1)S(1)} %slice.834), channel_id=1, source_target_pairs={{0,2},{1,3},{2,4},{3,5},{4,6},{5,7},{6,8},{7,9},{8,10},{9,11},{10,... | collective-permute-start | bytes 491528 | tf_op jit(solution)/shard_map/ppermute | solution.py:82
  162.1 52.8 %collective-permute-start.23 = (bf16[40,2048]{1,0:T(8,128)(2,1)S(1)}, bf16[40,2048]{1,0:T(8,128)(2,1)S(1)}, u32[]{:S(2)}, u32[]{:S(2)}) collective-permute-start(bf16[40,2048]{1,0:T(8,128)(2,1)S(1)} %slice.836), channel_id=1, source_target_pairs={{0,30},{1,31},{2,0},{3,1},{4,2},{5,3},{6,4},{7,5},{8,6},{9,7},{10,... | collective-permute-start | bytes 491528 | tf_op jit(solution)/shard_map/ppermute | solution.py:82
  165.9 31.2 %collective-permute-start.19 = (bf16[328,1024]{1,0:T(8,128)(2,1)S(1)}, bf16[328,1024]{1,0:T(8,128)(2,1)S(1)}, u32[]{:S(2)}, u32[]{:S(2)}) collective-permute-start(bf16[328,1024]{1,0:T(8,128)(2,1)S(1)} %collective-permute-done.13), channel_id=1, source_target_pairs={{0,2},{1,3},{2,4},{3,5},{4,6},{5,7},{6,8},{7,9},{8,10},{9,11},{10,... | collective-permute-start | bytes 2015240 | tf_op jit(solution)/shard_map/ppermute | solution.py:82
  184.7 26.1 %collective-permute-start.21 = (bf16[328,1024]{1,0:T(8,128)(2,1)S(1)}, bf16[328,1024]{1,0:T(8,128)(2,1)S(1)}, u32[]{:S(2)}, u32[]{:S(2)}) collective-permute-start(bf16[328,1024]{1,0:T(8,128)(2,1)S(1)} %collective-permute-done.15), channel_id=1, source_target_pairs={{0,30},{1,31},{2,0},{3,1},{4,2},{5,3},{6,4},{7,5},{8,6},{9,7},{10,... | collective-permute-start | bytes 2015240 | tf_op jit(solution)/shard_map/ppermute | solution.py:82
  197.4 33.2 %collective-permute-start.35 = (bf16[328,1024]{1,0:T(8,128)(2,1)S(1)}, bf16[328,1024]{1,0:T(8,128)(2,1)S(1)}, u32[]{:S(2)}, u32[]{:S(2)}) collective-permute-start(bf16[328,1024]{1,0:T(8,128)(2,1)S(1)} %collective-permute-done.19), channel_id=1, source_target_pairs={{0,2},{1,3},{2,4},{3,5},{4,6},{5,7},{6,8},{7,9},{8,10},{9,11},{10,... | collective-permute-start | bytes 2015240 | tf_op jit(solution)/shard_map/ppermute | solution.py:82
  197.9 32.9 %collective-permute-start.37 = (bf16[328,1024]{1,0:T(8,128)(2,1)S(1)}, bf16[328,1024]{1,0:T(8,128)(2,1)S(1)}, u32[]{:S(2)}, u32[]{:S(2)}) collective-permute-start(bf16[328,1024]{1,0:T(8,128)(2,1)S(1)} %collective-permute-done.22), channel_id=1, source_target_pairs={{0,30},{1,31},{2,0},{3,1},{4,2},{5,3},{6,4},{7,5},{8,6},{9,7},{10,... | collective-permute-start | bytes 2015240 | tf_op jit(solution)/shard_map/ppermute | solution.py:82
  210.9 28.8 %collective-permute-start.36 = (bf16[328,1024]{1,0:T(8,128)(2,1)S(1)}, bf16[328,1024]{1,0:T(8,128)(2,1)S(1)}, u32[]{:S(2)}, u32[]{:S(2)}) collective-permute-start(bf16[328,1024]{1,0:T(8,128)(2,1)S(1)} %collective-permute-done.21), channel_id=1, source_target_pairs={{0,30},{1,31},{2,0},{3,1},{4,2},{5,3},{6,4},{7,5},{8,6},{9,7},{10,... | collective-permute-start | bytes 2015240 | tf_op jit(solution)/shard_map/ppermute | solution.py:82
  215.3 73.7 %collective-permute-start.24 = (bf16[432,2048]{1,0:T(8,128)(2,1)S(1)}, bf16[432,2048]{1,0:T(8,128)(2,1)S(1)}, u32[]{:S(2)}, u32[]{:S(2)}) collective-permute-start(bf16[432,2048]{1,0:T(8,128)(2,1)S(1)} %get-tuple-element.98), channel_id=1, source_target_pairs={{0,1},{1,0},{2,3},{3,2},{4,5},{5,4},{6,7},{7,6},{8,9},{9,8},{10,11... | collective-permute-start | bytes 5308424 | tf_op jit(solution)/shard_map/ppermute | solution.py:157
  216.3 29.9 %collective-permute-start.38 = (bf16[264,1024]{1,0:T(8,128)(2,1)S(1)}, bf16[264,1024]{1,0:T(8,128)(2,1)S(1)}, u32[]{:S(2)}, u32[]{:S(2)}) collective-permute-start(bf16[264,1024]{1,0:T(8,128)(2,1)S(1)} %slice.873), channel_id=1, source_target_pairs={{0,2},{1,3},{2,4},{3,5},{4,6},{5,7},{6,8},{7,9},{8,10},{9,11},{10,... | collective-permute-start | bytes 1622024 | tf_op jit(solution)/shard_map/ppermute | solution.py:82
  246.3 23.1 %collective-permute-start.42 = (bf16[224,1024]{1,0:T(8,128)(2,1)S(1)}, bf16[224,1024]{1,0:T(8,128)(2,1)S(1)}, u32[]{:S(2)}, u32[]{:S(2)}) collective-permute-start(bf16[224,1024]{1,0:T(8,128)(2,1)S(1)} %slice.881), channel_id=1, source_target_pairs={{0,2},{1,3},{2,4},{3,5},{4,6},{5,7},{6,8},{7,9},{8,10},{9,11},{10,... | collective-permute-start | bytes 1376264 | tf_op jit(solution)/shard_map/ppermute | solution.py:82
  269.4 33.2 %collective-permute-start.46 = (bf16[144,1024]{1,0:T(8,128)(2,1)S(1)}, bf16[144,1024]{1,0:T(8,128)(2,1)S(1)}, u32[]{:S(2)}, u32[]{:S(2)}) collective-permute-start(bf16[144,1024]{1,0:T(8,128)(2,1)S(1)} %slice.889), channel_id=1, source_target_pairs={{0,2},{1,3},{2,4},{3,5},{4,6},{5,7},{6,8},{7,9},{8,10},{9,11},{10,... | collective-permute-start | bytes 884744 | tf_op jit(solution)/shard_map/ppermute | solution.py:82
  273.5 29.3 %collective-permute-start.47 = (bf16[144,1024]{1,0:T(8,128)(2,1)S(1)}, bf16[144,1024]{1,0:T(8,128)(2,1)S(1)}, u32[]{:S(2)}, u32[]{:S(2)}) collective-permute-start(bf16[144,1024]{1,0:T(8,128)(2,1)S(1)} %slice.890), channel_id=1, source_target_pairs={{0,2},{1,3},{2,4},{3,5},{4,6},{5,7},{6,8},{7,9},{8,10},{9,11},{10,... | collective-permute-start | bytes 884744 | tf_op jit(solution)/shard_map/ppermute | solution.py:82
  273.7 29.3 %collective-permute-start.49 = (bf16[144,1024]{1,0:T(8,128)(2,1)S(1)}, bf16[144,1024]{1,0:T(8,128)(2,1)S(1)}, u32[]{:S(2)}, u32[]{:S(2)}) collective-permute-start(bf16[144,1024]{1,0:T(8,128)(2,1)S(1)} %slice.894), channel_id=1, source_target_pairs={{0,30},{1,31},{2,0},{3,1},{4,2},{5,3},{6,4},{7,5},{8,6},{9,7},{10,... | collective-permute-start | bytes 884744 | tf_op jit(solution)/shard_map/ppermute | solution.py:82
  282.5 23.8 %collective-permute-start.48 = (bf16[144,1024]{1,0:T(8,128)(2,1)S(1)}, bf16[144,1024]{1,0:T(8,128)(2,1)S(1)}, u32[]{:S(2)}, u32[]{:S(2)}) collective-permute-start(bf16[144,1024]{1,0:T(8,128)(2,1)S(1)} %slice.893), channel_id=1, source_target_pairs={{0,30},{1,31},{2,0},{3,1},{4,2},{5,3},{6,4},{7,5},{8,6},{9,7},{10,... | collective-permute-start | bytes 884744 | tf_op jit(solution)/shard_map/ppermute | solution.py:82
  347.7 34.4 %collective-permute-start.55 = (bf16[480,2048]{1,0:T(8,128)(2,1)S(1)}, bf16[480,2048]{1,0:T(8,128)(2,1)S(1)}, u32[]{:S(2)}, u32[]{:S(2)}) collective-permute-start(bf16[480,2048]{1,0:T(8,128)(2,1)S(1)} %slice.906), channel_id=1, source_target_pairs={{0,1},{1,0},{2,3},{3,2},{4,5},{5,4},{6,7},{7,6},{8,9},{9,8},{10,11... | collective-permute-start | bytes 5898248 | tf_op jit(solution)/shard_map/ppermute | solution.py:159
  370.6 130.5 %collective-permute-start.29 = (bf16[200,2048]{1,0:T(8,128)(2,1)S(1)}, bf16[200,2048]{1,0:T(8,128)(2,1)S(1)}, u32[]{:S(2)}, u32[]{:S(2)}) collective-permute-start(bf16[200,2048]{1,0:T(8,128)(2,1)S(1)} %fusion.43), channel_id=1, source_target_pairs={{0,2},{1,3},{2,4},{3,5},{4,6},{5,7},{6,8},{7,9},{8,10},{9,11},{10,... | collective-permute-start | bytes 2457608 | tf_op jit(solution)/shard_map/ppermute | solution.py:82
  378.3 126.3 %collective-permute-start.33 = (bf16[200,2048]{1,0:T(8,128)(2,1)S(1)}, bf16[200,2048]{1,0:T(8,128)(2,1)S(1)}, u32[]{:S(2)}, u32[]{:S(2)}) collective-permute-start(bf16[200,2048]{1,0:T(8,128)(2,1)S(1)} %fusion.44), channel_id=1, source_target_pairs={{0,30},{1,31},{2,0},{3,1},{4,2},{5,3},{6,4},{7,5},{8,6},{9,7},{10,... | collective-permute-start | bytes 2457608 | tf_op jit(solution)/shard_map/ppermute | solution.py:82
  403.6 25.7 %collective-permute-start.84 = (bf16[144,1024]{1,0:T(8,128)(2,1)S(1)}, bf16[144,1024]{1,0:T(8,128)(2,1)S(1)}, u32[]{:S(2)}, u32[]{:S(2)}) collective-permute-start(bf16[144,1024]{1,0:T(8,128)(2,1)S(1)} %fusion.86), channel_id=1, source_target_pairs={{0,2},{1,3},{2,4},{3,5},{4,6},{5,7},{6,8},{7,9},{8,10},{9,11},{10,... | collective-permute-start | bytes 884744 | tf_op jit(solution)/shard_map/ppermute | solution.py:82
  468.2 25.5 %collective-permute-start.78 = (bf16[328,1024]{1,0:T(8,128)(2,1)S(1)}, bf16[328,1024]{1,0:T(8,128)(2,1)S(1)}, u32[]{:S(2)}, u32[]{:S(2)}) collective-permute-start(bf16[328,1024]{1,0:T(8,128)(2,1)S(1)} %fusion.69), channel_id=1, source_target_pairs={{0,30},{1,31},{2,0},{3,1},{4,2},{5,3},{6,4},{7,5},{8,6},{9,7},{10,... | collective-permute-start | bytes 2015240 | tf_op jit(solution)/shard_map/ppermute | solution.py:82
  470.3 27.6 %collective-permute-start.69 = (bf16[328,1024]{1,0:T(8,128)(2,1)S(1)}, bf16[328,1024]{1,0:T(8,128)(2,1)S(1)}, u32[]{:S(2)}, u32[]{:S(2)}) collective-permute-start(bf16[328,1024]{1,0:T(8,128)(2,1)S(1)} %fusion.64), channel_id=1, source_target_pairs={{0,2},{1,3},{2,4},{3,5},{4,6},{5,7},{6,8},{7,9},{8,10},{9,11},{10,... | collective-permute-start | bytes 2015240 | tf_op jit(solution)/shard_map/ppermute | solution.py:82
  497.9 29.4 %collective-permute-start.79 = (bf16[328,1024]{1,0:T(8,128)(2,1)S(1)}, bf16[328,1024]{1,0:T(8,128)(2,1)S(1)}, u32[]{:S(2)}, u32[]{:S(2)}) collective-permute-start(bf16[328,1024]{1,0:T(8,128)(2,1)S(1)} %fusion.68), channel_id=1, source_target_pairs={{0,30},{1,31},{2,0},{3,1},{4,2},{5,3},{6,4},{7,5},{8,6},{9,7},{10,... | collective-permute-start | bytes 2015240 | tf_op jit(solution)/shard_map/ppermute | solution.py:82
  500.0 31.5 %collective-permute-start.70 = (bf16[328,1024]{1,0:T(8,128)(2,1)S(1)}, bf16[328,1024]{1,0:T(8,128)(2,1)S(1)}, u32[]{:S(2)}, u32[]{:S(2)}) collective-permute-start(bf16[328,1024]{1,0:T(8,128)(2,1)S(1)} %fusion.63), channel_id=1, source_target_pairs={{0,2},{1,3},{2,4},{3,5},{4,6},{5,7},{6,8},{7,9},{8,10},{9,11},{10,... | collective-permute-start | bytes 2015240 | tf_op jit(solution)/shard_map/ppermute | solution.py:82
  501.0 31.1 %collective-permute-start.88 = (bf16[328,1024]{1,0:T(8,128)(2,1)S(1)}, bf16[328,1024]{1,0:T(8,128)(2,1)S(1)}, u32[]{:S(2)}, u32[]{:S(2)}) collective-permute-start(bf16[328,1024]{1,0:T(8,128)(2,1)S(1)} %fusion.73), channel_id=1, source_target_pairs={{0,2},{1,3},{2,4},{3,5},{4,6},{5,7},{6,8},{7,9},{8,10},{9,11},{10,... | collective-permute-start | bytes 2015240 | tf_op jit(solution)/shard_map/ppermute | solution.py:82
  513.3 42.5 %collective-permute-start.62 = (bf16[328,1024]{1,0:T(8,128)(2,1)S(1)}, bf16[328,1024]{1,0:T(8,128)(2,1)S(1)}, u32[]{:S(2)}, u32[]{:S(2)}) collective-permute-start(bf16[328,1024]{1,0:T(8,128)(2,1)S(1)} %fusion.59), channel_id=1, source_target_pairs={{0,30},{1,31},{2,0},{3,1},{4,2},{5,3},{6,4},{7,5},{8,6},{9,7},{10,... | collective-permute-start | bytes 2015240 | tf_op jit(solution)/shard_map/ppermute | solution.py:82
  527.7 23.9 %collective-permute-start.80 = (bf16[328,1024]{1,0:T(8,128)(2,1)S(1)}, bf16[328,1024]{1,0:T(8,128)(2,1)S(1)}, u32[]{:S(2)}, u32[]{:S(2)}) collective-permute-start(bf16[328,1024]{1,0:T(8,128)(2,1)S(1)} %fusion.67), channel_id=1, source_target_pairs={{0,30},{1,31},{2,0},{3,1},{4,2},{5,3},{6,4},{7,5},{8,6},{9,7},{10,... | collective-permute-start | bytes 2015240 | tf_op jit(solution)/shard_map/ppermute | solution.py:82
  532.0 27.0 %collective-permute-start.71 = (bf16[328,1024]{1,0:T(8,128)(2,1)S(1)}, bf16[328,1024]{1,0:T(8,128)(2,1)S(1)}, u32[]{:S(2)}, u32[]{:S(2)}) collective-permute-start(bf16[328,1024]{1,0:T(8,128)(2,1)S(1)} %fusion.62), channel_id=1, source_target_pairs={{0,2},{1,3},{2,4},{3,5},{4,6},{5,7},{6,8},{7,9},{8,10},{9,11},{10,... | collective-permute-start | bytes 2015240 | tf_op jit(solution)/shard_map/ppermute | solution.py:82
  532.6 25.4 %collective-permute-start.89 = (bf16[328,1024]{1,0:T(8,128)(2,1)S(1)}, bf16[328,1024]{1,0:T(8,128)(2,1)S(1)}, u32[]{:S(2)}, u32[]{:S(2)}) collective-permute-start(bf16[328,1024]{1,0:T(8,128)(2,1)S(1)} %fusion.72), channel_id=1, source_target_pairs={{0,2},{1,3},{2,4},{3,5},{4,6},{5,7},{6,8},{7,9},{8,10},{9,11},{10,... | collective-permute-start | bytes 2015240 | tf_op jit(solution)/shard_map/ppermute | solution.py:82
  556.3 29.4 %collective-permute-start.63 = (bf16[328,1024]{1,0:T(8,128)(2,1)S(1)}, bf16[328,1024]{1,0:T(8,128)(2,1)S(1)}, u32[]{:S(2)}, u32[]{:S(2)}) collective-permute-start(bf16[328,1024]{1,0:T(8,128)(2,1)S(1)} %fusion.58), channel_id=1, source_target_pairs={{0,30},{1,31},{2,0},{3,1},{4,2},{5,3},{6,4},{7,5},{8,6},{9,7},{10,... | collective-permute-start | bytes 2015240 | tf_op jit(solution)/shard_map/ppermute | solution.py:82
  558.4 31.5 %collective-permute-start.90 = (bf16[328,1024]{1,0:T(8,128)(2,1)S(1)}, bf16[328,1024]{1,0:T(8,128)(2,1)S(1)}, u32[]{:S(2)}, u32[]{:S(2)}) collective-permute-start(bf16[328,1024]{1,0:T(8,128)(2,1)S(1)} %fusion.71), channel_id=1, source_target_pairs={{0,2},{1,3},{2,4},{3,5},{4,6},{5,7},{6,8},{7,9},{8,10},{9,11},{10,... | collective-permute-start | bytes 2015240 | tf_op jit(solution)/shard_map/ppermute | solution.py:82
  559.5 31.1 %collective-permute-start.72 = (bf16[328,1024]{1,0:T(8,128)(2,1)S(1)}, bf16[328,1024]{1,0:T(8,128)(2,1)S(1)}, u32[]{:S(2)}, u32[]{:S(2)}) collective-permute-start(bf16[328,1024]{1,0:T(8,128)(2,1)S(1)} %fusion.61), channel_id=1, source_target_pairs={{0,2},{1,3},{2,4},{3,5},{4,6},{5,7},{6,8},{7,9},{8,10},{9,11},{10,... | collective-permute-start | bytes 2015240 | tf_op jit(solution)/shard_map/ppermute | solution.py:82
  571.8 28.0 %collective-permute-start.82 = (bf16[328,1024]{1,0:T(8,128)(2,1)S(1)}, bf16[328,1024]{1,0:T(8,128)(2,1)S(1)}, u32[]{:S(2)}, u32[]{:S(2)}) collective-permute-start(bf16[328,1024]{1,0:T(8,128)(2,1)S(1)} %fusion.65), channel_id=1, source_target_pairs={{0,30},{1,31},{2,0},{3,1},{4,2},{5,3},{6,4},{7,5},{8,6},{9,7},{10,... | collective-permute-start | bytes 2015240 | tf_op jit(solution)/shard_map/ppermute | solution.py:82
  (120 other events, 3945.5 us)
